TPU v7x, 512 devices: a whole 4x8x8 slice. The times are simulated.
512 devices in a mesh: sp: 64 (over z, y), tp: 8 (over x, core).
Axes of the slice: x: 4, y: 8, z: 8, core: 2. Of those that a mesh axis runs over, the one named last changes fastest.
Arguments:
- resid: bfloat16 [8192, 2048], P(('sp', 'tp')), may hold values from -3 to 3
- queries: bfloat16 [8192, 2048], P('sp', 'tp'), may hold values from -6 to 6
- keys: bfloat16 [8192, 2048], P('sp', 'tp'), may hold values from -6 to 6
- values: bfloat16 [8192, 2048], P('sp', 'tp'), may hold values from -8 to 8
- doc_ids: int32 [8192], P('sp'), may hold values from 0 to 15, never falling along the last dimension, each value on 1 to 896 neighbouring positions
- score_offset: float32 [32], P('tp'), may hold values from -10 to -3
- out_weight: bfloat16 [2048, 2048], P('tp'), may hold values from -0.1875 to 0.1875
- norm_gain: float32 [2048], replicated, may hold values from 0.1 to 1.9
- gate_weight: bfloat16 [2048, 6144], P('sp', 'tp'), may hold values from -0.125 to 0.125
- up_weight: bfloat16 [2048, 6144], P('sp', 'tp'), may hold values from -0.125 to 0.125
- down_weight: bfloat16 [6144, 2048], P('tp', 'sp'), may hold values from -0.078125 to 0.078125
Outputs:
- layer_out: bfloat16 [8192, 2048], P(('sp', 'tp'))
Inputs may be any that keep to these rules, and one draw needn't show every extreme that they name: `doc_ids`: document numbers never fall along the sequence; each document has 1 to 896 positions, and one has exactly 896.
All inputs are finite; a program needn't handle non-finite values.
Results may differ from a plain program's by a relative error of at most 0.017.
Values may be sent and summed in bfloat16 or wider, within the bound.
No kernel may reach another device: no remote copies, remote signals or barrier semaphores. Data moves between devices by JAX's collectives and lax.ppermute only.
A program may use at most 64 MiB of HBM per device.

v0:
```python
import jax
import jax.numpy as jnp
from jax import lax
from jax.sharding import PartitionSpec as P


def from_behind(shard, axis, by):
    peers = lax.axis_size(axis)
    pairs = [(i, i + by) for i in range(peers) if 0 <= i + by < peers]
    return lax.ppermute(shard, axis, pairs)


def cut_along(shard, dim, peers):
    lengths = shard.shape
    tiles = shard.reshape(*lengths[:dim], peers, lengths[dim] // peers, *lengths[dim + 1 :])
    return jnp.moveaxis(tiles, dim, 0)


def sent_and_summed(shard, axis, dim):
    peers = lax.axis_size(axis)
    tiles = lax.all_to_all(cut_along(shard, dim, peers), axis, 0, 0, tiled=True)
    return jnp.sum(tiles.astype(jnp.float32), axis=0)


def joined_along(tiles, dim):
    lengths = list(tiles.shape[1:])
    lengths[dim] *= tiles.shape[0]
    return jnp.moveaxis(tiles, 0, dim).reshape(lengths)


def from_everyone(shard, axis):
    copies = jnp.broadcast_to(shard, (lax.axis_size(axis), *shard.shape))
    return lax.all_to_all(copies, axis, split_axis=0, concat_axis=0, tiled=True)


def gather_directly(shard, axis, dim):
    return joined_along(from_everyone(shard, axis), dim)


def sent_together(arrays, axis, dim, along):
    both = jnp.concatenate(arrays, axis=along)
    out, at, done = (lax.all_gather(both, axis, axis=dim, tiled=True), 0, [])
    for a in arrays:
        done.append(lax.slice_in_dim(out, at, at + a.shape[along], axis=along))
        at += a.shape[along]
    return tuple(done)


def joined(earlier, later):
    return (
        jnp.concatenate([earlier[0], later[0]], axis=0),
        jnp.concatenate([earlier[1], later[1]], axis=0),
        jnp.concatenate([earlier[2], later[2]], axis=0),
    )


def block_update(carry, block, start, context):
    queries_h, q_pos, q_docs, offsets, scale = context
    total, carried = carry
    k_block, v_block, d_block = block
    count = k_block.shape[0]
    heads = offsets.shape[0]
    head_dim = queries_h.shape[2]

    def compute():
        key_pos = start + jnp.arange(count, dtype=jnp.int32)
        live = (
            (key_pos[None, :] >= 0)
            & (key_pos[None, :] < q_pos[:, None])
            & (d_block[None, :] == q_docs[:, None])
        )
        k_heads = k_block.reshape(count, heads, head_dim)
        v_heads = v_block.reshape(count, heads, head_dim)
        scores = (
            jnp.einsum("thd,shd->hts", queries_h, k_heads, preferred_element_type=jnp.float32)
            * scale
            + offsets[:, None, None]
        )
        log_keep = jnp.where(live[None], jax.nn.log_sigmoid(-scores), 0.0)
        tail = lax.cumsum(log_keep, axis=2, reverse=True) - log_keep + carried[:, :, None]
        weight = jnp.where(live[None], jnp.exp(jax.nn.log_sigmoid(scores) + tail), 0.0).astype(
            jnp.bfloat16
        )
        added = jnp.einsum("hts,shd->thd", weight, v_heads, preferred_element_type=jnp.float32)
        return (total + added, carried + jnp.sum(log_keep, axis=2))

    reached = (start + count > 0) & (d_block[-1] >= q_docs[0])
    return lax.cond(reached, compute, lambda: carry)


def on_device(
    resid,
    queries,
    keys,
    values,
    doc_ids,
    score_offset,
    out_weight,
    norm_gain,
    gate_weight,
    up_weight,
    down_weight,
):
    rows = queries.shape[0]
    heads = score_offset.shape[0]
    head_dim = queries.shape[1] // heads
    base = lax.axis_index("sp") * rows
    q_pos = base + jnp.arange(rows, dtype=jnp.int32)
    context = (
        queries.reshape(rows, heads, head_dim),
        q_pos,
        doc_ids,
        score_offset,
        head_dim ** (-0.5),
    )
    own = (keys, values, doc_ids)
    carry = (jnp.zeros((rows, heads, head_dim), jnp.float32), jnp.zeros((heads, rows), jnp.float32))
    arrived = own
    later = own
    for back in range(1, 8):
        arrived = from_behind((arrived[0], arrived[1], arrived[2]), "sp", 1)
        if back % 2 == 1:
            carry = block_update(carry, joined(arrived, later), base - back * rows, context)
        else:
            later = arrived
    attended = carry[0].reshape(rows, heads * head_dim).astype(jnp.bfloat16)
    mixed_attn = sent_and_summed(
        jnp.dot(attended, out_weight, preferred_element_type=jnp.float32).astype(jnp.bfloat16),
        "tp",
        0,
    )
    stream = resid.astype(jnp.float32) + mixed_attn
    normed = (
        stream * lax.rsqrt(jnp.mean(stream * stream, axis=1, keepdims=True) + 1e-06) * norm_gain
    ).astype(jnp.bfloat16)
    span_rows = gather_directly(normed, "tp", 0)
    pieces = sent_together((gate_weight, up_weight), "sp", 0, 1)
    gate = jnp.dot(span_rows, pieces[0], preferred_element_type=jnp.float32)
    upper = jnp.dot(span_rows, pieces[1], preferred_element_type=jnp.float32)
    hidden = (jax.nn.silu(gate) * upper).astype(jnp.bfloat16)
    partial_out = jnp.dot(
        hidden,
        lax.all_gather(down_weight, "sp", axis=1, tiled=True),
        preferred_element_type=jnp.float32,
    )
    feed = sent_and_summed(partial_out.astype(jnp.bfloat16), "tp", 0)
    return (stream + feed).astype(jnp.bfloat16)


def solution(mesh):
    in_specs = (
        P(("sp", "tp"), None),
        P("sp", "tp"),
        P("sp", "tp"),
        P("sp", "tp"),
        P("sp"),
        P("tp"),
        P("tp", None),
        P(),
        P("sp", "tp"),
        P("sp", "tp"),
        P("tp", "sp"),
    )
    out_specs = P(("sp", "tp"), None)
    return jax.shard_map(
        on_device, mesh=mesh, in_specs=in_specs, out_specs=out_specs, check_vma=False
    )
```

profile of v0, /device:TPU:1, one launch (start us, length us, event | category | flops | bytes accessed | tf_op | source)
XLA Modules:
  0.0 225.3 jit_solution(14189140103926369568)
XLA Ops:
  8.9 4.0 %collective-permute-start = (s32[128]{0:T(128)}, s32[128]{0:T(128)S(1)}, u32[]{:S(2)}, u32[]{:S(2)}) collective-permute-start(s32[128]{0:T(128)} %param.23), channel_id=1, source_target_pairs={{0,8},{8,16},{16,24},{24,32},{32,40},{40,48},{48,56},{56,64},{64,7... | collective-permute-start | bytes 1544 | tf_op jit(solution)/shard_map/ppermute | solution.py:10
  13.9 3.2 %collective-permute-start.7 = (bf16[128,256]{0,1:T(8,128)(2,1)S(1)}, bf16[128,256]{0,1:T(8,128)(2,1)S(1)}, u32[]{:S(2)}, u32[]{:S(2)}) collective-permute-start(bf16[128,256]{0,1:T(8,128)(2,1)S(1)} %copy.23), channel_id=1, source_target_pairs={{0,8},{8,16},{16,24},{24,32},{32,40},{40,48},{48,56},{56,64},{64,7... | collective-permute-start | bytes 196616 | tf_op jit(solution)/shard_map/ppermute | solution.py:10
  18.0 3.2 %collective-permute-start.6 = (bf16[128,256]{0,1:T(8,128)(2,1)S(1)}, bf16[128,256]{0,1:T(8,128)(2,1)S(1)}, u32[]{:S(2)}, u32[]{:S(2)}) collective-permute-start(bf16[128,256]{0,1:T(8,128)(2,1)S(1)} %copy.20), channel_id=1, source_target_pairs={{0,8},{8,16},{16,24},{24,32},{32,40},{40,48},{48,56},{56,64},{64,7... | collective-permute-start | bytes 196616 | tf_op jit(solution)/shard_map/ppermute | solution.py:10
  22.6 4.4 %collective-permute-start.1 = (s32[128]{0:T(128)S(1)}, s32[128]{0:T(128)S(1)}, u32[]{:S(2)}, u32[]{:S(2)}) collective-permute-start(s32[128]{0:T(128)S(1)} %collective-permute-done), channel_id=1, source_target_pairs={{0,8},{8,16},{16,24},{24,32},{32,40},{40,48},{48,56},{56,64},{64,7... | collective-permute-start | bytes 1544 | tf_op jit(solution)/shard_map/ppermute | solution.py:10
  27.7 3.6 %collective-permute-start.2 = (s32[128]{0:T(128)S(1)}, s32[128]{0:T(128)S(1)}, u32[]{:S(2)}, u32[]{:S(2)}) collective-permute-start(s32[128]{0:T(128)S(1)} %collective-permute-done.1), channel_id=1, source_target_pairs={{0,8},{8,16},{16,24},{24,32},{32,40},{40,48},{48,56},{56,64},{64,7... | collective-permute-start | bytes 1544 | tf_op jit(solution)/shard_map/ppermute | solution.py:10
  32.0 3.6 %collective-permute-start.3 = (s32[128]{0:T(128)S(1)}, s32[128]{0:T(128)S(1)}, u32[]{:S(2)}, u32[]{:S(2)}) collective-permute-start(s32[128]{0:T(128)S(1)} %collective-permute-done.2), channel_id=1, source_target_pairs={{0,8},{8,16},{16,24},{24,32},{32,40},{40,48},{48,56},{56,64},{64,7... | collective-permute-start | bytes 1544 | tf_op jit(solution)/shard_map/ppermute | solution.py:10
  46.9 4.7 %collective-permute-start.16 = (s32[128]{0:T(128)S(1)}, s32[128]{0:T(128)S(1)}, u32[]{:S(2)}, u32[]{:S(2)}) collective-permute-start(s32[128]{0:T(128)S(1)} %collective-permute-done.5), channel_id=1, source_target_pairs={{0,8},{8,16},{16,24},{24,32},{32,40},{40,48},{48,56},{56,64},{64,7... | collective-permute-start | bytes 1544 | tf_op jit(solution)/shard_map/ppermute | solution.py:10
  54.2 4.3 %collective-permute-start.10 = (bf16[128,256]{0,1:T(8,128)(2,1)S(1)}, bf16[128,256]{0,1:T(8,128)(2,1)}, u32[]{:S(2)}, u32[]{:S(2)}) collective-permute-start(bf16[128,256]{0,1:T(8,128)(2,1)S(1)} %collective-permute-done.7), channel_id=1, source_target_pairs={{0,8},{8,16},{16,24},{24,32},{32,40},{40,48},{48,56},{56,64},{64,7... | collective-permute-start | bytes 196616 | tf_op jit(solution)/shard_map/ppermute | solution.py:10
  58.5 3.0 %collective-permute-start.8 = (bf16[128,256]{0,1:T(8,128)(2,1)S(1)}, bf16[128,256]{0,1:T(8,128)(2,1)}, u32[]{:S(2)}, u32[]{:S(2)}) collective-permute-start(bf16[128,256]{0,1:T(8,128)(2,1)S(1)} %collective-permute-done.6), channel_id=1, source_target_pairs={{0,8},{8,16},{16,24},{24,32},{32,40},{40,48},{48,56},{56,64},{64,7... | collective-permute-start | bytes 196616 | tf_op jit(solution)/shard_map/ppermute | solution.py:10
  61.5 3.6 %collective-permute-start.11 = (bf16[128,256]{0,1:T(8,128)(2,1)}, bf16[128,256]{0,1:T(8,128)(2,1)}, u32[]{:S(2)}, u32[]{:S(2)}) collective-permute-start(bf16[128,256]{0,1:T(8,128)(2,1)} %collective-permute-done.10), channel_id=1, source_target_pairs={{0,8},{8,16},{16,24},{24,32},{32,40},{40,48},{48,56},{56,64},{64,7... | collective-permute-start | bytes 196616 | tf_op jit(solution)/shard_map/ppermute | solution.py:10
  65.1 4.4 %collective-permute-start.9 = (bf16[128,256]{0,1:T(8,128)(2,1)}, bf16[128,256]{0,1:T(8,128)(2,1)}, u32[]{:S(2)}, u32[]{:S(2)}) collective-permute-start(bf16[128,256]{0,1:T(8,128)(2,1)} %collective-permute-done.8), channel_id=1, source_target_pairs={{0,8},{8,16},{16,24},{24,32},{32,40},{40,48},{48,56},{56,64},{64,7... | collective-permute-start | bytes 196616 | tf_op jit(solution)/shard_map/ppermute | solution.py:10
  69.6 9.3 %conditional.4 = (f32[128,4,64]{0,2,1:T(8,128)S(1)}, f32[4,128]{1,0:T(4,128)S(1)}) conditional(s32[]{:T(128)} %convert_element_type.66, () %tuple.49, (s32[]{:T(128)}, s32[128]{0:T(128)S(1)}, s32[256]{0:T(256)S(1)}, s32[128]{0:T(128)}, bf16[256,256]{0,1:T(8,128)(2,1)S(1)}, /*index=5*/bf16[128,4,64]{0,2,1:T(8,128)(2,1)S(1)}, f32[4]{0:T(128)}, ...), branch_computations={%region_0.0_spmd, %region_1.5_spmd} | conditional | flops 55936768 | bytes 10654308 | solution.py:88
  72.6 4.3 %fusion.69 = f32[4,128,2,128]{1,2,3,0:T(2,128)S(1)} fusion(f32[4,128,2,128]{1,2,3,0:T(2,128)S(1)} %copy.12), kind=kOutput, calls=%fused_computation.123 | output fusion | flops 16646144 | bytes 1048576 | tf_op jit(solution)/shard_map/reduce-window
  78.9 4.2 %collective-permute-start.14 = (bf16[128,256]{0,1:T(8,128)(2,1)}, bf16[128,256]{0,1:T(8,128)(2,1)}, u32[]{:S(2)}, u32[]{:S(2)}) collective-permute-start(bf16[128,256]{0,1:T(8,128)(2,1)} %collective-permute-done.11), channel_id=1, source_target_pairs={{0,8},{8,16},{16,24},{24,32},{32,40},{40,48},{48,56},{56,64},{64,7... | collective-permute-start | bytes 196616 | tf_op jit(solution)/shard_map/ppermute | solution.py:10
  83.1 3.9 %collective-permute-start.12 = (bf16[128,256]{0,1:T(8,128)(2,1)}, bf16[128,256]{0,1:T(8,128)(2,1)}, u32[]{:S(2)}, u32[]{:S(2)}) collective-permute-start(bf16[128,256]{0,1:T(8,128)(2,1)} %collective-permute-done.9), channel_id=1, source_target_pairs={{0,8},{8,16},{16,24},{24,32},{32,40},{40,48},{48,56},{56,64},{64,7... | collective-permute-start | bytes 196616 | tf_op jit(solution)/shard_map/ppermute | solution.py:10
  87.9 4.5 %collective-permute-start.15 = (bf16[128,256]{0,1:T(8,128)(2,1)}, bf16[128,256]{0,1:T(8,128)(2,1)}, u32[]{:S(2)}, u32[]{:S(2)}) collective-permute-start(bf16[128,256]{0,1:T(8,128)(2,1)} %collective-permute-done.14), channel_id=1, source_target_pairs={{0,8},{8,16},{16,24},{24,32},{32,40},{40,48},{48,56},{56,64},{64,7... | collective-permute-start | bytes 196616 | tf_op jit(solution)/shard_map/ppermute | solution.py:10
  92.4 3.8 %collective-permute-start.13 = (bf16[128,256]{0,1:T(8,128)(2,1)}, bf16[128,256]{0,1:T(8,128)(2,1)}, u32[]{:S(2)}, u32[]{:S(2)}) collective-permute-start(bf16[128,256]{0,1:T(8,128)(2,1)} %collective-permute-done.12), channel_id=1, source_target_pairs={{0,8},{8,16},{16,24},{24,32},{32,40},{40,48},{48,56},{56,64},{64,7... | collective-permute-start | bytes 196616 | tf_op jit(solution)/shard_map/ppermute | solution.py:10
  99.7 5.1 %collective-permute-start.17 = (bf16[128,256]{0,1:T(8,128)(2,1)}, bf16[128,256]{0,1:T(8,128)(2,1)}, u32[]{:S(2)}, u32[]{:S(2)}) collective-permute-start(bf16[128,256]{0,1:T(8,128)(2,1)} %collective-permute-done.13), channel_id=1, source_target_pairs={{0,8},{8,16},{16,24},{24,32},{32,40},{40,48},{48,56},{56,64},{64,7... | collective-permute-start | bytes 196616 | tf_op jit(solution)/shard_map/ppermute | solution.py:10
  105.7 11.4 %collective-permute-start.20 = (bf16[128,256]{0,1:T(8,128)(2,1)}, bf16[128,256]{0,1:T(8,128)(2,1)}, u32[]{:S(2)}, u32[]{:S(2)}) collective-permute-start(bf16[128,256]{0,1:T(8,128)(2,1)} %collective-permute-done.19), channel_id=1, source_target_pairs={{0,8},{8,16},{16,24},{24,32},{32,40},{40,48},{48,56},{56,64},{64,7... | collective-permute-start | bytes 196616 | tf_op jit(solution)/shard_map/ppermute | solution.py:10
  122.7 27.5 %all_to_all.15 = bf16[8,16,2048]{2,1,0:T(8,128)(2,1)S(1)} all-to-all(bf16[8,16,2048]{2,1,0:T(8,128)(2,1)S(1)} %bitcast.60), channel_id=1, replica_groups=mesh['sp'=64,'tp'=8] {'tp'}, dimensions={0} | all-to-all | bytes 1048576 | tf_op jit(solution)/shard_map/all_to_all | solution.py:21
  150.6 12.8 %all_to_all.16 = bf16[8,16,2048]{2,1,0:T(8,128)(2,1)S(1)} all-to-all(bf16[8,16,2048]{2,1,0:T(8,128)(2,1)S(1)} %broadcast_in_dim.91), channel_id=1, replica_groups=mesh['sp'=64,'tp'=8] {'tp'}, dimensions={0} | all-to-all | bytes 1048576 | tf_op jit(solution)/shard_map/all_to_all | solution.py:33
  165.9 29.6 %all-gather.5.cloned.1.call-done = bf16[768,2048]{0,1:T(8,128)(2,1)} async-done(((bf16[768,32]{0,1:T(8,128)(2,1)}), bf16[768,2048]{0,1:T(8,128)(2,1)}) %all-gather.5.cloned.1.call-update) | async-done | bytes 3145744 | tf_op jit(solution)/shard_map/all_gather | solution.py:143
  195.4 4.5 %convolution_convert_fusion = bf16[128,2048]{1,0:T(8,128)(2,1)S(1)} fusion(bf16[768,2048]{0,1:T(8,128)(2,1)} %all-gather.5.cloned.1.call-done, bf16[128,2048]{1,0:T(8,128)(2,1)S(1)} %bitcast.69, bf16[2048,1536]{1,0:T(8,128)(2,1)} %all-gather.3.cloned.1.call-done, f32[128,768]{1,0:T(8,128)S(1)} %fusion.50), kind=kOutput, calls=%fused_computation.89 | convolution fusion | flops 806158336 | bytes 7733248 | tf_op jit(solution)/shard_map/dot_general | solution.py:141
  199.9 17.8 %all_to_all.17 = bf16[8,16,2048]{2,1,0:T(8,128)(2,1)S(1)} all-to-all(bf16[8,16,2048]{2,1,0:T(8,128)(2,1)S(1)} %bitcast.70), channel_id=1, replica_groups=mesh['sp'=64,'tp'=8] {'tp'}, dimensions={0} | all-to-all | bytes 1048576 | tf_op jit(solution)/shard_map/all_to_all | solution.py:21
  (88 shorter events, 34.8 us)
Async XLA Ops:
  6.5 115.9 %copy-start = (bf16[256,2048]{1,0:T(8,128)(2,1)S(1)}, bf16[256,2048]{1,0:T(8,128)(2,1)}, u32[]{:S(2)}) copy-start(bf16[256,2048]{1,0:T(8,128)(2,1)} %param.25) | copy-start | bytes 3145732
  6.5 156.9 %all-gather.3.cloned.1.call-start = ((), (), s32[]{:S(2)}) async-start(), calls=%async_computation.3 | async-start | bytes 6389760 | tf_op jit(solution)/shard_map/all_gather | solution.py:42
  8.1 187.3 %all-gather.5.cloned.1.call-start = ((), (), s32[]{:S(2)}) async-start(), calls=%async_computation.4 | async-start | bytes 3194880 | tf_op jit(solution)/shard_map/all_gather | solution.py:143
  8.9 13.7 %collective-permute-start = (s32[128]{0:T(128)}, s32[128]{0:T(128)S(1)}, u32[]{:S(2)}, u32[]{:S(2)}) collective-permute-start(s32[128]{0:T(128)} %param.23), channel_id=1, source_target_pairs={{0,8},{8,16},{16,24},{24,32},{32,40},{40,48},{48,56},{56,64},{64,7... | collective-permute-start | bytes 1544 | tf_op jit(solution)/shard_map/ppermute | solution.py:10
  13.9 40.3 %collective-permute-start.7 = (bf16[128,256]{0,1:T(8,128)(2,1)S(1)}, bf16[128,256]{0,1:T(8,128)(2,1)S(1)}, u32[]{:S(2)}, u32[]{:S(2)}) collective-permute-start(bf16[128,256]{0,1:T(8,128)(2,1)S(1)} %copy.23), channel_id=1, source_target_pairs={{0,8},{8,16},{16,24},{24,32},{32,40},{40,48},{48,56},{56,64},{64,7... | collective-permute-start | bytes 196616 | tf_op jit(solution)/shard_map/ppermute | solution.py:10
  18.0 40.5 %collective-permute-start.6 = (bf16[128,256]{0,1:T(8,128)(2,1)S(1)}, bf16[128,256]{0,1:T(8,128)(2,1)S(1)}, u32[]{:S(2)}, u32[]{:S(2)}) collective-permute-start(bf16[128,256]{0,1:T(8,128)(2,1)S(1)} %copy.20), channel_id=1, source_target_pairs={{0,8},{8,16},{16,24},{24,32},{32,40},{40,48},{48,56},{56,64},{64,7... | collective-permute-start | bytes 196616 | tf_op jit(solution)/shard_map/ppermute | solution.py:10
  22.6 5.1 %collective-permute-start.1 = (s32[128]{0:T(128)S(1)}, s32[128]{0:T(128)S(1)}, u32[]{:S(2)}, u32[]{:S(2)}) collective-permute-start(s32[128]{0:T(128)S(1)} %collective-permute-done), channel_id=1, source_target_pairs={{0,8},{8,16},{16,24},{24,32},{32,40},{40,48},{48,56},{56,64},{64,7... | collective-permute-start | bytes 1544 | tf_op jit(solution)/shard_map/ppermute | solution.py:10
  27.7 4.3 %collective-permute-start.2 = (s32[128]{0:T(128)S(1)}, s32[128]{0:T(128)S(1)}, u32[]{:S(2)}, u32[]{:S(2)}) collective-permute-start(s32[128]{0:T(128)S(1)} %collective-permute-done.1), channel_id=1, source_target_pairs={{0,8},{8,16},{16,24},{24,32},{32,40},{40,48},{48,56},{56,64},{64,7... | collective-permute-start | bytes 1544 | tf_op jit(solution)/shard_map/ppermute | solution.py:10
  32.0 5.8 %collective-permute-start.3 = (s32[128]{0:T(128)S(1)}, s32[128]{0:T(128)S(1)}, u32[]{:S(2)}, u32[]{:S(2)}) collective-permute-start(s32[128]{0:T(128)S(1)} %collective-permute-done.2), channel_id=1, source_target_pairs={{0,8},{8,16},{16,24},{24,32},{32,40},{40,48},{48,56},{56,64},{64,7... | collective-permute-start | bytes 1544 | tf_op jit(solution)/shard_map/ppermute | solution.py:10
  37.8 5.0 %collective-permute-start.4 = (s32[128]{0:T(128)S(1)}, s32[128]{0:T(128)S(1)}, u32[]{:S(2)}, u32[]{:S(2)}) collective-permute-start(s32[128]{0:T(128)S(1)} %collective-permute-done.3), channel_id=1, source_target_pairs={{0,8},{8,16},{16,24},{24,32},{32,40},{40,48},{48,56},{56,64},{64,7... | collective-permute-start | bytes 1544 | tf_op jit(solution)/shard_map/ppermute | solution.py:10
  42.8 4.1 %collective-permute-start.5 = (s32[128]{0:T(128)S(1)}, s32[128]{0:T(128)S(1)}, u32[]{:S(2)}, u32[]{:S(2)}) collective-permute-start(s32[128]{0:T(128)S(1)} %collective-permute-done.4), channel_id=1, source_target_pairs={{0,8},{8,16},{16,24},{24,32},{32,40},{40,48},{48,56},{56,64},{64,7... | collective-permute-start | bytes 1544 | tf_op jit(solution)/shard_map/ppermute | solution.py:10
  46.9 7.3 %collective-permute-start.16 = (s32[128]{0:T(128)S(1)}, s32[128]{0:T(128)S(1)}, u32[]{:S(2)}, u32[]{:S(2)}) collective-permute-start(s32[128]{0:T(128)S(1)} %collective-permute-done.5), channel_id=1, source_target_pairs={{0,8},{8,16},{16,24},{24,32},{32,40},{40,48},{48,56},{56,64},{64,7... | collective-permute-start | bytes 1544 | tf_op jit(solution)/shard_map/ppermute | solution.py:10
  54.2 7.3 %collective-permute-start.10 = (bf16[128,256]{0,1:T(8,128)(2,1)S(1)}, bf16[128,256]{0,1:T(8,128)(2,1)}, u32[]{:S(2)}, u32[]{:S(2)}) collective-permute-start(bf16[128,256]{0,1:T(8,128)(2,1)S(1)} %collective-permute-done.7), channel_id=1, source_target_pairs={{0,8},{8,16},{16,24},{24,32},{32,40},{40,48},{48,56},{56,64},{64,7... | collective-permute-start | bytes 196616 | tf_op jit(solution)/shard_map/ppermute | solution.py:10
  58.5 6.6 %collective-permute-start.8 = (bf16[128,256]{0,1:T(8,128)(2,1)S(1)}, bf16[128,256]{0,1:T(8,128)(2,1)}, u32[]{:S(2)}, u32[]{:S(2)}) collective-permute-start(bf16[128,256]{0,1:T(8,128)(2,1)S(1)} %collective-permute-done.6), channel_id=1, source_target_pairs={{0,8},{8,16},{16,24},{24,32},{32,40},{40,48},{48,56},{56,64},{64,7... | collective-permute-start | bytes 196616 | tf_op jit(solution)/shard_map/ppermute | solution.py:10
  61.5 17.4 %collective-permute-start.11 = (bf16[128,256]{0,1:T(8,128)(2,1)}, bf16[128,256]{0,1:T(8,128)(2,1)}, u32[]{:S(2)}, u32[]{:S(2)}) collective-permute-start(bf16[128,256]{0,1:T(8,128)(2,1)} %collective-permute-done.10), channel_id=1, source_target_pairs={{0,8},{8,16},{16,24},{24,32},{32,40},{40,48},{48,56},{56,64},{64,7... | collective-permute-start | bytes 196616 | tf_op jit(solution)/shard_map/ppermute | solution.py:10
  65.1 18.0 %collective-permute-start.9 = (bf16[128,256]{0,1:T(8,128)(2,1)}, bf16[128,256]{0,1:T(8,128)(2,1)}, u32[]{:S(2)}, u32[]{:S(2)}) collective-permute-start(bf16[128,256]{0,1:T(8,128)(2,1)} %collective-permute-done.8), channel_id=1, source_target_pairs={{0,8},{8,16},{16,24},{24,32},{32,40},{40,48},{48,56},{56,64},{64,7... | collective-permute-start | bytes 196616 | tf_op jit(solution)/shard_map/ppermute | solution.py:10
  78.9 9.0 %collective-permute-start.14 = (bf16[128,256]{0,1:T(8,128)(2,1)}, bf16[128,256]{0,1:T(8,128)(2,1)}, u32[]{:S(2)}, u32[]{:S(2)}) collective-permute-start(bf16[128,256]{0,1:T(8,128)(2,1)} %collective-permute-done.11), channel_id=1, source_target_pairs={{0,8},{8,16},{16,24},{24,32},{32,40},{40,48},{48,56},{56,64},{64,7... | collective-permute-start | bytes 196616 | tf_op jit(solution)/shard_map/ppermute | solution.py:10
  83.1 9.3 %collective-permute-start.12 = (bf16[128,256]{0,1:T(8,128)(2,1)}, bf16[128,256]{0,1:T(8,128)(2,1)}, u32[]{:S(2)}, u32[]{:S(2)}) collective-permute-start(bf16[128,256]{0,1:T(8,128)(2,1)} %collective-permute-done.9), channel_id=1, source_target_pairs={{0,8},{8,16},{16,24},{24,32},{32,40},{40,48},{48,56},{56,64},{64,7... | collective-permute-start | bytes 196616 | tf_op jit(solution)/shard_map/ppermute | solution.py:10
  87.9 9.5 %collective-permute-start.15 = (bf16[128,256]{0,1:T(8,128)(2,1)}, bf16[128,256]{0,1:T(8,128)(2,1)}, u32[]{:S(2)}, u32[]{:S(2)}) collective-permute-start(bf16[128,256]{0,1:T(8,128)(2,1)} %collective-permute-done.14), channel_id=1, source_target_pairs={{0,8},{8,16},{16,24},{24,32},{32,40},{40,48},{48,56},{56,64},{64,7... | collective-permute-start | bytes 196616 | tf_op jit(solution)/shard_map/ppermute | solution.py:10
  92.4 7.3 %collective-permute-start.13 = (bf16[128,256]{0,1:T(8,128)(2,1)}, bf16[128,256]{0,1:T(8,128)(2,1)}, u32[]{:S(2)}, u32[]{:S(2)}) collective-permute-start(bf16[128,256]{0,1:T(8,128)(2,1)} %collective-permute-done.12), channel_id=1, source_target_pairs={{0,8},{8,16},{16,24},{24,32},{32,40},{40,48},{48,56},{56,64},{64,7... | collective-permute-start | bytes 196616 | tf_op jit(solution)/shard_map/ppermute | solution.py:10
  97.4 8.3 %collective-permute-start.19 = (bf16[128,256]{0,1:T(8,128)(2,1)}, bf16[128,256]{0,1:T(8,128)(2,1)}, u32[]{:S(2)}, u32[]{:S(2)}) collective-permute-start(bf16[128,256]{0,1:T(8,128)(2,1)} %collective-permute-done.15), channel_id=1, source_target_pairs={{0,8},{8,16},{16,24},{24,32},{32,40},{40,48},{48,56},{56,64},{64,7... | collective-permute-start | bytes 196616 | tf_op jit(solution)/shard_map/ppermute | solution.py:10
  99.7 18.5 %collective-permute-start.17 = (bf16[128,256]{0,1:T(8,128)(2,1)}, bf16[128,256]{0,1:T(8,128)(2,1)}, u32[]{:S(2)}, u32[]{:S(2)}) collective-permute-start(bf16[128,256]{0,1:T(8,128)(2,1)} %collective-permute-done.13), channel_id=1, source_target_pairs={{0,8},{8,16},{16,24},{24,32},{32,40},{40,48},{48,56},{56,64},{64,7... | collective-permute-start | bytes 196616 | tf_op jit(solution)/shard_map/ppermute | solution.py:10
  105.7 13.9 %collective-permute-start.20 = (bf16[128,256]{0,1:T(8,128)(2,1)}, bf16[128,256]{0,1:T(8,128)(2,1)}, u32[]{:S(2)}, u32[]{:S(2)}) collective-permute-start(bf16[128,256]{0,1:T(8,128)(2,1)} %collective-permute-done.19), channel_id=1, source_target_pairs={{0,8},{8,16},{16,24},{24,32},{32,40},{40,48},{48,56},{56,64},{64,7... | collective-permute-start | bytes 196616 | tf_op jit(solution)/shard_map/ppermute | solution.py:10
  118.3 2.9 %collective-permute-start.18 = (bf16[128,256]{0,1:T(8,128)(2,1)}, bf16[128,256]{0,1:T(8,128)(2,1)S(1)}, u32[]{:S(2)}, u32[]{:S(2)}) collective-permute-start(bf16[128,256]{0,1:T(8,128)(2,1)} %collective-permute-done.17), channel_id=1, source_target_pairs={{0,8},{8,16},{16,24},{24,32},{32,40},{40,48},{48,56},{56,64},{64,7... | collective-permute-start | bytes 196616 | tf_op jit(solution)/shard_map/ppermute | solution.py:10
  (4 other events, 64.0 us)
Sparse Core Ops, SparseCore 0:
  10.3 101.3 all-gather.2
  114.8 80.6 all-gather.4
where the time goes:
time: 227 us; the launch traced here: 225 us
  starting transfers between devices  83.4 us (37%)
  blocking collectives  58.1 us (26%)
  waiting for transfers between devices  32.4 us (14%)
  between operations  18.9 us (8%)
  other arithmetic  15 us (7%)
  matrix products  9.17 us (4%)
  local copies, waits for them, and re-layouts  7.56 us (3%)
    ppermute x21, starting transfers between devices, from_behind(): return lax.ppermute(shard, axis, pairs)  83.3 us
    all_to_all x2, blocking collectives, sent_and_summed(): tiles = lax.all_to_all(cut_along(shard, dim, peers), axis, 0, 0, tiled=True)  45.3 us
    all_gather x1, waiting for transfers between devices, on_device(): lax.all_gather(down_weight, 'sp', axis=1, tiled=True)  29.6 us
    all_to_all x1, blocking collectives, from_everyone(): return lax.all_to_all(copies, axis, split_axis=0, concat_axis=0, tiled=True)  12.8 us
  transfers between devices with their start and end apart: 23, of which 4 were waited for; matrix products, arithmetic and copies ran while one was open for 11% of the time, Pallas kernels for 0%

commit v1 on v0

v1 whole, which is shorter than its diff:
```python
import jax
import jax.numpy as jnp
from jax import lax
from jax.experimental import pallas as pl
from jax.experimental.pallas import tpu as pltpu
from jax.sharding import PartitionSpec as P


def shifted(block, by):
    spans = lax.axis_size("sp")
    return lax.ppermute(block, "sp", [(i, (i + by) % spans) for i in range(spans)])


def summed_for_owner(partial):
    peers = lax.axis_size("tp")
    tiles = partial.reshape(peers, partial.shape[0] // peers, partial.shape[1])
    tiles = lax.all_to_all(tiles, "tp", 0, 0, tiled=True)
    return jnp.sum(tiles.astype(jnp.float32), axis=0)


def from_everyone(shard):
    copies = jnp.broadcast_to(shard, (lax.axis_size("tp"), *shard.shape))
    return lax.all_to_all(copies, "tp", split_axis=0, concat_axis=0, tiled=True)


def attention_kernel(heads, head_dim, rows, offsets, queries, *refs):
    blocks, out = refs[:-1], refs[-1]
    width = heads * head_dim
    own_docs = blocks[0][rows : rows + 1, :rows].astype(jnp.float32)
    q_docs = jnp.broadcast_to(own_docs, (rows, rows)).T
    q_docs = jnp.concatenate([q_docs, q_docs], axis=1)
    r = lax.broadcasted_iota(jnp.int32, (rows, 2 * rows), 0)
    c = lax.broadcasted_iota(jnp.int32, (rows, 2 * rows), 1)
    causal = c - rows < r
    j = lax.broadcasted_iota(jnp.int32, (2 * rows, 2 * rows), 0)
    s = lax.broadcasted_iota(jnp.int32, (2 * rows, 2 * rows), 1)
    later = (j > s).astype(jnp.float32).astype(jnp.bfloat16)
    totals = [jnp.zeros((rows, head_dim), jnp.float32) for _ in range(heads)]
    carried = [jnp.zeros((rows, 1), jnp.float32) for _ in range(heads)]
    scale = head_dim ** (-0.5)
    for pair in range(len(blocks) // 2):
        near, far = blocks[2 * pair], blocks[2 * pair + 1]
        k_docs = jnp.concatenate([far[rows : rows + 1, :rows], near[rows : rows + 1, :rows]], axis=1)
        live = k_docs.astype(jnp.float32) == q_docs
        if pair == 0:
            live = live & causal
        for h in range(heads):
            cols = slice(h * head_dim, (h + 1) * head_dim)
            v_cols = slice(width + h * head_dim, width + (h + 1) * head_dim)
            k = jnp.concatenate([far[:rows, cols], near[:rows, cols]], axis=0)
            v = jnp.concatenate([far[:rows, v_cols], near[:rows, v_cols]], axis=0)
            z = lax.dot_general(
                queries[:, cols], k, (((1,), (1,)), ((), ())), preferred_element_type=jnp.float32
            ) * scale + offsets[h]
            soft = jnp.log(1.0 + jnp.exp(-jnp.abs(z)))
            keep = jnp.where(live, jnp.minimum(-z, 0.0) - soft, 0.0)
            high = keep.astype(jnp.bfloat16)
            low = (keep - high.astype(jnp.float32)).astype(jnp.bfloat16)
            tail = jnp.dot(high, later, preferred_element_type=jnp.float32) + jnp.dot(
                low, later, preferred_element_type=jnp.float32
            )
            weight = jnp.where(live, jnp.exp(jnp.minimum(z, 0.0) - soft + tail + carried[h]), 0.0)
            totals[h] += jnp.dot(weight.astype(jnp.bfloat16), v, preferred_element_type=jnp.float32)
            carried[h] += tail[:, :1] + keep[:, :1]
    out[...] = jnp.concatenate(totals, axis=1).astype(jnp.bfloat16)


def attention(queries, blocks, offsets):
    rows, width = queries.shape
    heads = offsets.shape[0]
    vmem = pl.BlockSpec(memory_space=pltpu.VMEM)

    def body(*refs):
        attention_kernel(heads, width // heads, rows, *refs)

    return pl.pallas_call(
        body,
        out_shape=jax.ShapeDtypeStruct((rows, width), jnp.bfloat16),
        in_specs=[pl.BlockSpec(memory_space=pltpu.SMEM)] + [vmem] * (1 + len(blocks)),
        out_specs=vmem,
        name="attention",
    )(offsets, queries, *blocks)


def on_device(
    resid,
    queries,
    keys,
    values,
    doc_ids,
    score_offset,
    out_weight,
    norm_gain,
    gate_weight,
    up_weight,
    down_weight,
):
    rows = queries.shape[0]
    units = gate_weight.shape[1]
    packed = jnp.concatenate([gate_weight, up_weight, down_weight.T], axis=1)
    weights = lax.all_gather(packed, "sp", axis=0, tiled=True)

    docs = jnp.pad(doc_ids.astype(jnp.bfloat16)[None], ((0, 15), (0, 2 * keys.shape[1] - rows)))
    own = jnp.concatenate([jnp.concatenate([keys, values], axis=1), docs], axis=0)
    blocks = {0: own}
    blocks[7] = shifted(own, 7)
    for back in range(1, 5):
        blocks[back] = shifted(blocks[back - 1], 1)
        if back < 3:
            blocks[7 - back] = shifted(blocks[8 - back], -1)
    attended = attention(queries, [blocks[b] for b in range(8)], score_offset)

    mixed_attn = summed_for_owner(
        jnp.dot(attended, out_weight, preferred_element_type=jnp.float32).astype(jnp.bfloat16)
    )
    stream = resid.astype(jnp.float32) + mixed_attn
    normed = (
        stream * lax.rsqrt(jnp.mean(stream * stream, axis=1, keepdims=True) + 1e-06) * norm_gain
    ).astype(jnp.bfloat16)
    span_rows = from_everyone(normed).reshape(rows, -1)
    gate = jnp.dot(span_rows, weights[:, :units], preferred_element_type=jnp.float32)
    upper = jnp.dot(span_rows, weights[:, units : 2 * units], preferred_element_type=jnp.float32)
    hidden = (jax.nn.silu(gate) * upper).astype(jnp.bfloat16)
    partial_out = lax.dot_general(
        hidden,
        weights[:, 2 * units :],
        (((1,), (1,)), ((), ())),
        preferred_element_type=jnp.float32,
    )
    feed = summed_for_owner(partial_out.astype(jnp.bfloat16))
    return (stream + feed).astype(jnp.bfloat16)


def solution(mesh):
    in_specs = (
        P(("sp", "tp"), None),
        P("sp", "tp"),
        P("sp", "tp"),
        P("sp", "tp"),
        P("sp"),
        P("tp"),
        P("tp", None),
        P(),
        P("sp", "tp"),
        P("sp", "tp"),
        P("tp", "sp"),
    )
    out_specs = P(("sp", "tp"), None)
    return jax.shard_map(
        on_device, mesh=mesh, in_specs=in_specs, out_specs=out_specs, check_vma=False
    )
```

time: 227 us -> 150 us (0.66)
  starting transfers between devices: 83.4 us -> 28.3 us
  blocking collectives: 58.1 us -> 46.5 us
  other arithmetic: 15 us -> 5.87 us
  local copies, waits for them, and re-layouts: 7.56 us -> 0.73 us
  Pallas kernels: 0 us -> 6.72 us
  waiting for transfers between devices: 32.4 us -> 39 us
  between operations: 18.9 us -> 13.6 us
    ppermute x21 -> x7, starting transfers between devices: 83.3 us -> 28.3 us  [shifted(): lax.ppermute(block, 'sp', [(i, (i + by) % spans) for i in range(spans)])]
    ppermute x21 -> x7, waiting for transfers between devices: 2.16 us -> 19 us  [shifted(): lax.ppermute(block, 'sp', [(i, (i + by) % spans) for i in range(spans)])]
    all_to_all x3, blocking collectives: 58.1 us -> 46.5 us  [the longest x2 33.7 us: summed_for_owner(): tiles = lax.all_to_all(tiles, 'tp', 0, 0, tiled=True)]
    all_gather x2 -> x1, waiting for transfers between devices: 29.6 us -> 20 us  [on_device(): weights = lax.all_gather(packed, 'sp', axis=0, tiled=True)]
    pallas_call x0 -> x1, Pallas kernels: none -> 6.72 us  [attention(): pl.pallas_call(body, out_shape=jax.ShapeDtypeStruct((rows, width), jnp.bf...]
    concatenate x13 -> x2, other arithmetic: 8.14 us -> 2.49 us  [the longest x1 1.6 us: on_device(): packed = jnp.concatenate([gate_weight, up_weight, down_weight.T], axis=1)]
    another operation x3 -> x0, other arithmetic: 4.52 us -> none
    slice x4 -> x0, local copies, waits for them, and re-layouts: 3.14 us -> none  [block_update(): reached = (start + count > 0) & (d_block[-1] >= q_docs[0])]
  transfers between devices with their start and end apart: 23 -> 8, of which waited for: 4 -> 5; matrix products, arithmetic and copies ran while one was open for 11% -> 3% of each run, Pallas kernels for 0% -> 5%
where the time goes in v1:
time: 150 us; the launch traced here: 149 us
  blocking collectives  46.5 us (31%)
  waiting for transfers between devices  39 us (26%)
  starting transfers between devices  28.3 us (19%)
  between operations  13.6 us (9%)
  matrix products  8.13 us (5%)
  Pallas kernels  6.72 us (4%)
  other arithmetic  5.87 us (4%)
    all_to_all x2, blocking collectives, summed_for_owner(): tiles = lax.all_to_all(tiles, 'tp', 0, 0, tiled=True)  33.7 us
    ppermute x7, starting transfers between devices, shifted(): lax.ppermute(block, 'sp', [(i, (i + by) % spans) for i in range(spans)])  28.3 us
    all_gather x1, waiting for transfers between devices, on_device(): weights = lax.all_gather(packed, 'sp', axis=0, tiled=True)  20 us
    ppermute x7, waiting for transfers between devices, shifted(): lax.ppermute(block, 'sp', [(i, (i + by) % spans) for i in range(spans)])  19 us
    all_to_all x1, blocking collectives, from_everyone(): return lax.all_to_all(copies, 'tp', split_axis=0, concat_axis=0, tiled=True)  12.8 us
    pallas_call x1, Pallas kernels, attention(): pl.pallas_call(body, out_shape=jax.ShapeDtypeStruct((rows, width), jnp.bf...  6.72 us
    dot_general x1, matrix products, on_device(): lax.dot_general(hidden, weights[:, 2 * units:], (((1,), (1,)), ((), ())),...  4.52 us
  transfers between devices with their start and end apart: 8, of which 5 were waited for; matrix products, arithmetic and copies ran while one was open for 3% of the time, Pallas kernels for 5%

profile of v1, /device:TPU:1, one launch (start us, length us, event | category | flops | bytes accessed | tf_op | source)
XLA Modules:
  0.0 148.8 jit_solution(18098648380142617551)
XLA Ops:
  6.5 1.6 %pad_maximum_fusion = bf16[32,2304]{1,0:T(8,128)(2,1)} fusion(bf16[32,768]{1,0:T(8,128)(2,1)} %bitcast.14, bf16[32,768]{1,0:T(8,128)(2,1)} %param.20, bf16[32,768]{1,0:T(8,128)(2,1)} %param.19), kind=kLoop, calls=%fused_computation.21 | loop fusion | flops 442368 | bytes 294912 | tf_op jit(solution)/shard_map/concatenate | solution.py:100
  8.2 0.7 convert_bitcast_fusion
  8.8 0.9 fusion.24.refs_2_
  9.7 4.0 %collective-permute-start = (bf16[144,512]{1,0:T(8,128)(2,1)S(1)}, bf16[144,512]{1,0:T(8,128)(2,1)S(1)}, u32[]{:S(2)}, u32[]{:S(2)}) collective-permute-start(bf16[144,512]{1,0:T(8,128)(2,1)S(1)} %fusion.24.refs_2_), channel_id=1, source_target_pairs={{0,8},{8,16},{16,24},{24,32},{32,40},{40,48},{48,56},{56,64},{64,7... | collective-permute-start | bytes 442376 | tf_op jit(solution)/shard_map/ppermute | solution.py:11
  13.8 5.1 %collective-permute-start.4 = (bf16[144,512]{1,0:T(8,128)(2,1)S(1)}, bf16[144,512]{1,0:T(8,128)(2,1)S(1)}, u32[]{:S(2)}, u32[]{:S(2)}) collective-permute-start(bf16[144,512]{1,0:T(8,128)(2,1)S(1)} %fusion.24.refs_2_), channel_id=1, source_target_pairs={{0,56},{8,64},{16,72},{24,80},{32,88},{40,96},{48,104},{56,112},{6... | collective-permute-start | bytes 442376 | tf_op jit(solution)/shard_map/ppermute | solution.py:11
  18.9 9.5 %collective-permute-done.refs_3_ = bf16[144,512]{1,0:T(8,128)(2,1)S(1)} collective-permute-done((bf16[144,512]{1,0:T(8,128)(2,1)S(1)}, bf16[144,512]{1,0:T(8,128)(2,1)S(1)}, u32[]{:S(2)}, u32[]{:S(2)}) %collective-permute-start) | collective-permute-done | bytes 147488 | tf_op jit(solution)/shard_map/ppermute | solution.py:11
  28.4 1.9 %collective-permute-start.1 = (bf16[144,512]{1,0:T(8,128)(2,1)S(1)}, bf16[144,512]{1,0:T(8,128)(2,1)S(1)}, u32[]{:S(2)}, u32[]{:S(2)}) collective-permute-start(bf16[144,512]{1,0:T(8,128)(2,1)S(1)} %collective-permute-done.refs_3_), channel_id=1, source_target_pairs={{0,8},{8,16},{16,24},{24,32},{32,40},{40,48},{48,56},{56,64},{64,7... | collective-permute-start | bytes 442376 | tf_op jit(solution)/shard_map/ppermute | solution.py:11
  30.3 6.7 %collective-permute-start.5 = (bf16[144,512]{1,0:T(8,128)(2,1)S(1)}, bf16[144,512]{1,0:T(8,128)(2,1)S(1)}, u32[]{:S(2)}, u32[]{:S(2)}) collective-permute-start(bf16[144,512]{1,0:T(8,128)(2,1)S(1)} %collective-permute-done.4.refs_9_), channel_id=1, source_target_pairs={{0,504},{8,0},{16,8},{24,16},{32,24},{40,32},{48,40},{56,48},{64,5... | collective-permute-start | bytes 442376 | tf_op jit(solution)/shard_map/ppermute | solution.py:11
  37.0 0.7 collective-permute-done.1.refs_4_
  37.6 1.9 %collective-permute-start.2 = (bf16[144,512]{1,0:T(8,128)(2,1)S(1)}, bf16[144,512]{1,0:T(8,128)(2,1)S(1)}, u32[]{:S(2)}, u32[]{:S(2)}) collective-permute-start(bf16[144,512]{1,0:T(8,128)(2,1)S(1)} %collective-permute-done.1.refs_4_), channel_id=1, source_target_pairs={{0,8},{8,16},{16,24},{24,32},{32,40},{40,48},{48,56},{56,64},{64,7... | collective-permute-start | bytes 442376 | tf_op jit(solution)/shard_map/ppermute | solution.py:11
  39.6 6.7 %collective-permute-start.6 = (bf16[144,512]{1,0:T(8,128)(2,1)S(1)}, bf16[144,512]{1,0:T(8,128)(2,1)S(1)}, u32[]{:S(2)}, u32[]{:S(2)}) collective-permute-start(bf16[144,512]{1,0:T(8,128)(2,1)S(1)} %collective-permute-done.5.refs_8_), channel_id=1, source_target_pairs={{0,504},{8,0},{16,8},{24,16},{32,24},{40,32},{48,40},{56,48},{64,5... | collective-permute-start | bytes 442376 | tf_op jit(solution)/shard_map/ppermute | solution.py:11
  46.3 1.2 collective-permute-done.2.refs_5_
  47.5 1.9 %collective-permute-start.3 = (bf16[144,512]{1,0:T(8,128)(2,1)S(1)}, bf16[144,512]{1,0:T(8,128)(2,1)S(1)}, u32[]{:S(2)}, u32[]{:S(2)}) collective-permute-start(bf16[144,512]{1,0:T(8,128)(2,1)S(1)} %collective-permute-done.2.refs_5_), channel_id=1, source_target_pairs={{0,8},{8,16},{16,24},{24,32},{32,40},{40,48},{48,56},{56,64},{64,7... | collective-permute-start | bytes 442376 | tf_op jit(solution)/shard_map/ppermute | solution.py:11
  49.5 7.7 %collective-permute-done.3.refs_6_ = bf16[144,512]{1,0:T(8,128)(2,1)S(1)} collective-permute-done((bf16[144,512]{1,0:T(8,128)(2,1)S(1)}, bf16[144,512]{1,0:T(8,128)(2,1)S(1)}, u32[]{:S(2)}, u32[]{:S(2)}) %collective-permute-start.3) | collective-permute-done | bytes 147488 | tf_op jit(solution)/shard_map/ppermute | solution.py:11
  57.8 6.7 %attention.1 = bf16[128,256]{1,0:T(8,128)(2,1)} custom-call(f32[4]{0:T(128)} %refs_0_.1, bf16[128,256]{1,0:T(8,128)(2,1)} %refs_1_.1, bf16[144,512]{1,0:T(8,128)(2,1)} %copy-done.1, bf16[144,512]{1,0:T(8,128)(2,1)} %copy-done.3, bf16[144,512]{1,0:T(8,128)(2,1)} %copy-done.5, bf16[144,512]{1,0:T(8,128)(2,1)} %copy-done.7, bf16[144,512]{1,0:T(8,128)(2,1)} %copy-done.9, ...), custom_call_target="tpu_custom_call" | custom-call | tf_op jit(solution)/shard_map/attention/pallas_call | solution.py:76
  64.6 1.1 convolution_convert_fusion
  65.7 19.5 %all_to_all.15 = bf16[8,16,2048]{2,1,0:T(8,128)(2,1)S(1)} all-to-all(bf16[8,16,2048]{2,1,0:T(8,128)(2,1)S(1)} %bitcast.10), channel_id=1, replica_groups=mesh['sp'=64,'tp'=8] {'tp'}, dimensions={0} | all-to-all | bytes 1048576 | tf_op jit(solution)/shard_map/all_to_all | solution.py:17
  85.3 1.0 multiply_reduce_fusion
  86.3 0.9 multiply_convert_fusion
  87.3 12.8 %all_to_all.16 = bf16[8,16,2048]{2,1,0:T(8,128)(2,1)S(1)} all-to-all(bf16[8,16,2048]{2,1,0:T(8,128)(2,1)S(1)} %broadcast_in_dim.9), channel_id=1, replica_groups=mesh['sp'=64,'tp'=8] {'tp'}, dimensions={0} | all-to-all | bytes 1048576 | tf_op jit(solution)/shard_map/all_to_all | solution.py:23
  100.1 20.0 %all-gather.2.cloned.1.call-done = bf16[2048,2304]{1,0:T(8,128)(2,1)} async-done(((bf16[32,2304]{1,0:T(8,128)(2,1)}), bf16[2048,2304]{1,0:T(8,128)(2,1)}) %all-gather.2.cloned.1.call-update) | async-done | bytes 9437200 | tf_op jit(solution)/shard_map/all_gather | solution.py:101
  120.0 2.5 %fusion.4 = f32[128,768]{1,0:T(8,128)S(1)} fusion(bf16[128,2048]{1,0:T(8,128)(2,1)S(1)} %bitcast.11, bf16[2048,2304]{1,0:T(8,128)(2,1)} %all-gather.2.cloned.1.call-done), kind=kOutput, calls=%fused_computation.4 | convolution fusion | flops 402653184 | bytes 4063232 | tf_op jit(solution)/shard_map/dot_general | solution.py:121
  122.5 4.5 %fusion.6 = bf16[128,2048]{1,0:T(8,128)(2,1)S(1)} fusion(bf16[2048,2304]{1,0:T(8,128)(2,1)} %all-gather.2.cloned.1.call-done, bf16[128,2048]{1,0:T(8,128)(2,1)S(1)} %bitcast.12, f32[128,768]{1,0:T(8,128)S(1)} %fusion.4), kind=kOutput, calls=%fused_computation.6 | convolution fusion | flops 806158336 | bytes 7733248 | tf_op jit(solution)/shard_map/dot_general | solution.py:124
  127.0 14.2 %all_to_all.17 = bf16[8,16,2048]{2,1,0:T(8,128)(2,1)S(1)} all-to-all(bf16[8,16,2048]{2,1,0:T(8,128)(2,1)S(1)} %bitcast.13), channel_id=1, replica_groups=mesh['sp'=64,'tp'=8] {'tp'}, dimensions={0} | all-to-all | bytes 1048576 | tf_op jit(solution)/shard_map/all_to_all | solution.py:17
  (30 shorter events, 1.6 us)
Async XLA Ops:
  6.5 58.0 %copy-start = (bf16[256,2048]{1,0:T(8,128)(2,1)S(1)}, bf16[256,2048]{1,0:T(8,128)(2,1)}, u32[]{:S(2)}) copy-start(bf16[256,2048]{1,0:T(8,128)(2,1)} %param.17) | copy-start | bytes 3145732
  6.5 113.5 %all-gather.2.cloned.1.call-start = ((), (), s32[]{:S(2)}) async-start(), calls=%async_computation.3 | async-start | bytes 9584640 | tf_op jit(solution)/shard_map/all_gather | solution.py:101
  9.7 47.4 %copy-start.1 = (bf16[144,512]{1,0:T(8,128)(2,1)}, bf16[144,512]{1,0:T(8,128)(2,1)S(1)}, u32[]{:S(2)}) copy-start(bf16[144,512]{1,0:T(8,128)(2,1)S(1)} %fusion.24.refs_2_) | copy-start | bytes 442372
  9.7 18.6 %collective-permute-start = (bf16[144,512]{1,0:T(8,128)(2,1)S(1)}, bf16[144,512]{1,0:T(8,128)(2,1)S(1)}, u32[]{:S(2)}, u32[]{:S(2)}) collective-permute-start(bf16[144,512]{1,0:T(8,128)(2,1)S(1)} %fusion.24.refs_2_), channel_id=1, source_target_pairs={{0,8},{8,16},{16,24},{24,32},{32,40},{40,48},{48,56},{56,64},{64,7... | collective-permute-start | bytes 442376 | tf_op jit(solution)/shard_map/ppermute | solution.py:11
  13.8 16.6 %collective-permute-start.4 = (bf16[144,512]{1,0:T(8,128)(2,1)S(1)}, bf16[144,512]{1,0:T(8,128)(2,1)S(1)}, u32[]{:S(2)}, u32[]{:S(2)}) collective-permute-start(bf16[144,512]{1,0:T(8,128)(2,1)S(1)} %fusion.24.refs_2_), channel_id=1, source_target_pairs={{0,56},{8,64},{16,72},{24,80},{32,88},{40,96},{48,104},{56,112},{6... | collective-permute-start | bytes 442376 | tf_op jit(solution)/shard_map/ppermute | solution.py:11
  28.3 28.8 %copy-start.3 = (bf16[144,512]{1,0:T(8,128)(2,1)}, bf16[144,512]{1,0:T(8,128)(2,1)S(1)}, u32[]{:S(2)}) copy-start(bf16[144,512]{1,0:T(8,128)(2,1)S(1)} %collective-permute-done.refs_3_) | copy-start | bytes 442372
  28.4 9.3 %collective-permute-start.1 = (bf16[144,512]{1,0:T(8,128)(2,1)S(1)}, bf16[144,512]{1,0:T(8,128)(2,1)S(1)}, u32[]{:S(2)}, u32[]{:S(2)}) collective-permute-start(bf16[144,512]{1,0:T(8,128)(2,1)S(1)} %collective-permute-done.refs_3_), channel_id=1, source_target_pairs={{0,8},{8,16},{16,24},{24,32},{32,40},{40,48},{48,56},{56,64},{64,7... | collective-permute-start | bytes 442376 | tf_op jit(solution)/shard_map/ppermute | solution.py:11
  30.3 26.8 %copy-start.4 = (bf16[144,512]{1,0:T(8,128)(2,1)}, bf16[144,512]{1,0:T(8,128)(2,1)S(1)}, u32[]{:S(2)}) copy-start(bf16[144,512]{1,0:T(8,128)(2,1)S(1)} %collective-permute-done.4.refs_9_) | copy-start | bytes 442372
  30.3 9.3 %collective-permute-start.5 = (bf16[144,512]{1,0:T(8,128)(2,1)S(1)}, bf16[144,512]{1,0:T(8,128)(2,1)S(1)}, u32[]{:S(2)}, u32[]{:S(2)}) collective-permute-start(bf16[144,512]{1,0:T(8,128)(2,1)S(1)} %collective-permute-done.4.refs_9_), channel_id=1, source_target_pairs={{0,504},{8,0},{16,8},{24,16},{32,24},{40,32},{48,40},{56,48},{64,5... | collective-permute-start | bytes 442376 | tf_op jit(solution)/shard_map/ppermute | solution.py:11
  37.6 19.5 %copy-start.5 = (bf16[144,512]{1,0:T(8,128)(2,1)}, bf16[144,512]{1,0:T(8,128)(2,1)S(1)}, u32[]{:S(2)}) copy-start(bf16[144,512]{1,0:T(8,128)(2,1)S(1)} %collective-permute-done.1.refs_4_) | copy-start | bytes 442372
  37.6 9.9 %collective-permute-start.2 = (bf16[144,512]{1,0:T(8,128)(2,1)S(1)}, bf16[144,512]{1,0:T(8,128)(2,1)S(1)}, u32[]{:S(2)}, u32[]{:S(2)}) collective-permute-start(bf16[144,512]{1,0:T(8,128)(2,1)S(1)} %collective-permute-done.1.refs_4_), channel_id=1, source_target_pairs={{0,8},{8,16},{16,24},{24,32},{32,40},{40,48},{48,56},{56,64},{64,7... | collective-permute-start | bytes 442376 | tf_op jit(solution)/shard_map/ppermute | solution.py:11
  39.6 17.6 %copy-start.6 = (bf16[144,512]{1,0:T(8,128)(2,1)}, bf16[144,512]{1,0:T(8,128)(2,1)S(1)}, u32[]{:S(2)}) copy-start(bf16[144,512]{1,0:T(8,128)(2,1)S(1)} %collective-permute-done.5.refs_8_) | copy-start | bytes 442372
  39.6 9.9 %collective-permute-start.6 = (bf16[144,512]{1,0:T(8,128)(2,1)S(1)}, bf16[144,512]{1,0:T(8,128)(2,1)S(1)}, u32[]{:S(2)}, u32[]{:S(2)}) collective-permute-start(bf16[144,512]{1,0:T(8,128)(2,1)S(1)} %collective-permute-done.5.refs_8_), channel_id=1, source_target_pairs={{0,504},{8,0},{16,8},{24,16},{32,24},{40,32},{48,40},{56,48},{64,5... | collective-permute-start | bytes 442376 | tf_op jit(solution)/shard_map/ppermute | solution.py:11
  47.5 9.6 %copy-start.7 = (bf16[144,512]{1,0:T(8,128)(2,1)}, bf16[144,512]{1,0:T(8,128)(2,1)S(1)}, u32[]{:S(2)}) copy-start(bf16[144,512]{1,0:T(8,128)(2,1)S(1)} %collective-permute-done.2.refs_5_) | copy-start | bytes 442372
  47.5 9.6 %collective-permute-start.3 = (bf16[144,512]{1,0:T(8,128)(2,1)S(1)}, bf16[144,512]{1,0:T(8,128)(2,1)S(1)}, u32[]{:S(2)}, u32[]{:S(2)}) collective-permute-start(bf16[144,512]{1,0:T(8,128)(2,1)S(1)} %collective-permute-done.2.refs_5_), channel_id=1, source_target_pairs={{0,8},{8,16},{16,24},{24,32},{32,40},{40,48},{48,56},{56,64},{64,7... | collective-permute-start | bytes 442376 | tf_op jit(solution)/shard_map/ppermute | solution.py:11
  49.5 7.7 %copy-start.8 = (bf16[144,512]{1,0:T(8,128)(2,1)}, bf16[144,512]{1,0:T(8,128)(2,1)S(1)}, u32[]{:S(2)}) copy-start(bf16[144,512]{1,0:T(8,128)(2,1)S(1)} %collective-permute-done.6.refs_7_) | copy-start | bytes 442372
  57.2 0.7 copy-start.9
  87.2 54.1 %copy-start.2 = (bf16[16,2048]{1,0:T(8,128)(2,1)S(1)}, bf16[16,2048]{1,0:T(8,128)(2,1)}, u32[]{:S(2)}) copy-start(bf16[16,2048]{1,0:T(8,128)(2,1)} %param.11) | copy-start | bytes 196612
Sparse Core Ops, SparseCore 0:
  10.3 109.6 all-gather.1

commit v2 on v1

--- a/solution.py
+++ b/solution.py
@@ -1,3 +1,5 @@
+from functools import partial
+
 import jax
 import jax.numpy as jnp
 from jax import lax
@@ -11,9 +13,9 @@
     return lax.ppermute(block, "sp", [(i, (i + by) % spans) for i in range(spans)])
 
 
-def summed_for_owner(partial):
+def summed_for_owner(terms):
     peers = lax.axis_size("tp")
-    tiles = partial.reshape(peers, partial.shape[0] // peers, partial.shape[1])
+    tiles = terms.reshape(peers, terms.shape[0] // peers, terms.shape[1])
     tiles = lax.all_to_all(tiles, "tp", 0, 0, tiled=True)
     return jnp.sum(tiles.astype(jnp.float32), axis=0)
 
@@ -82,7 +84,65 @@
     )(offsets, queries, *blocks)
 
 
+def ffn_kernel(parts, place, x, gate_up, *refs):
+    downs, out = refs[:parts], refs[parts]
+    gu, dn, gu_sems, dn_sems = refs[parts + 1 :]
+    units = gu.shape[1] // 2
+    step = gu.shape[0] // parts
+    wide = dn.shape[1]
+    gu_copies = [
+        pltpu.make_async_copy(gate_up.at[pl.ds(i * step, step)], gu.at[pl.ds(i * step, step)], gu_sems.at[i])
+        for i in range(parts)
+    ]
+    dn_copies = [pltpu.make_async_copy(downs[i], dn.at[i], dn_sems.at[i]) for i in range(parts)]
+    for copy in gu_copies + dn_copies:
+        copy.start()
+    acc = None
+    for i in range(parts):
+        gu_copies[i].wait()
+        term = jnp.dot(
+            x[:, i * step : (i + 1) * step],
+            gu[i * step : (i + 1) * step, :],
+            preferred_element_type=jnp.float32,
+        )
+        acc = term if acc is None else acc + term
+    gate, upper = acc[:, :units], acc[:, units:]
+    hidden = (gate / (1.0 + jnp.exp(-gate)) * upper).astype(jnp.bfloat16)
+    for i in range(parts):
+        dn_copies[i].wait()
+        term = lax.dot_general(
+            hidden, dn[i], (((1,), (1,)), ((), ())), preferred_element_type=jnp.float32
+        )
+        at = pl.multiple_of(place[i] * wide, wide)
+        out[:, pl.ds(at, wide)] = term.astype(jnp.bfloat16)
+
+
+def ffn(x, gate_up, downs, place):
+    parts = len(downs)
+    wide, units = downs[0].shape
+    vmem = pl.BlockSpec(memory_space=pltpu.VMEM)
+    hbm = pl.BlockSpec(memory_space=pl.ANY)
+
+    def body(*refs):
+        ffn_kernel(parts, *refs)
+
+    return pl.pallas_call(
+        body,
+        out_shape=jax.ShapeDtypeStruct((x.shape[0], parts * wide), jnp.bfloat16),
+        in_specs=[pl.BlockSpec(memory_space=pltpu.SMEM), vmem] + [hbm] * (1 + parts),
+        out_specs=vmem,
+        scratch_shapes=[
+            pltpu.VMEM(gate_up.shape, jnp.bfloat16),
+            pltpu.VMEM((parts, wide, units), jnp.bfloat16),
+            pltpu.SemaphoreType.DMA((parts,)),
+            pltpu.SemaphoreType.DMA((parts,)),
+        ],
+        name="ffn",
+    )(place, x, gate_up, *downs)
+
+
 def on_device(
+    ring,
     resid,
     queries,
     keys,
@@ -96,19 +156,25 @@
     down_weight,
 ):
     rows = queries.shape[0]
-    units = gate_weight.shape[1]
-    packed = jnp.concatenate([gate_weight, up_weight, down_weight.T], axis=1)
-    weights = lax.all_gather(packed, "sp", axis=0, tiled=True)
+    gate_up = lax.all_gather(
+        jnp.concatenate([gate_weight, up_weight], axis=1), "sp", axis=0, tiled=True
+    )
+
+    spans = lax.axis_size("sp")
+    rings = spans // ring
+    groups = [list(range(i * ring, (i + 1) * ring)) for i in range(rings)]
+    down = lax.all_gather(down_weight.T, "sp", axis=0, tiled=True, axis_index_groups=groups)
+    downs = {0: down}
+    for back in range(1, rings // 2 + 1):
+        downs[back] = shifted(downs[back - 1], ring)
+        if rings - back > rings // 2:
+            downs[rings - back] = shifted(downs[(rings - back + 1) % rings], -ring)
+    place = (lax.axis_index("sp") // ring - jnp.arange(rings, dtype=jnp.int32)) % rings
 
     docs = jnp.pad(doc_ids.astype(jnp.bfloat16)[None], ((0, 15), (0, 2 * keys.shape[1] - rows)))
     own = jnp.concatenate([jnp.concatenate([keys, values], axis=1), docs], axis=0)
-    blocks = {0: own}
-    blocks[7] = shifted(own, 7)
-    for back in range(1, 5):
-        blocks[back] = shifted(blocks[back - 1], 1)
-        if back < 3:
-            blocks[7 - back] = shifted(blocks[8 - back], -1)
-    attended = attention(queries, [blocks[b] for b in range(8)], score_offset)
+    blocks = [own] + [shifted(own, back) for back in range(1, 8)]
+    attended = attention(queries, blocks, score_offset)
 
     mixed_attn = summed_for_owner(
         jnp.dot(attended, out_weight, preferred_element_type=jnp.float32).astype(jnp.bfloat16)
@@ -118,16 +184,7 @@
         stream * lax.rsqrt(jnp.mean(stream * stream, axis=1, keepdims=True) + 1e-06) * norm_gain
     ).astype(jnp.bfloat16)
     span_rows = from_everyone(normed).reshape(rows, -1)
-    gate = jnp.dot(span_rows, weights[:, :units], preferred_element_type=jnp.float32)
-    upper = jnp.dot(span_rows, weights[:, units : 2 * units], preferred_element_type=jnp.float32)
-    hidden = (jax.nn.silu(gate) * upper).astype(jnp.bfloat16)
-    partial_out = lax.dot_general(
-        hidden,
-        weights[:, 2 * units :],
-        (((1,), (1,)), ((), ())),
-        preferred_element_type=jnp.float32,
-    )
-    feed = summed_for_owner(partial_out.astype(jnp.bfloat16))
+    feed = summed_for_owner(ffn(span_rows, gate_up, [downs[i] for i in range(rings)], place))
     return (stream + feed).astype(jnp.bfloat16)
 
 
@@ -147,5 +204,5 @@
     )
     out_specs = P(("sp", "tp"), None)
     return jax.shard_map(
-        on_device, mesh=mesh, in_specs=in_specs, out_specs=out_specs, check_vma=False
-    )
+        partial(on_device, 8), mesh=mesh, in_specs=in_specs, out_specs=out_specs, check_vma=False
+    )

time: 150 us -> 197 us (1.31)
  starting transfers between devices: 28.3 us -> 71.3 us
  blocking collectives: 46.5 us -> 37.5 us
  waiting for transfers between devices: 39 us -> 47.9 us
  Pallas kernels: 6.72 us -> 15.4 us
  matrix products: 8.13 us -> 1.96 us
    ppermute x7 -> x14, starting transfers between devices: 28.3 us -> 58.6 us  [shifted(): lax.ppermute(block, 'sp', [(i, (i + by) % spans) for i in range(spans)])]
    ppermute x7 -> x14, waiting for transfers between devices: 19 us -> 46 us  [shifted(): lax.ppermute(block, 'sp', [(i, (i + by) % spans) for i in range(spans)])]
    all_gather x0 -> x1, blocking collectives: none -> 22.6 us  [on_device(): lax.all_gather(down_weight.T, 'sp', axis=0, tiled=True, axis_index_groups...]
    all_gather x1, waiting for transfers between devices: 20 us -> 0.01 us  [on_device(): lax.all_gather(jnp.concatenate([gate_weight, up_weight], axis=1), 'sp', a...]
    all_to_all x2 -> x1, blocking collectives: 33.7 us -> 14.9 us  [summed_for_owner(): tiles = lax.all_to_all(tiles, 'tp', 0, 0, tiled=True)]
    all_to_all x1 -> x0, blocking collectives: 12.8 us -> none  [from_everyone(): return lax.all_to_all(copies, 'tp', split_axis=0, concat_axis=0, tiled=True)]
    all_to_all x0 -> x2, starting transfers between devices: none -> 12.7 us  [the longest x1 6.72 us: from_everyone(): return lax.all_to_all(copies, 'tp', split_axis=0, concat_axis=0, tiled=True)]
    pallas_call x0 -> x1, Pallas kernels: none -> 8.7 us  [ffn(): pl.pallas_call(body, out_shape=jax.ShapeDtypeStruct((x.shape[0], parts *...]
  transfers between devices with their start and end apart: 8 -> 17, of which waited for: 5 -> 8; matrix products, arithmetic and copies ran while one was open for 3% -> 4% of each run, Pallas kernels for 5% -> 3%
where the time goes in v2:
time: 197 us; the launch traced here: 196 us
  starting transfers between devices  71.3 us (36%)
  waiting for transfers between devices  47.9 us (24%)
  blocking collectives  37.5 us (19%)
  Pallas kernels  15.4 us (8%)
  between operations  13.7 us (7%)
  other arithmetic  6.33 us (3%)
    ppermute x14, starting transfers between devices, shifted(): lax.ppermute(block, 'sp', [(i, (i + by) % spans) for i in range(spans)])  58.6 us
    ppermute x14, waiting for transfers between devices, shifted(): lax.ppermute(block, 'sp', [(i, (i + by) % spans) for i in range(spans)])  46 us
    all_gather x1, blocking collectives, on_device(): lax.all_gather(down_weight.T, 'sp', axis=0, tiled=True, axis_index_groups...  22.6 us
    all_to_all x1, blocking collectives, summed_for_owner(): tiles = lax.all_to_all(tiles, 'tp', 0, 0, tiled=True)  14.9 us
    pallas_call x1, Pallas kernels, ffn(): pl.pallas_call(body, out_shape=jax.ShapeDtypeStruct((x.shape[0], parts *...  8.7 us
    pallas_call x1, Pallas kernels, attention(): pl.pallas_call(body, out_shape=jax.ShapeDtypeStruct((rows, width), jnp.bf...  6.73 us
    all_to_all x1, starting transfers between devices, from_everyone(): return lax.all_to_all(copies, 'tp', split_axis=0, concat_axis=0, tiled=True)  6.72 us
    all_to_all x1, starting transfers between devices, summed_for_owner(): tiles = lax.all_to_all(tiles, 'tp', 0, 0, tiled=True)  5.97 us
  transfers between devices with their start and end apart: 17, of which 8 were waited for; matrix products, arithmetic and copies ran while one was open for 4% of the time, Pallas kernels for 3%

profile of v2, /device:TPU:1, one launch (start us, length us, event | category | flops | bytes accessed | tf_op | source)
XLA Modules:
  0.0 195.7 jit_solution(17768612564014688034)
XLA Ops:
  9.7 4.0 %collective-permute-start = (bf16[144,512]{1,0:T(8,128)(2,1)S(1)}, bf16[144,512]{1,0:T(8,128)(2,1)S(1)}, u32[]{:S(2)}, u32[]{:S(2)}) collective-permute-start(bf16[144,512]{1,0:T(8,128)(2,1)S(1)} %fusion.1.refs_2_), channel_id=1, source_target_pairs={{0,8},{8,16},{16,24},{24,32},{32,40},{40,48},{48,56},{56,64},{64,7... | collective-permute-start | bytes 442376 | tf_op jit(solution)/shard_map/ppermute | solution.py:13
  13.7 4.2 %collective-permute-start.1 = (bf16[144,512]{1,0:T(8,128)(2,1)S(1)}, bf16[144,512]{1,0:T(8,128)(2,1)S(1)}, u32[]{:S(2)}, u32[]{:S(2)}) collective-permute-start(bf16[144,512]{1,0:T(8,128)(2,1)S(1)} %fusion.1.refs_2_), channel_id=1, source_target_pairs={{0,16},{8,24},{16,32},{24,40},{32,48},{40,56},{48,64},{56,72},{64,... | collective-permute-start | bytes 442376 | tf_op jit(solution)/shard_map/ppermute | solution.py:13
  17.9 4.6 %collective-permute-start.2 = (bf16[144,512]{1,0:T(8,128)(2,1)S(1)}, bf16[144,512]{1,0:T(8,128)(2,1)S(1)}, u32[]{:S(2)}, u32[]{:S(2)}) collective-permute-start(bf16[144,512]{1,0:T(8,128)(2,1)S(1)} %fusion.1.refs_2_), channel_id=1, source_target_pairs={{0,24},{8,32},{16,40},{24,48},{32,56},{40,64},{48,72},{56,80},{64,... | collective-permute-start | bytes 442376 | tf_op jit(solution)/shard_map/ppermute | solution.py:13
  22.6 5.3 %collective-permute-start.3 = (bf16[144,512]{1,0:T(8,128)(2,1)S(1)}, bf16[144,512]{1,0:T(8,128)(2,1)S(1)}, u32[]{:S(2)}, u32[]{:S(2)}) collective-permute-start(bf16[144,512]{1,0:T(8,128)(2,1)S(1)} %fusion.1.refs_2_), channel_id=1, source_target_pairs={{0,32},{8,40},{16,48},{24,56},{32,64},{40,72},{48,80},{56,88},{64,... | collective-permute-start | bytes 442376 | tf_op jit(solution)/shard_map/ppermute | solution.py:13
  27.9 4.9 %collective-permute-start.4 = (bf16[144,512]{1,0:T(8,128)(2,1)S(1)}, bf16[144,512]{1,0:T(8,128)(2,1)S(1)}, u32[]{:S(2)}, u32[]{:S(2)}) collective-permute-start(bf16[144,512]{1,0:T(8,128)(2,1)S(1)} %fusion.1.refs_2_), channel_id=1, source_target_pairs={{0,40},{8,48},{16,56},{24,64},{32,72},{40,80},{48,88},{56,96},{64,... | collective-permute-start | bytes 442376 | tf_op jit(solution)/shard_map/ppermute | solution.py:13
  32.8 6.8 %collective-permute-start.5 = (bf16[144,512]{1,0:T(8,128)(2,1)S(1)}, bf16[144,512]{1,0:T(8,128)(2,1)S(1)}, u32[]{:S(2)}, u32[]{:S(2)}) collective-permute-start(bf16[144,512]{1,0:T(8,128)(2,1)S(1)} %fusion.1.refs_2_), channel_id=1, source_target_pairs={{0,48},{8,56},{16,64},{24,72},{32,80},{40,88},{48,96},{56,104},{64... | collective-permute-start | bytes 442376 | tf_op jit(solution)/shard_map/ppermute | solution.py:13
  39.6 4.8 %collective-permute-start.6 = (bf16[144,512]{1,0:T(8,128)(2,1)S(1)}, bf16[144,512]{1,0:T(8,128)(2,1)S(1)}, u32[]{:S(2)}, u32[]{:S(2)}) collective-permute-start(bf16[144,512]{1,0:T(8,128)(2,1)S(1)} %fusion.1.refs_2_), channel_id=1, source_target_pairs={{0,56},{8,64},{16,72},{24,80},{32,88},{40,96},{48,104},{56,112},{6... | collective-permute-start | bytes 442376 | tf_op jit(solution)/shard_map/ppermute | solution.py:13
  44.5 7.8 %collective-permute-done.3.refs_6_ = bf16[144,512]{1,0:T(8,128)(2,1)S(1)} collective-permute-done((bf16[144,512]{1,0:T(8,128)(2,1)S(1)}, bf16[144,512]{1,0:T(8,128)(2,1)S(1)}, u32[]{:S(2)}, u32[]{:S(2)}) %collective-permute-start.3) | collective-permute-done | bytes 147488 | tf_op jit(solution)/shard_map/ppermute | solution.py:13
  52.3 6.2 %collective-permute-done.5.refs_8_ = bf16[144,512]{1,0:T(8,128)(2,1)S(1)} collective-permute-done((bf16[144,512]{1,0:T(8,128)(2,1)S(1)}, bf16[144,512]{1,0:T(8,128)(2,1)S(1)}, u32[]{:S(2)}, u32[]{:S(2)}) %collective-permute-start.5) | collective-permute-done | bytes 147488 | tf_op jit(solution)/shard_map/ppermute | solution.py:13
  58.5 3.2 %collective-permute-done.6.refs_9_ = bf16[144,512]{1,0:T(8,128)(2,1)S(1)} collective-permute-done((bf16[144,512]{1,0:T(8,128)(2,1)S(1)}, bf16[144,512]{1,0:T(8,128)(2,1)S(1)}, u32[]{:S(2)}, u32[]{:S(2)}) %collective-permute-start.6) | collective-permute-done | bytes 147488 | tf_op jit(solution)/shard_map/ppermute | solution.py:13
  62.5 6.7 %attention.1 = bf16[128,256]{1,0:T(8,128)(2,1)} custom-call(f32[4]{0:T(128)} %refs_0_.1, bf16[128,256]{1,0:T(8,128)(2,1)} %refs_1_.1, bf16[144,512]{1,0:T(8,128)(2,1)} %copy-done.3, bf16[144,512]{1,0:T(8,128)(2,1)} %copy-done.8, bf16[144,512]{1,0:T(8,128)(2,1)} %copy-done.9, bf16[144,512]{1,0:T(8,128)(2,1)} %copy-done.10, bf16[144,512]{1,0:T(8,128)(2,1)} %copy-done.11, ...), custom_call_target="tpu_custom_call" | custom-call | tf_op jit(solution)/shard_map/attention/pallas_call | solution.py:78
  69.2 2.0 %convolution_convert_fusion = bf16[128,2048]{1,0:T(8,128)(2,1)} fusion(bf16[128,256]{1,0:T(8,128)(2,1)} %attention.1, bf16[256,2048]{1,0:T(8,128)(2,1)S(1)} %copy-done), kind=kOutput, calls=%fused_computation | convolution fusion | flops 134479872 | bytes 1638400 | tf_op jit(solution)/shard_map/dot_general | solution.py:180
  71.1 6.0 %all-to-all-start = ((bf16[8,16,2048]{2,1,0:T(8,128)(2,1)}), bf16[8,16,2048]{2,1,0:T(8,128)(2,1)S(1)}, u32[]{:S(2)}, u32[]{:S(2)}) async-start(bf16[8,16,2048]{2,1,0:T(8,128)(2,1)} %bitcast.1), calls=%async_computation | async-start | bytes 1048576 | tf_op jit(solution)/shard_map/all_to_all | solution.py:19
  77.1 22.6 %all_gather.7.refs_3_ = bf16[256,768]{1,0:T(8,128)(2,1)S(1)} all-gather(bf16[32,768]{1,0:T(8,128)(2,1)} %bitcast.10), channel_id=1, replica_groups={{0,8,16,24,32,40,48,56},{64,72,80,88,96,104,112,120},{128,136,144,152,1..., dimensions={0}, use_global_device_ids=true | all-gather | bytes 442368 | tf_op jit(solution)/shard_map/all_gather | solution.py:166
  101.6 6.8 %collective-permute-start.11 = (bf16[256,768]{1,0:T(8,128)(2,1)S(1)}, bf16[256,768]{1,0:T(8,128)(2,1)S(1)}, u32[]{:S(2)}, u32[]{:S(2)}) collective-permute-start(bf16[256,768]{1,0:T(8,128)(2,1)S(1)} %all_gather.7.refs_3_), channel_id=1, source_target_pairs={{0,448},{8,456},{16,464},{24,472},{32,480},{40,488},{48,496},{56,5... | collective-permute-start | bytes 1179656 | tf_op jit(solution)/shard_map/ppermute | solution.py:13
  108.4 14.9 %collective-permute-done.7.refs_4_ = bf16[256,768]{1,0:T(8,128)(2,1)S(1)} collective-permute-done((bf16[256,768]{1,0:T(8,128)(2,1)S(1)}, bf16[256,768]{1,0:T(8,128)(2,1)S(1)}, u32[]{:S(2)}, u32[]{:S(2)}) %collective-permute-start.7) | collective-permute-done | bytes 393248 | tf_op jit(solution)/shard_map/ppermute | solution.py:13
  125.3 4.6 %collective-permute-start.12 = (bf16[256,768]{1,0:T(8,128)(2,1)S(1)}, bf16[256,768]{1,0:T(8,128)(2,1)}, u32[]{:S(2)}, u32[]{:S(2)}) collective-permute-start(bf16[256,768]{1,0:T(8,128)(2,1)S(1)} %collective-permute-done.11.refs_10_), channel_id=1, source_target_pairs={{0,448},{8,456},{16,464},{24,472},{32,480},{40,488},{48,496},{56,5... | collective-permute-start | bytes 1179656 | tf_op jit(solution)/shard_map/ppermute | solution.py:13
  130.9 4.3 %collective-permute-done.8.refs_5_ = bf16[256,768]{1,0:T(8,128)(2,1)S(1)} collective-permute-done((bf16[256,768]{1,0:T(8,128)(2,1)S(1)}, bf16[256,768]{1,0:T(8,128)(2,1)S(1)}, u32[]{:S(2)}, u32[]{:S(2)}) %collective-permute-start.8) | collective-permute-done | bytes 393248 | tf_op jit(solution)/shard_map/ppermute | solution.py:13
  139.0 6.7 %all-to-all-start.1 = ((bf16[8,16,2048]{2,1,0:T(8,128)(2,1)}), bf16[8,16,2048]{2,1,0:T(8,128)(2,1)S(1)}, u32[]{:S(2)}, u32[]{:S(2)}) async-start(bf16[8,16,2048]{2,1,0:T(8,128)(2,1)} %broadcast_in_dim.9), calls=%async_computation.1 | async-start | bytes 1048576 | tf_op jit(solution)/shard_map/all_to_all | solution.py:25
  145.7 5.0 %collective-permute-start.13 = (bf16[256,768]{1,0:T(8,128)(2,1)}, bf16[256,768]{1,0:T(8,128)(2,1)}, u32[]{:S(2)}, u32[]{:S(2)}) collective-permute-start(bf16[256,768]{1,0:T(8,128)(2,1)} %collective-permute-done.12.refs_9_), channel_id=1, source_target_pairs={{0,448},{8,456},{16,464},{24,472},{32,480},{40,488},{48,496},{56,5... | collective-permute-start | bytes 1179656 | tf_op jit(solution)/shard_map/ppermute | solution.py:13
  155.0 4.4 %collective-permute-done.13.refs_8_ = bf16[256,768]{1,0:T(8,128)(2,1)} collective-permute-done((bf16[256,768]{1,0:T(8,128)(2,1)}, bf16[256,768]{1,0:T(8,128)(2,1)}, u32[]{:S(2)}, u32[]{:S(2)}) %collective-permute-start.13) | collective-permute-done | bytes 393248 | tf_op jit(solution)/shard_map/ppermute | solution.py:13
  159.4 5.1 %collective-permute-done.10.refs_7_ = bf16[256,768]{1,0:T(8,128)(2,1)} collective-permute-done((bf16[256,768]{1,0:T(8,128)(2,1)}, bf16[256,768]{1,0:T(8,128)(2,1)}, u32[]{:S(2)}, u32[]{:S(2)}) %collective-permute-start.10) | collective-permute-done | bytes 393248 | tf_op jit(solution)/shard_map/ppermute | solution.py:13
  164.5 8.7 %ffn.1 = bf16[128,2048]{1,0:T(8,128)(2,1)} custom-call(s32[8]{0:T(128)} %and_select_fusion.refs_0_, bf16[128,2048]{1,0:T(8,128)(2,1)} %bitcast.8, bf16[2048,1536]{1,0:T(8,128)(2,1)} %all-gather.2.cloned.1.call-done.refs_2_, bf16[256,768]{1,0:T(8,128)(2,1)} %copy-done.2, bf16[256,768]{1,0:T(8,128)(2,1)} %copy-done.5, bf16[256,768]{1,0:T(8,128)(2,1)} %copy-done.7, ...), custom_call_target="tpu_custom_call" | custom-call | tf_op jit(solution)/shard_map/ffn/pallas_call | solution.py:129
  173.2 14.9 %all_to_all.15 = bf16[8,16,2048]{2,1,0:T(8,128)(2,1)S(1)} all-to-all(bf16[8,16,2048]{2,1,0:T(8,128)(2,1)} %bitcast.9), channel_id=1, replica_groups=mesh['sp'=64,'tp'=8] {'tp'}, dimensions={0} | all-to-all | bytes 1048576 | tf_op jit(solution)/shard_map/all_to_all | solution.py:19
  (57 shorter events, 17.5 us)
Async XLA Ops:
  6.5 62.6 %copy-start = (bf16[256,2048]{1,0:T(8,128)(2,1)S(1)}, bf16[256,2048]{1,0:T(8,128)(2,1)}, u32[]{:S(2)}) copy-start(bf16[256,2048]{1,0:T(8,128)(2,1)} %param.17) | copy-start | bytes 3145732
  6.5 157.9 %all-gather.2.cloned.1.call-start = ((), (), s32[]{:S(2)}) async-start(), calls=%async_computation.3 | async-start | bytes 6389760 | tf_op jit(solution)/shard_map/all_gather | solution.py:159
  9.7 52.1 %copy-start.3 = (bf16[144,512]{1,0:T(8,128)(2,1)}, bf16[144,512]{1,0:T(8,128)(2,1)S(1)}, u32[]{:S(2)}) copy-start(bf16[144,512]{1,0:T(8,128)(2,1)S(1)} %fusion.1.refs_2_) | copy-start | bytes 442372
  9.7 23.1 %collective-permute-start = (bf16[144,512]{1,0:T(8,128)(2,1)S(1)}, bf16[144,512]{1,0:T(8,128)(2,1)S(1)}, u32[]{:S(2)}, u32[]{:S(2)}) collective-permute-start(bf16[144,512]{1,0:T(8,128)(2,1)S(1)} %fusion.1.refs_2_), channel_id=1, source_target_pairs={{0,8},{8,16},{16,24},{24,32},{32,40},{40,48},{48,56},{56,64},{64,7... | collective-permute-start | bytes 442376 | tf_op jit(solution)/shard_map/ppermute | solution.py:13
  13.7 25.9 %collective-permute-start.1 = (bf16[144,512]{1,0:T(8,128)(2,1)S(1)}, bf16[144,512]{1,0:T(8,128)(2,1)S(1)}, u32[]{:S(2)}, u32[]{:S(2)}) collective-permute-start(bf16[144,512]{1,0:T(8,128)(2,1)S(1)} %fusion.1.refs_2_), channel_id=1, source_target_pairs={{0,16},{8,24},{16,32},{24,40},{32,48},{40,56},{48,64},{56,72},{64,... | collective-permute-start | bytes 442376 | tf_op jit(solution)/shard_map/ppermute | solution.py:13
  17.9 26.5 %collective-permute-start.2 = (bf16[144,512]{1,0:T(8,128)(2,1)S(1)}, bf16[144,512]{1,0:T(8,128)(2,1)S(1)}, u32[]{:S(2)}, u32[]{:S(2)}) collective-permute-start(bf16[144,512]{1,0:T(8,128)(2,1)S(1)} %fusion.1.refs_2_), channel_id=1, source_target_pairs={{0,24},{8,32},{16,40},{24,48},{32,56},{40,64},{48,72},{56,80},{64,... | collective-permute-start | bytes 442376 | tf_op jit(solution)/shard_map/ppermute | solution.py:13
  22.6 29.7 %collective-permute-start.3 = (bf16[144,512]{1,0:T(8,128)(2,1)S(1)}, bf16[144,512]{1,0:T(8,128)(2,1)S(1)}, u32[]{:S(2)}, u32[]{:S(2)}) collective-permute-start(bf16[144,512]{1,0:T(8,128)(2,1)S(1)} %fusion.1.refs_2_), channel_id=1, source_target_pairs={{0,32},{8,40},{16,48},{24,56},{32,64},{40,72},{48,80},{56,88},{64,... | collective-permute-start | bytes 442376 | tf_op jit(solution)/shard_map/ppermute | solution.py:13
  27.9 24.4 %collective-permute-start.4 = (bf16[144,512]{1,0:T(8,128)(2,1)S(1)}, bf16[144,512]{1,0:T(8,128)(2,1)S(1)}, u32[]{:S(2)}, u32[]{:S(2)}) collective-permute-start(bf16[144,512]{1,0:T(8,128)(2,1)S(1)} %fusion.1.refs_2_), channel_id=1, source_target_pairs={{0,40},{8,48},{16,56},{24,64},{32,72},{40,80},{48,88},{56,96},{64,... | collective-permute-start | bytes 442376 | tf_op jit(solution)/shard_map/ppermute | solution.py:13
  32.8 25.7 %collective-permute-start.5 = (bf16[144,512]{1,0:T(8,128)(2,1)S(1)}, bf16[144,512]{1,0:T(8,128)(2,1)S(1)}, u32[]{:S(2)}, u32[]{:S(2)}) collective-permute-start(bf16[144,512]{1,0:T(8,128)(2,1)S(1)} %fusion.1.refs_2_), channel_id=1, source_target_pairs={{0,48},{8,56},{16,64},{24,72},{32,80},{40,88},{48,96},{56,104},{64... | collective-permute-start | bytes 442376 | tf_op jit(solution)/shard_map/ppermute | solution.py:13
  39.6 22.1 %collective-permute-start.6 = (bf16[144,512]{1,0:T(8,128)(2,1)S(1)}, bf16[144,512]{1,0:T(8,128)(2,1)S(1)}, u32[]{:S(2)}, u32[]{:S(2)}) collective-permute-start(bf16[144,512]{1,0:T(8,128)(2,1)S(1)} %fusion.1.refs_2_), channel_id=1, source_target_pairs={{0,56},{8,64},{16,72},{24,80},{32,88},{40,96},{48,104},{56,112},{6... | collective-permute-start | bytes 442376 | tf_op jit(solution)/shard_map/ppermute | solution.py:13
  71.1 58.7 %all-to-all-start = ((bf16[8,16,2048]{2,1,0:T(8,128)(2,1)}), bf16[8,16,2048]{2,1,0:T(8,128)(2,1)S(1)}, u32[]{:S(2)}, u32[]{:S(2)}) async-start(bf16[8,16,2048]{2,1,0:T(8,128)(2,1)} %bitcast.1), calls=%async_computation | async-start | bytes 1048576 | tf_op jit(solution)/shard_map/all_to_all | solution.py:19
  99.7 64.8 %copy-start.2 = (bf16[256,768]{1,0:T(8,128)(2,1)}, bf16[256,768]{1,0:T(8,128)(2,1)S(1)}, u32[]{:S(2)}) copy-start(bf16[256,768]{1,0:T(8,128)(2,1)S(1)} %all_gather.7.refs_3_) | copy-start | bytes 1179652
  99.7 23.6 %collective-permute-start.7 = (bf16[256,768]{1,0:T(8,128)(2,1)S(1)}, bf16[256,768]{1,0:T(8,128)(2,1)S(1)}, u32[]{:S(2)}, u32[]{:S(2)}) collective-permute-start(bf16[256,768]{1,0:T(8,128)(2,1)S(1)} %all_gather.7.refs_3_), channel_id=1, source_target_pairs={{0,64},{8,72},{16,80},{24,88},{32,96},{40,104},{48,112},{56,120},{... | collective-permute-start | bytes 1179656 | tf_op jit(solution)/shard_map/ppermute | solution.py:13
  101.6 23.6 %collective-permute-start.11 = (bf16[256,768]{1,0:T(8,128)(2,1)S(1)}, bf16[256,768]{1,0:T(8,128)(2,1)S(1)}, u32[]{:S(2)}, u32[]{:S(2)}) collective-permute-start(bf16[256,768]{1,0:T(8,128)(2,1)S(1)} %all_gather.7.refs_3_), channel_id=1, source_target_pairs={{0,448},{8,456},{16,464},{24,472},{32,480},{40,488},{48,496},{56,5... | collective-permute-start | bytes 1179656 | tf_op jit(solution)/shard_map/ppermute | solution.py:13
  123.3 41.2 %copy-start.5 = (bf16[256,768]{1,0:T(8,128)(2,1)}, bf16[256,768]{1,0:T(8,128)(2,1)S(1)}, u32[]{:S(2)}) copy-start(bf16[256,768]{1,0:T(8,128)(2,1)S(1)} %collective-permute-done.7.refs_4_) | copy-start | bytes 1179652
  123.3 11.9 %collective-permute-start.8 = (bf16[256,768]{1,0:T(8,128)(2,1)S(1)}, bf16[256,768]{1,0:T(8,128)(2,1)S(1)}, u32[]{:S(2)}, u32[]{:S(2)}) collective-permute-start(bf16[256,768]{1,0:T(8,128)(2,1)S(1)} %collective-permute-done.7.refs_4_), channel_id=1, source_target_pairs={{0,64},{8,72},{16,80},{24,88},{32,96},{40,104},{48,112},{56,120},{... | collective-permute-start | bytes 1179656 | tf_op jit(solution)/shard_map/ppermute | solution.py:13
  125.3 39.2 %copy-start.6 = (bf16[256,768]{1,0:T(8,128)(2,1)}, bf16[256,768]{1,0:T(8,128)(2,1)S(1)}, u32[]{:S(2)}) copy-start(bf16[256,768]{1,0:T(8,128)(2,1)S(1)} %collective-permute-done.11.refs_10_) | copy-start | bytes 1179652
  125.3 20.4 %collective-permute-start.12 = (bf16[256,768]{1,0:T(8,128)(2,1)S(1)}, bf16[256,768]{1,0:T(8,128)(2,1)}, u32[]{:S(2)}, u32[]{:S(2)}) collective-permute-start(bf16[256,768]{1,0:T(8,128)(2,1)S(1)} %collective-permute-done.11.refs_10_), channel_id=1, source_target_pairs={{0,448},{8,456},{16,464},{24,472},{32,480},{40,488},{48,496},{56,5... | collective-permute-start | bytes 1179656 | tf_op jit(solution)/shard_map/ppermute | solution.py:13
  135.2 29.3 %copy-start.7 = (bf16[256,768]{1,0:T(8,128)(2,1)}, bf16[256,768]{1,0:T(8,128)(2,1)S(1)}, u32[]{:S(2)}) copy-start(bf16[256,768]{1,0:T(8,128)(2,1)S(1)} %collective-permute-done.8.refs_5_) | copy-start | bytes 1179652
  135.2 15.4 %collective-permute-start.9 = (bf16[256,768]{1,0:T(8,128)(2,1)S(1)}, bf16[256,768]{1,0:T(8,128)(2,1)}, u32[]{:S(2)}, u32[]{:S(2)}) collective-permute-start(bf16[256,768]{1,0:T(8,128)(2,1)S(1)} %collective-permute-done.8.refs_5_), channel_id=1, source_target_pairs={{0,64},{8,72},{16,80},{24,88},{32,96},{40,104},{48,112},{56,120},{... | collective-permute-start | bytes 1179656 | tf_op jit(solution)/shard_map/ppermute | solution.py:13
  139.0 16.1 %all-to-all-start.1 = ((bf16[8,16,2048]{2,1,0:T(8,128)(2,1)}), bf16[8,16,2048]{2,1,0:T(8,128)(2,1)S(1)}, u32[]{:S(2)}, u32[]{:S(2)}) async-start(bf16[8,16,2048]{2,1,0:T(8,128)(2,1)} %broadcast_in_dim.9), calls=%async_computation.1 | async-start | bytes 1048576 | tf_op jit(solution)/shard_map/all_to_all | solution.py:25
  145.7 42.5 %copy-start.4 = (bf16[16,2048]{1,0:T(8,128)(2,1)S(1)}, bf16[16,2048]{1,0:T(8,128)(2,1)}, u32[]{:S(2)}) copy-start(bf16[16,2048]{1,0:T(8,128)(2,1)} %param.11) | copy-start | bytes 196612
  145.7 13.7 %collective-permute-start.13 = (bf16[256,768]{1,0:T(8,128)(2,1)}, bf16[256,768]{1,0:T(8,128)(2,1)}, u32[]{:S(2)}, u32[]{:S(2)}) collective-permute-start(bf16[256,768]{1,0:T(8,128)(2,1)} %collective-permute-done.12.refs_9_), channel_id=1, source_target_pairs={{0,448},{8,456},{16,464},{24,472},{32,480},{40,488},{48,496},{56,5... | collective-permute-start | bytes 1179656 | tf_op jit(solution)/shard_map/ppermute | solution.py:13
  150.7 13.8 %collective-permute-start.10 = (bf16[256,768]{1,0:T(8,128)(2,1)}, bf16[256,768]{1,0:T(8,128)(2,1)}, u32[]{:S(2)}, u32[]{:S(2)}) collective-permute-start(bf16[256,768]{1,0:T(8,128)(2,1)} %collective-permute-done.9.refs_6_), channel_id=1, source_target_pairs={{0,64},{8,72},{16,80},{24,88},{32,96},{40,104},{48,112},{56,120},{... | collective-permute-start | bytes 1179656 | tf_op jit(solution)/shard_map/ppermute | solution.py:13
  (8 other events, 100.8 us)
Sparse Core Ops, SparseCore 0:
  10.3 113.5 all-gather.1

commit v3 on v1

--- a/solution.py
+++ b/solution.py
@@ -1,3 +1,5 @@
+from functools import partial
+
 import jax
 import jax.numpy as jnp
 from jax import lax
@@ -11,9 +13,9 @@
     return lax.ppermute(block, "sp", [(i, (i + by) % spans) for i in range(spans)])
 
 
-def summed_for_owner(partial):
+def summed_for_owner(terms):
     peers = lax.axis_size("tp")
-    tiles = partial.reshape(peers, partial.shape[0] // peers, partial.shape[1])
+    tiles = terms.reshape(peers, terms.shape[0] // peers, terms.shape[1])
     tiles = lax.all_to_all(tiles, "tp", 0, 0, tiled=True)
     return jnp.sum(tiles.astype(jnp.float32), axis=0)
 
@@ -78,11 +80,75 @@
         out_shape=jax.ShapeDtypeStruct((rows, width), jnp.bfloat16),
         in_specs=[pl.BlockSpec(memory_space=pltpu.SMEM)] + [vmem] * (1 + len(blocks)),
         out_specs=vmem,
+        compiler_params=pltpu.CompilerParams(vmem_limit_bytes=12 << 20),
         name="attention",
     )(offsets, queries, *blocks)
 
 
+def around(block, pairs, steps):
+    got = {0: block}
+    for back in range(1, steps // 2 + 1):
+        got[back] = lax.ppermute(got[back - 1], "sp", pairs)
+        if steps - back > steps // 2:
+            got[steps - back] = lax.ppermute(
+                got[(steps - back + 1) % steps], "sp", [(j, i) for i, j in pairs]
+            )
+    return [got[k] for k in range(steps)]
+
+
+def spread(copies, groups):
+    tiles = lax.all_to_all(copies, "sp", 0, 0, tiled=True, axis_index_groups=groups)
+    return tiles.reshape(copies.shape[0] * copies.shape[1], copies.shape[2])
+
+
+def ffn_kernel(ring, low, places, x, *refs):
+    first, second, (out, x_turned) = refs[:ring], refs[ring : 2 * ring], refs[2 * ring :]
+    step = first[0].shape[0]
+    high = first[0].shape[1] - (second[0].shape[1] - low)
+
+    def part(rows, i):
+        return rows[:, pl.ds(pl.multiple_of(places[i] * step, step), step)]
+
+    wide = step // ring
+    for y in range(ring):
+        x_turned[:, y * step : (y + 1) * step] = jnp.concatenate(
+            [x[:, z * step + y * wide : z * step + (y + 1) * wide] for z in range(ring)], axis=1
+        )
+    gate_high = low_up = None
+    for k in range(ring):
+        one = jnp.dot(part(x, k), first[k][:, :high], preferred_element_type=jnp.float32)
+        two = jnp.dot(part(x_turned, ring + k), second[k][...], preferred_element_type=jnp.float32)
+        gate_high = one if k == 0 else gate_high + one
+        low_up = two if k == 0 else low_up + two
+    gate = jnp.concatenate([low_up[:, :low], gate_high], axis=1)
+    hidden = (gate / (1.0 + jnp.exp(-gate)) * low_up[:, low:]).astype(jnp.bfloat16)
+    for k in range(ring):
+        term = lax.dot_general(
+            hidden, first[k][:, high:], (((1,), (1,)), ((), ())), preferred_element_type=jnp.float32
+        )
+        out[:, pl.ds(pl.multiple_of(places[k] * step, step), step)] = term.astype(jnp.bfloat16)
+
+
+def ffn(x, first, second, places, low):
+    ring = len(first)
+    vmem = pl.BlockSpec(memory_space=pltpu.VMEM)
+
+    def body(*refs):
+        ffn_kernel(ring, low, *refs)
+
+    return pl.pallas_call(
+        body,
+        out_shape=jax.ShapeDtypeStruct(x.shape, jnp.bfloat16),
+        in_specs=[pl.BlockSpec(memory_space=pltpu.SMEM)] + [vmem] * (1 + 2 * ring),
+        out_specs=vmem,
+        scratch_shapes=[pltpu.VMEM(x.shape, jnp.bfloat16)],
+        compiler_params=pltpu.CompilerParams(vmem_limit_bytes=24 << 20),
+        name="ffn",
+    )(places, x, *first, *second)
+
+
 def on_device(
+    ring,
     resid,
     queries,
     keys,
@@ -97,17 +163,39 @@
 ):
     rows = queries.shape[0]
     units = gate_weight.shape[1]
-    packed = jnp.concatenate([gate_weight, up_weight, down_weight.T], axis=1)
-    weights = lax.all_gather(packed, "sp", axis=0, tiled=True)
+    low = units // 2
+    spans = lax.axis_size("sp")
+    rings = spans // ring
+    along_y = [[z * ring + y for y in range(ring)] for z in range(rings)]
+    along_z = [[z * ring + y for z in range(rings)] for y in range(ring)]
+    next_y = [(g[i], g[(i + 1) % ring]) for g in along_y for i in range(ring)]
+    next_z = [(g[i], g[(i + 1) % rings]) for g in along_z for i in range(rings)]
+    first = jnp.concatenate([gate_weight[:, low:], down_weight.T], axis=1)
+    second = jnp.concatenate([gate_weight[:, :low], up_weight], axis=1)
+    first = jnp.broadcast_to(first, (ring, *first.shape))
+    second = jnp.broadcast_to(second, (rings, *second.shape))
+    first, second = lax.optimization_barrier((first, second))
+    with jax.named_scope("spread_first"):
+        first = spread(first, along_y)
+    with jax.named_scope("spread_second"):
+        second = spread(second, along_z)
+    with jax.named_scope("ring_first"):
+        first = around(first, next_z, rings)
+    with jax.named_scope("ring_second"):
+        second = around(second, next_y, ring)
+    at = lax.axis_index("sp")
+    back = jnp.arange(ring, dtype=jnp.int32)
+    places = jnp.concatenate(
+        [(at // ring + rings - back) & (rings - 1), ((at & (ring - 1)) + ring - back) & (ring - 1)]
+    )
 
     docs = jnp.pad(doc_ids.astype(jnp.bfloat16)[None], ((0, 15), (0, 2 * keys.shape[1] - rows)))
     own = jnp.concatenate([jnp.concatenate([keys, values], axis=1), docs], axis=0)
-    blocks = {0: own}
-    blocks[7] = shifted(own, 7)
-    for back in range(1, 5):
-        blocks[back] = shifted(blocks[back - 1], 1)
-        if back < 3:
-            blocks[7 - back] = shifted(blocks[8 - back], -1)
+    with jax.named_scope("kv_near"):
+        near = {k: shifted(own, k) for k in (2, 6, 1, 7)}
+    with jax.named_scope("kv_far"):
+        far = {4: shifted(near[2], 2), 3: shifted(near[2], 1), 5: shifted(near[6], -1)}
+    blocks = {0: own, **near, **far}
     attended = attention(queries, [blocks[b] for b in range(8)], score_offset)
 
     mixed_attn = summed_for_owner(
@@ -117,17 +205,8 @@
     normed = (
         stream * lax.rsqrt(jnp.mean(stream * stream, axis=1, keepdims=True) + 1e-06) * norm_gain
     ).astype(jnp.bfloat16)
-    span_rows = from_everyone(normed).reshape(rows, -1)
-    gate = jnp.dot(span_rows, weights[:, :units], preferred_element_type=jnp.float32)
-    upper = jnp.dot(span_rows, weights[:, units : 2 * units], preferred_element_type=jnp.float32)
-    hidden = (jax.nn.silu(gate) * upper).astype(jnp.bfloat16)
-    partial_out = lax.dot_general(
-        hidden,
-        weights[:, 2 * units :],
-        (((1,), (1,)), ((), ())),
-        preferred_element_type=jnp.float32,
-    )
-    feed = summed_for_owner(partial_out.astype(jnp.bfloat16))
+    x = from_everyone(normed).reshape(rows, -1)
+    feed = summed_for_owner(ffn(x, first, second, places, low))
     return (stream + feed).astype(jnp.bfloat16)
 
 
@@ -147,5 +226,5 @@
     )
     out_specs = P(("sp", "tp"), None)
     return jax.shard_map(
-        on_device, mesh=mesh, in_specs=in_specs, out_specs=out_specs, check_vma=False
-    )
+        partial(on_device, 8), mesh=mesh, in_specs=in_specs, out_specs=out_specs, check_vma=False
+    )

time: 150 us -> 184 us (1.23)
  starting transfers between devices: 28.3 us -> 83.3 us
  between operations: 13.6 us -> 0.41 us
  matrix products: 8.13 us -> 1.1 us
  other arithmetic: 5.87 us -> 1.14 us
  Pallas kernels: 6.72 us -> 11.1 us
  blocking collectives: 46.5 us -> 42.3 us
  local copies, waits for them, and re-layouts: 0.73 us -> 2.76 us
    ppermute x0 -> x14, starting transfers between devices: none -> 38.2 us  [the longest x8 20.1 us: around(): got[back] = lax.ppermute(got[back - 1], 'sp', pairs)]
    all_to_all x0 -> x3, starting transfers between devices: none -> 26.5 us  [the longest x1 13.7 us: summed_for_owner(): tiles = lax.all_to_all(tiles, 'tp', 0, 0, tiled=True)]
    all_to_all x0 -> x3, waiting for transfers between devices: none -> 22.5 us  [the longest x1 13.2 us: spread(): lax.all_to_all(copies, 'sp', 0, 0, tiled=True, axis_index_groups=groups)]
    all_gather x1 -> x0, waiting for transfers between devices: 20 us -> none  [on_device(): weights = lax.all_gather(packed, 'sp', axis=0, tiled=True)]
    all_to_all x2 -> x1, blocking collectives: 33.7 us -> 14.1 us  [summed_for_owner(): tiles = lax.all_to_all(tiles, 'tp', 0, 0, tiled=True)]
    all_to_all x1, blocking collectives: 12.8 us -> 28.2 us  [spread(): lax.all_to_all(copies, 'sp', 0, 0, tiled=True, axis_index_groups=groups)]
    ppermute x7, starting transfers between devices: 28.3 us -> 18.6 us  [shifted(): lax.ppermute(block, 'sp', [(i, (i + by) % spans) for i in range(spans)])]
    ppermute x7, waiting for transfers between devices: 19 us -> 11.9 us  [shifted(): lax.ppermute(block, 'sp', [(i, (i + by) % spans) for i in range(spans)])]
  transfers between devices with their start and end apart: 8 -> 24, of which waited for: 5 -> 7; matrix products, arithmetic and copies ran while one was open for 3% -> 1% of each run, Pallas kernels for 5% -> 3%
where the time goes in v3:
time: 184 us; the launch traced here: 183 us
  starting transfers between devices  83.3 us (45%)
  blocking collectives  42.3 us (23%)
  waiting for transfers between devices  40.6 us (22%)
  Pallas kernels  11.1 us (6%)
  local copies, waits for them, and re-layouts  2.76 us (2%)
    all_to_all x1, blocking collectives, spread(): lax.all_to_all(copies, 'sp', 0, 0, tiled=True, axis_index_groups=groups)  28.2 us
    ppermute x8, starting transfers between devices, around(): got[back] = lax.ppermute(got[back - 1], 'sp', pairs)  20.1 us
    ppermute x7, starting transfers between devices, shifted(): lax.ppermute(block, 'sp', [(i, (i + by) % spans) for i in range(spans)])  18.6 us
    ppermute x6, starting transfers between devices, around(): lax.ppermute(got[(steps - back + 1) % steps], 'sp', [(j, i) for i, j in p...  18.1 us
    all_to_all x1, blocking collectives, summed_for_owner(): tiles = lax.all_to_all(tiles, 'tp', 0, 0, tiled=True)  14.1 us
    all_to_all x1, starting transfers between devices, summed_for_owner(): tiles = lax.all_to_all(tiles, 'tp', 0, 0, tiled=True)  13.7 us
    all_to_all x1, waiting for transfers between devices, spread(): lax.all_to_all(copies, 'sp', 0, 0, tiled=True, axis_index_groups=groups)  13.2 us
    ppermute x7, waiting for transfers between devices, shifted(): lax.ppermute(block, 'sp', [(i, (i + by) % spans) for i in range(spans)])  11.9 us
  transfers between devices with their start and end apart: 24, of which 7 were waited for; matrix products, arithmetic and copies ran while one was open for 1% of the time, Pallas kernels for 3%

profile of v3, /device:TPU:1, one launch (start us, length us, event | category | flops | bytes accessed | tf_op | source)
XLA Modules:
  0.0 182.8 jit_solution(14810086455783353263)
XLA Ops:
  1.9 28.2 %all_to_all.25 = bf16[8,32,1152]{2,1,0:T(8,128)(2,1)S(1)} all-to-all(bf16[8,32,1152]{2,1,0:T(8,128)(2,1)S(1)} %broadcast_in_dim.17), channel_id=1, replica_groups={{0,64,128,192,256,320,384,448},{8,72,136,200,264,328,392,456},{16,80,14..., dimensions={0} | all-to-all | bytes 1179648 | tf_op jit(solution)/shard_map/spread_second/all_to_all | solution.py:100
  30.1 7.0 %all-to-all-start.2 = ((bf16[8,32,1152]{2,1,0:T(8,128)(2,1)}), bf16[8,32,1152]{2,1,0:T(8,128)(2,1)S(1)}, u32[]{:S(2)}, u32[]{:S(2)}) async-start(bf16[8,32,1152]{2,1,0:T(8,128)(2,1)} %broadcast_in_dim.16), calls=%async_computation.2 | async-start | bytes 1179648 | tf_op jit(solution)/shard_map/spread_first/all_to_all | solution.py:100
  37.0 3.5 %collective-permute-start.14 = (bf16[256,1152]{1,0:T(8,128)(2,1)S(1)}, bf16[256,1152]{1,0:T(8,128)(2,1)S(1)}, u32[]{:S(2)}, u32[]{:S(2)}) collective-permute-start(bf16[256,1152]{1,0:T(8,128)(2,1)S(1)} %bitcast.10), channel_id=1, source_target_pairs={{0,8},{8,16},{16,24},{24,32},{32,40},{40,48},{48,56},{56,0},{64,72... | collective-permute-start | bytes 1769480 | tf_op jit(solution)/shard_map/ring_second/ppermute | solution.py:91
  40.5 13.2 %all-to-all-done.2 = bf16[8,32,1152]{2,1,0:T(8,128)(2,1)S(1)} async-done(((bf16[8,32,1152]{2,1,0:T(8,128)(2,1)}), bf16[8,32,1152]{2,1,0:T(8,128)(2,1)S(1)}, u32[]{:S(2)}, u32[]{:S(2)}) %all-to-all-start.2) | async-done | bytes 589856 | tf_op jit(solution)/shard_map/spread_first/all_to_all | solution.py:100
  59.7 3.2 %collective-permute-start.1 = (bf16[144,512]{1,0:T(8,128)(2,1)S(1)}, bf16[144,512]{1,0:T(8,128)(2,1)S(1)}, u32[]{:S(2)}, u32[]{:S(2)}) collective-permute-start(bf16[144,512]{1,0:T(8,128)(2,1)S(1)} %fusion.1.refs_2_), channel_id=1, source_target_pairs={{0,16},{8,24},{16,32},{24,40},{32,48},{40,56},{48,64},{56,72},{64,... | collective-permute-start | bytes 442376 | tf_op jit(solution)/shard_map/kv_near/ppermute | solution.py:13
  63.9 3.9 %collective-permute-start = (bf16[144,512]{1,0:T(8,128)(2,1)S(1)}, bf16[144,512]{1,0:T(8,128)(2,1)S(1)}, u32[]{:S(2)}, u32[]{:S(2)}) collective-permute-start(bf16[144,512]{1,0:T(8,128)(2,1)S(1)} %fusion.1.refs_2_), channel_id=1, source_target_pairs={{0,8},{8,16},{16,24},{24,32},{32,40},{40,48},{48,56},{56,64},{64,7... | collective-permute-start | bytes 442376 | tf_op jit(solution)/shard_map/kv_near/ppermute | solution.py:13
  67.8 2.5 %collective-permute-done.4.refs_8_ = bf16[144,512]{1,0:T(8,128)(2,1)S(1)} collective-permute-done((bf16[144,512]{1,0:T(8,128)(2,1)S(1)}, bf16[144,512]{1,0:T(8,128)(2,1)S(1)}, u32[]{:S(2)}, u32[]{:S(2)}) %collective-permute-start.4) | collective-permute-done | bytes 147488 | tf_op jit(solution)/shard_map/kv_near/ppermute | solution.py:13
  74.5 3.4 %collective-permute-start.2 = (bf16[144,512]{1,0:T(8,128)(2,1)S(1)}, bf16[144,512]{1,0:T(8,128)(2,1)S(1)}, u32[]{:S(2)}, u32[]{:S(2)}) collective-permute-start(bf16[144,512]{1,0:T(8,128)(2,1)S(1)} %collective-permute-done.1.refs_4_), channel_id=1, source_target_pairs={{0,8},{8,16},{16,24},{24,32},{32,40},{40,48},{48,56},{56,64},{64,7... | collective-permute-start | bytes 442376 | tf_op jit(solution)/shard_map/kv_far/ppermute | solution.py:13
  77.9 4.9 %collective-permute-done.3.refs_6_ = bf16[144,512]{1,0:T(8,128)(2,1)S(1)} collective-permute-done((bf16[144,512]{1,0:T(8,128)(2,1)S(1)}, bf16[144,512]{1,0:T(8,128)(2,1)S(1)}, u32[]{:S(2)}, u32[]{:S(2)}) %collective-permute-start.3) | collective-permute-done | bytes 147488 | tf_op jit(solution)/shard_map/kv_far/ppermute | solution.py:13
  82.8 3.6 %collective-permute-done.2.refs_5_ = bf16[144,512]{1,0:T(8,128)(2,1)S(1)} collective-permute-done((bf16[144,512]{1,0:T(8,128)(2,1)S(1)}, bf16[144,512]{1,0:T(8,128)(2,1)S(1)}, u32[]{:S(2)}, u32[]{:S(2)}) %collective-permute-start.2) | collective-permute-done | bytes 147488 | tf_op jit(solution)/shard_map/kv_far/ppermute | solution.py:13
  86.4 5.3 %attention.1 = bf16[128,256]{1,0:T(8,128)(2,1)S(1)} custom-call(f32[4]{0:T(128)S(1)} %copy-done.2, bf16[128,256]{1,0:T(8,128)(2,1)S(1)} %copy-done.1, bf16[144,512]{1,0:T(8,128)(2,1)S(1)} %fusion.1.refs_2_, bf16[144,512]{1,0:T(8,128)(2,1)S(1)} %collective-permute-done.refs_3_, bf16[144,512]{1,0:T(8,128)(2,1)S(1)} %collective-permute-done.1.refs_4_, ...), custom_call_target="tpu_custom_call" | custom-call | tf_op jit(solution)/shard_map/attention/pallas_call | solution.py:78
  95.5 3.4 %collective-permute-start.15 = (bf16[256,1152]{1,0:T(8,128)(2,1)S(1)}, bf16[256,1152]{1,0:T(8,128)(2,1)}, u32[]{:S(2)}, u32[]{:S(2)}) collective-permute-start(bf16[256,1152]{1,0:T(8,128)(2,1)S(1)} %collective-permute-done.14.refs_11_), channel_id=1, source_target_pairs={{0,8},{8,16},{16,24},{24,32},{32,40},{40,48},{48,56},{56,0},{64,72... | collective-permute-start | bytes 1769480 | tf_op jit(solution)/shard_map/ring_second/ppermute | solution.py:91
  98.9 3.4 %collective-permute-start.8 = (bf16[256,1152]{1,0:T(8,128)(2,1)}, bf16[256,1152]{1,0:T(8,128)(2,1)}, u32[]{:S(2)}, u32[]{:S(2)}) collective-permute-start(bf16[256,1152]{1,0:T(8,128)(2,1)} %collective-permute-done.7.refs_3_), channel_id=1, source_target_pairs={{0,64},{64,128},{128,192},{192,256},{256,320},{320,384},{384,448},... | collective-permute-start | bytes 1769480 | tf_op jit(solution)/shard_map/ring_first/ppermute | solution.py:91
  103.4 13.7 %all-to-all-start = ((bf16[8,16,2048]{2,1,0:T(8,128)(2,1)}), bf16[8,16,2048]{2,1,0:T(8,128)(2,1)S(1)}, u32[]{:S(2)}, u32[]{:S(2)}) async-start(bf16[8,16,2048]{2,1,0:T(8,128)(2,1)} %bitcast.1), calls=%async_computation | async-start | bytes 1048576 | tf_op jit(solution)/shard_map/all_to_all | solution.py:19
  117.1 3.0 %collective-permute-start.19 = (bf16[256,1152]{1,0:T(8,128)(2,1)}, bf16[256,1152]{1,0:T(8,128)(2,1)}, u32[]{:S(2)}, u32[]{:S(2)}) collective-permute-start(bf16[256,1152]{1,0:T(8,128)(2,1)} %collective-permute-done.18.refs_17_), channel_id=1, source_target_pairs={{8,0},{16,8},{24,16},{32,24},{40,32},{48,40},{56,48},{0,56},{72,64... | collective-permute-start | bytes 1769480 | tf_op jit(solution)/shard_map/ring_second/ppermute | solution.py:93
  120.1 3.6 %collective-permute-start.12 = (bf16[256,1152]{1,0:T(8,128)(2,1)}, bf16[256,1152]{1,0:T(8,128)(2,1)}, u32[]{:S(2)}, u32[]{:S(2)}) collective-permute-start(bf16[256,1152]{1,0:T(8,128)(2,1)} %collective-permute-done.11.refs_9_), channel_id=1, source_target_pairs={{64,0},{128,64},{192,128},{256,192},{320,256},{384,320},{448,384},... | collective-permute-start | bytes 1769480 | tf_op jit(solution)/shard_map/ring_first/ppermute | solution.py:93
  125.6 2.2 %collective-permute-start.9 = (bf16[256,1152]{1,0:T(8,128)(2,1)}, bf16[256,1152]{1,0:T(8,128)(2,1)}, u32[]{:S(2)}, u32[]{:S(2)}) collective-permute-start(bf16[256,1152]{1,0:T(8,128)(2,1)} %collective-permute-done.8.refs_4_), channel_id=1, source_target_pairs={{0,64},{64,128},{128,192},{192,256},{256,320},{320,384},{384,448},... | collective-permute-start | bytes 1769480 | tf_op jit(solution)/shard_map/ring_first/ppermute | solution.py:91
  128.1 6.2 %collective-permute-done.19.refs_16_ = bf16[256,1152]{1,0:T(8,128)(2,1)} collective-permute-done((bf16[256,1152]{1,0:T(8,128)(2,1)}, bf16[256,1152]{1,0:T(8,128)(2,1)}, u32[]{:S(2)}, u32[]{:S(2)}) %collective-permute-start.19) | collective-permute-done | bytes 589856 | tf_op jit(solution)/shard_map/ring_second/ppermute | solution.py:93
  134.3 4.1 %collective-permute-start.20 = (bf16[256,1152]{1,0:T(8,128)(2,1)}, bf16[256,1152]{1,0:T(8,128)(2,1)}, u32[]{:S(2)}, u32[]{:S(2)}) collective-permute-start(bf16[256,1152]{1,0:T(8,128)(2,1)} %collective-permute-done.19.refs_16_), channel_id=1, source_target_pairs={{8,0},{16,8},{24,16},{32,24},{40,32},{48,40},{56,48},{0,56},{72,64... | collective-permute-start | bytes 1769480 | tf_op jit(solution)/shard_map/ring_second/ppermute | solution.py:93
  138.3 3.6 %collective-permute-start.13 = (bf16[256,1152]{1,0:T(8,128)(2,1)}, bf16[256,1152]{1,0:T(8,128)(2,1)}, u32[]{:S(2)}, u32[]{:S(2)}) collective-permute-start(bf16[256,1152]{1,0:T(8,128)(2,1)} %collective-permute-done.12.refs_8_), channel_id=1, source_target_pairs={{64,0},{128,64},{192,128},{256,192},{320,256},{384,320},{448,384},... | collective-permute-start | bytes 1769480 | tf_op jit(solution)/shard_map/ring_first/ppermute | solution.py:93
  146.8 5.9 %all-to-all-start.1 = ((bf16[8,16,2048]{2,1,0:T(8,128)(2,1)}), bf16[8,16,2048]{2,1,0:T(8,128)(2,1)S(1)}, u32[]{:S(2)}, u32[]{:S(2)}) async-start(bf16[8,16,2048]{2,1,0:T(8,128)(2,1)} %broadcast_in_dim.15), calls=%async_computation.1 | async-start | bytes 1048576 | tf_op jit(solution)/shard_map/all_to_all | solution.py:25
  152.8 9.3 %all-to-all-done.1 = bf16[8,16,2048]{2,1,0:T(8,128)(2,1)S(1)} async-done(((bf16[8,16,2048]{2,1,0:T(8,128)(2,1)}), bf16[8,16,2048]{2,1,0:T(8,128)(2,1)S(1)}, u32[]{:S(2)}, u32[]{:S(2)}) %all-to-all-start.1) | async-done | bytes 524320 | tf_op jit(solution)/shard_map/all_to_all | solution.py:25
  162.1 5.8 %ffn.1 = bf16[128,2048]{1,0:T(8,128)(2,1)S(1)} custom-call(s32[16]{0:T(128)S(1)} %pad_add_fusion.refs_0_, bf16[128,2048]{1,0:T(8,128)(2,1)S(1)} %bitcast.16, bf16[256,1152]{1,0:T(8,128)(2,1)S(1)} %bitcast.15, bf16[256,1152]{1,0:T(8,128)(2,1)} %collective-permute-done.7.refs_3_, bf16[256,1152]{1,0:T(8,128)(2,1)} %collective-permute-done.8.refs_4_, ...), custom_call_target="tpu_custom_call" | custom-call | tf_op jit(solution)/shard_map/ffn/pallas_call | solution.py:139
  167.9 14.1 %all_to_all.26 = bf16[8,16,2048]{2,1,0:T(8,128)(2,1)S(1)} all-to-all(bf16[8,16,2048]{2,1,0:T(8,128)(2,1)S(1)} %bitcast.17), channel_id=1, replica_groups=mesh['sp'=64,'tp'=8] {'tp'}, dimensions={0} | all-to-all | bytes 1048576 | tf_op jit(solution)/shard_map/all_to_all | solution.py:19
  (64 shorter events, 25.5 us)
Async XLA Ops:
  30.1 23.7 %all-to-all-start.2 = ((bf16[8,32,1152]{2,1,0:T(8,128)(2,1)}), bf16[8,32,1152]{2,1,0:T(8,128)(2,1)S(1)}, u32[]{:S(2)}, u32[]{:S(2)}) async-start(bf16[8,32,1152]{2,1,0:T(8,128)(2,1)} %broadcast_in_dim.16), calls=%async_computation.2 | async-start | bytes 1179648 | tf_op jit(solution)/shard_map/spread_first/all_to_all | solution.py:100
  37.0 58.5 %collective-permute-start.14 = (bf16[256,1152]{1,0:T(8,128)(2,1)S(1)}, bf16[256,1152]{1,0:T(8,128)(2,1)S(1)}, u32[]{:S(2)}, u32[]{:S(2)}) collective-permute-start(bf16[256,1152]{1,0:T(8,128)(2,1)S(1)} %bitcast.10), channel_id=1, source_target_pairs={{0,8},{8,16},{16,24},{24,32},{32,40},{40,48},{48,56},{56,0},{64,72... | collective-permute-start | bytes 1769480 | tf_op jit(solution)/shard_map/ring_second/ppermute | solution.py:91
  53.8 45.1 %collective-permute-start.7 = (bf16[256,1152]{1,0:T(8,128)(2,1)S(1)}, bf16[256,1152]{1,0:T(8,128)(2,1)}, u32[]{:S(2)}, u32[]{:S(2)}) collective-permute-start(bf16[256,1152]{1,0:T(8,128)(2,1)S(1)} %bitcast.13), channel_id=1, source_target_pairs={{0,64},{64,128},{128,192},{192,256},{256,320},{320,384},{384,448},... | collective-permute-start | bytes 1769480 | tf_op jit(solution)/shard_map/ring_first/ppermute | solution.py:91
  55.8 8.1 %collective-permute-start.6 = (bf16[144,512]{1,0:T(8,128)(2,1)S(1)}, bf16[144,512]{1,0:T(8,128)(2,1)S(1)}, u32[]{:S(2)}, u32[]{:S(2)}) collective-permute-start(bf16[144,512]{1,0:T(8,128)(2,1)S(1)} %fusion.1.refs_2_), channel_id=1, source_target_pairs={{0,56},{8,64},{16,72},{24,80},{32,88},{40,96},{48,104},{56,112},{6... | collective-permute-start | bytes 442376 | tf_op jit(solution)/shard_map/kv_near/ppermute | solution.py:13
  57.7 12.6 %collective-permute-start.4 = (bf16[144,512]{1,0:T(8,128)(2,1)S(1)}, bf16[144,512]{1,0:T(8,128)(2,1)S(1)}, u32[]{:S(2)}, u32[]{:S(2)}) collective-permute-start(bf16[144,512]{1,0:T(8,128)(2,1)S(1)} %fusion.1.refs_2_), channel_id=1, source_target_pairs={{0,48},{8,56},{16,64},{24,72},{32,80},{40,88},{48,96},{56,104},{64... | collective-permute-start | bytes 442376 | tf_op jit(solution)/shard_map/kv_near/ppermute | solution.py:13
  59.7 12.8 %collective-permute-start.1 = (bf16[144,512]{1,0:T(8,128)(2,1)S(1)}, bf16[144,512]{1,0:T(8,128)(2,1)S(1)}, u32[]{:S(2)}, u32[]{:S(2)}) collective-permute-start(bf16[144,512]{1,0:T(8,128)(2,1)S(1)} %fusion.1.refs_2_), channel_id=1, source_target_pairs={{0,16},{8,24},{16,32},{24,40},{32,48},{40,56},{48,64},{56,72},{64,... | collective-permute-start | bytes 442376 | tf_op jit(solution)/shard_map/kv_near/ppermute | solution.py:13
  63.9 10.6 %collective-permute-start = (bf16[144,512]{1,0:T(8,128)(2,1)S(1)}, bf16[144,512]{1,0:T(8,128)(2,1)S(1)}, u32[]{:S(2)}, u32[]{:S(2)}) collective-permute-start(bf16[144,512]{1,0:T(8,128)(2,1)S(1)} %fusion.1.refs_2_), channel_id=1, source_target_pairs={{0,8},{8,16},{16,24},{24,32},{32,40},{40,48},{48,56},{56,64},{64,7... | collective-permute-start | bytes 442376 | tf_op jit(solution)/shard_map/kv_near/ppermute | solution.py:13
  70.3 7.6 %collective-permute-start.5 = (bf16[144,512]{1,0:T(8,128)(2,1)S(1)}, bf16[144,512]{1,0:T(8,128)(2,1)S(1)}, u32[]{:S(2)}, u32[]{:S(2)}) collective-permute-start(bf16[144,512]{1,0:T(8,128)(2,1)S(1)} %collective-permute-done.4.refs_8_), channel_id=1, source_target_pairs={{0,504},{8,0},{16,8},{24,16},{32,24},{40,32},{48,40},{56,48},{64,5... | collective-permute-start | bytes 442376 | tf_op jit(solution)/shard_map/kv_far/ppermute | solution.py:13
  72.5 10.3 %collective-permute-start.3 = (bf16[144,512]{1,0:T(8,128)(2,1)S(1)}, bf16[144,512]{1,0:T(8,128)(2,1)S(1)}, u32[]{:S(2)}, u32[]{:S(2)}) collective-permute-start(bf16[144,512]{1,0:T(8,128)(2,1)S(1)} %collective-permute-done.1.refs_4_), channel_id=1, source_target_pairs={{0,16},{8,24},{16,32},{24,40},{32,48},{40,56},{48,64},{56,72},{64,... | collective-permute-start | bytes 442376 | tf_op jit(solution)/shard_map/kv_far/ppermute | solution.py:13
  74.5 11.9 %collective-permute-start.2 = (bf16[144,512]{1,0:T(8,128)(2,1)S(1)}, bf16[144,512]{1,0:T(8,128)(2,1)S(1)}, u32[]{:S(2)}, u32[]{:S(2)}) collective-permute-start(bf16[144,512]{1,0:T(8,128)(2,1)S(1)} %collective-permute-done.1.refs_4_), channel_id=1, source_target_pairs={{0,8},{8,16},{16,24},{24,32},{32,40},{40,48},{48,56},{56,64},{64,7... | collective-permute-start | bytes 442376 | tf_op jit(solution)/shard_map/kv_far/ppermute | solution.py:13
  91.7 25.4 %collective-permute-start.18 = (bf16[256,1152]{1,0:T(8,128)(2,1)S(1)}, bf16[256,1152]{1,0:T(8,128)(2,1)}, u32[]{:S(2)}, u32[]{:S(2)}) collective-permute-start(bf16[256,1152]{1,0:T(8,128)(2,1)S(1)} %bitcast.11), channel_id=1, source_target_pairs={{8,0},{16,8},{24,16},{32,24},{40,32},{48,40},{56,48},{0,56},{72,64... | collective-permute-start | bytes 1769480 | tf_op jit(solution)/shard_map/ring_second/ppermute | solution.py:93
  93.6 26.5 %collective-permute-start.11 = (bf16[256,1152]{1,0:T(8,128)(2,1)S(1)}, bf16[256,1152]{1,0:T(8,128)(2,1)}, u32[]{:S(2)}, u32[]{:S(2)}) collective-permute-start(bf16[256,1152]{1,0:T(8,128)(2,1)S(1)} %bitcast.14), channel_id=1, source_target_pairs={{64,0},{128,64},{192,128},{256,192},{320,256},{384,320},{448,384},... | collective-permute-start | bytes 1769480 | tf_op jit(solution)/shard_map/ring_first/ppermute | solution.py:93
  95.5 28.1 %collective-permute-start.15 = (bf16[256,1152]{1,0:T(8,128)(2,1)S(1)}, bf16[256,1152]{1,0:T(8,128)(2,1)}, u32[]{:S(2)}, u32[]{:S(2)}) collective-permute-start(bf16[256,1152]{1,0:T(8,128)(2,1)S(1)} %collective-permute-done.14.refs_11_), channel_id=1, source_target_pairs={{0,8},{8,16},{16,24},{24,32},{32,40},{40,48},{48,56},{56,0},{64,72... | collective-permute-start | bytes 1769480 | tf_op jit(solution)/shard_map/ring_second/ppermute | solution.py:91
  98.9 26.7 %collective-permute-start.8 = (bf16[256,1152]{1,0:T(8,128)(2,1)}, bf16[256,1152]{1,0:T(8,128)(2,1)}, u32[]{:S(2)}, u32[]{:S(2)}) collective-permute-start(bf16[256,1152]{1,0:T(8,128)(2,1)} %collective-permute-done.7.refs_3_), channel_id=1, source_target_pairs={{0,64},{64,128},{128,192},{192,256},{256,320},{320,384},{384,448},... | collective-permute-start | bytes 1769480 | tf_op jit(solution)/shard_map/ring_first/ppermute | solution.py:91
  103.4 24.4 %all-to-all-start = ((bf16[8,16,2048]{2,1,0:T(8,128)(2,1)}), bf16[8,16,2048]{2,1,0:T(8,128)(2,1)S(1)}, u32[]{:S(2)}, u32[]{:S(2)}) async-start(bf16[8,16,2048]{2,1,0:T(8,128)(2,1)} %bitcast.1), calls=%async_computation | async-start | bytes 1048576 | tf_op jit(solution)/shard_map/all_to_all | solution.py:19
  117.1 17.2 %collective-permute-start.19 = (bf16[256,1152]{1,0:T(8,128)(2,1)}, bf16[256,1152]{1,0:T(8,128)(2,1)}, u32[]{:S(2)}, u32[]{:S(2)}) collective-permute-start(bf16[256,1152]{1,0:T(8,128)(2,1)} %collective-permute-done.18.refs_17_), channel_id=1, source_target_pairs={{8,0},{16,8},{24,16},{32,24},{40,32},{48,40},{56,48},{0,56},{72,64... | collective-permute-start | bytes 1769480 | tf_op jit(solution)/shard_map/ring_second/ppermute | solution.py:93
  120.1 18.3 %collective-permute-start.12 = (bf16[256,1152]{1,0:T(8,128)(2,1)}, bf16[256,1152]{1,0:T(8,128)(2,1)}, u32[]{:S(2)}, u32[]{:S(2)}) collective-permute-start(bf16[256,1152]{1,0:T(8,128)(2,1)} %collective-permute-done.11.refs_9_), channel_id=1, source_target_pairs={{64,0},{128,64},{192,128},{256,192},{320,256},{384,320},{448,384},... | collective-permute-start | bytes 1769480 | tf_op jit(solution)/shard_map/ring_first/ppermute | solution.py:93
  123.7 18.3 %collective-permute-start.16 = (bf16[256,1152]{1,0:T(8,128)(2,1)}, bf16[256,1152]{1,0:T(8,128)(2,1)}, u32[]{:S(2)}, u32[]{:S(2)}) collective-permute-start(bf16[256,1152]{1,0:T(8,128)(2,1)} %collective-permute-done.15.refs_12_), channel_id=1, source_target_pairs={{0,8},{8,16},{16,24},{24,32},{32,40},{40,48},{48,56},{56,0},{64,72... | collective-permute-start | bytes 1769480 | tf_op jit(solution)/shard_map/ring_second/ppermute | solution.py:91
  125.6 18.3 %collective-permute-start.9 = (bf16[256,1152]{1,0:T(8,128)(2,1)}, bf16[256,1152]{1,0:T(8,128)(2,1)}, u32[]{:S(2)}, u32[]{:S(2)}) collective-permute-start(bf16[256,1152]{1,0:T(8,128)(2,1)} %collective-permute-done.8.refs_4_), channel_id=1, source_target_pairs={{0,64},{64,128},{128,192},{192,256},{256,320},{320,384},{384,448},... | collective-permute-start | bytes 1769480 | tf_op jit(solution)/shard_map/ring_first/ppermute | solution.py:91
  134.3 27.8 %collective-permute-start.20 = (bf16[256,1152]{1,0:T(8,128)(2,1)}, bf16[256,1152]{1,0:T(8,128)(2,1)}, u32[]{:S(2)}, u32[]{:S(2)}) collective-permute-start(bf16[256,1152]{1,0:T(8,128)(2,1)} %collective-permute-done.19.refs_16_), channel_id=1, source_target_pairs={{8,0},{16,8},{24,16},{32,24},{40,32},{48,40},{56,48},{0,56},{72,64... | collective-permute-start | bytes 1769480 | tf_op jit(solution)/shard_map/ring_second/ppermute | solution.py:93
  138.3 23.7 %collective-permute-start.13 = (bf16[256,1152]{1,0:T(8,128)(2,1)}, bf16[256,1152]{1,0:T(8,128)(2,1)}, u32[]{:S(2)}, u32[]{:S(2)}) collective-permute-start(bf16[256,1152]{1,0:T(8,128)(2,1)} %collective-permute-done.12.refs_8_), channel_id=1, source_target_pairs={{64,0},{128,64},{192,128},{256,192},{320,256},{384,320},{448,384},... | collective-permute-start | bytes 1769480 | tf_op jit(solution)/shard_map/ring_first/ppermute | solution.py:93
  142.0 20.1 %collective-permute-start.17 = (bf16[256,1152]{1,0:T(8,128)(2,1)}, bf16[256,1152]{1,0:T(8,128)(2,1)}, u32[]{:S(2)}, u32[]{:S(2)}) collective-permute-start(bf16[256,1152]{1,0:T(8,128)(2,1)} %collective-permute-done.16.refs_13_), channel_id=1, source_target_pairs={{0,8},{8,16},{16,24},{24,32},{32,40},{40,48},{48,56},{56,0},{64,72... | collective-permute-start | bytes 1769480 | tf_op jit(solution)/shard_map/ring_second/ppermute | solution.py:91
  143.9 18.2 %collective-permute-start.10 = (bf16[256,1152]{1,0:T(8,128)(2,1)}, bf16[256,1152]{1,0:T(8,128)(2,1)}, u32[]{:S(2)}, u32[]{:S(2)}) collective-permute-start(bf16[256,1152]{1,0:T(8,128)(2,1)} %collective-permute-done.9.refs_5_), channel_id=1, source_target_pairs={{0,64},{64,128},{128,192},{192,256},{256,320},{320,384},{384,448},... | collective-permute-start | bytes 1769480 | tf_op jit(solution)/shard_map/ring_first/ppermute | solution.py:91
  146.8 15.2 %all-to-all-start.1 = ((bf16[8,16,2048]{2,1,0:T(8,128)(2,1)}), bf16[8,16,2048]{2,1,0:T(8,128)(2,1)S(1)}, u32[]{:S(2)}, u32[]{:S(2)}) async-start(bf16[8,16,2048]{2,1,0:T(8,128)(2,1)} %broadcast_in_dim.15), calls=%async_computation.1 | async-start | bytes 1048576 | tf_op jit(solution)/shard_map/all_to_all | solution.py:25
  (10 other events, 264.1 us)

commit v4 on v3

--- a/solution.py
+++ b/solution.py
@@ -85,52 +85,81 @@
     )(offsets, queries, *blocks)
 
 
-def around(block, pairs, steps):
-    got = {0: block}
-    for back in range(1, steps // 2 + 1):
-        got[back] = lax.ppermute(got[back - 1], "sp", pairs)
-        if steps - back > steps // 2:
-            got[steps - back] = lax.ppermute(
-                got[(steps - back + 1) % steps], "sp", [(j, i) for i, j in pairs]
-            )
-    return [got[k] for k in range(steps)]
-
-
-def spread(copies, groups):
-    tiles = lax.all_to_all(copies, "sp", 0, 0, tiled=True, axis_index_groups=groups)
-    return tiles.reshape(copies.shape[0] * copies.shape[1], copies.shape[2])
+def turned(groups, by):
+    return [(g[i], g[(i + by) % len(g)]) for g in groups for i in range(len(g))]
+
+
+def neighbours(shard, groups):
+    after = lax.ppermute(shard, "sp", turned(groups, -1))
+    before = lax.ppermute(shard, "sp", turned(groups, 1))
+    middle = lax.ppermute(jnp.concatenate([before, shard, after]), "sp", turned(groups, -3))
+    late = lax.ppermute(jnp.concatenate([shard, after]), "sp", turned(groups, 3))
+    return jnp.concatenate([shard, after, middle, late, before])
+
+
+def around(block, groups):
+    up, down = turned(groups, 1), turned(groups, -1)
+    half = block.shape[0] // 2
+    got = {0: block, 8: block}
+    for k in range(1, 4):
+        got[k] = lax.ppermute(got[k - 1], "sp", up)
+        got[8 - k] = lax.ppermute(got[9 - k], "sp", down)
+    far = (lax.ppermute(got[3][:half], "sp", up), lax.ppermute(got[5][half:], "sp", down))
+    return [got[0], got[1], got[2], got[3], *far, got[5], got[6], got[7]]
 
 
 def ffn_kernel(ring, low, places, x, *refs):
-    first, second, (out, x_turned) = refs[:ring], refs[ring : 2 * ring], refs[2 * ring :]
+    first, second = refs[: ring + 1], refs[ring + 1 : 2 * ring + 2]
+    out, x_first, x_second = refs[2 * ring + 2 :]
     step = first[0].shape[0]
+    half = step // 2
+    wide = step // ring
     high = first[0].shape[1] - (second[0].shape[1] - low)
-
-    def part(rows, i):
-        return rows[:, pl.ds(pl.multiple_of(places[i] * step, step), step)]
-
-    wide = step // ring
-    for y in range(ring):
-        x_turned[:, y * step : (y + 1) * step] = jnp.concatenate(
-            [x[:, z * step + y * wide : z * step + (y + 1) * wide] for z in range(ring)], axis=1
-        )
+    z, y = places[0], places[ring]
+    for i in range(ring):
+        cols = slice(i * step, (i + 1) * step)
+        own = x[:, cols].astype(jnp.float32)
+        x_first[:, cols] = pltpu.roll(own, (step - y * wide) & (step - 1), 1).astype(jnp.bfloat16)
+        across = jnp.concatenate(
+            [x[:, k * step + i * wide : k * step + (i + 1) * wide] for k in range(ring)], axis=1
+        ).astype(jnp.float32)
+        x_second[:, cols] = pltpu.roll(across, (step - z * wide) & (step - 1), 1).astype(jnp.bfloat16)
+
+    def pieces(blocks):
+        far = ring // 2
+        for k in range(ring):
+            if k == far:
+                yield k, 0, blocks[far]
+                yield k, half, blocks[far + 1]
+            else:
+                yield k, 0, blocks[k if k < far else k + 1]
+
+    def part(rows, i, offset, count):
+        return rows[:, pl.ds(pl.multiple_of(places[i] * step + offset, half), count)]
+
     gate_high = low_up = None
-    for k in range(ring):
-        one = jnp.dot(part(x, k), first[k][:, :high], preferred_element_type=jnp.float32)
-        two = jnp.dot(part(x_turned, ring + k), second[k][...], preferred_element_type=jnp.float32)
-        gate_high = one if k == 0 else gate_high + one
-        low_up = two if k == 0 else low_up + two
+    for k, offset, block in pieces(first):
+        rows = part(x_first, k, offset, block.shape[0])
+        one = jnp.dot(rows, block[:, :high], preferred_element_type=jnp.float32)
+        gate_high = one if gate_high is None else gate_high + one
+    for k, offset, block in pieces(second):
+        rows = part(x_second, ring + k, offset, block.shape[0])
+        two = jnp.dot(rows, block[...], preferred_element_type=jnp.float32)
+        low_up = two if low_up is None else low_up + two
     gate = jnp.concatenate([low_up[:, :low], gate_high], axis=1)
     hidden = (gate / (1.0 + jnp.exp(-gate)) * low_up[:, low:]).astype(jnp.bfloat16)
+    terms = {}
+    for k, offset, block in pieces(first):
+        term = lax.dot_general(
+            hidden, block[:, high:], (((1,), (1,)), ((), ())), preferred_element_type=jnp.float32
+        )
+        terms[k] = term if offset == 0 else jnp.concatenate([terms[k], term], axis=1)
     for k in range(ring):
-        term = lax.dot_general(
-            hidden, first[k][:, high:], (((1,), (1,)), ((), ())), preferred_element_type=jnp.float32
-        )
-        out[:, pl.ds(pl.multiple_of(places[k] * step, step), step)] = term.astype(jnp.bfloat16)
-
-
-def ffn(x, first, second, places, low):
-    ring = len(first)
+        straight = pltpu.roll(terms[k], y * wide, 1)
+        out[:, pl.ds(pl.multiple_of(places[k] * step, step), step)] = straight.astype(jnp.bfloat16)
+
+
+def ffn(x, first, second, places, ring, low):
     vmem = pl.BlockSpec(memory_space=pltpu.VMEM)
 
     def body(*refs):
@@ -139,9 +168,9 @@
     return pl.pallas_call(
         body,
         out_shape=jax.ShapeDtypeStruct(x.shape, jnp.bfloat16),
-        in_specs=[pl.BlockSpec(memory_space=pltpu.SMEM)] + [vmem] * (1 + 2 * ring),
+        in_specs=[pl.BlockSpec(memory_space=pltpu.SMEM)] + [vmem] * (3 + 2 * ring),
         out_specs=vmem,
-        scratch_shapes=[pltpu.VMEM(x.shape, jnp.bfloat16)],
+        scratch_shapes=[pltpu.VMEM(x.shape, jnp.bfloat16)] * 2,
         compiler_params=pltpu.CompilerParams(vmem_limit_bytes=24 << 20),
         name="ffn",
     )(places, x, *first, *second)
@@ -168,21 +197,16 @@
     rings = spans // ring
     along_y = [[z * ring + y for y in range(ring)] for z in range(rings)]
     along_z = [[z * ring + y for z in range(rings)] for y in range(ring)]
-    next_y = [(g[i], g[(i + 1) % ring]) for g in along_y for i in range(ring)]
-    next_z = [(g[i], g[(i + 1) % rings]) for g in along_z for i in range(rings)]
     first = jnp.concatenate([gate_weight[:, low:], down_weight.T], axis=1)
     second = jnp.concatenate([gate_weight[:, :low], up_weight], axis=1)
-    first = jnp.broadcast_to(first, (ring, *first.shape))
-    second = jnp.broadcast_to(second, (rings, *second.shape))
-    first, second = lax.optimization_barrier((first, second))
     with jax.named_scope("spread_first"):
-        first = spread(first, along_y)
+        first = neighbours(first, along_y)
     with jax.named_scope("spread_second"):
-        second = spread(second, along_z)
+        second = neighbours(second, along_z)
     with jax.named_scope("ring_first"):
-        first = around(first, next_z, rings)
+        first = around(first, along_z)
     with jax.named_scope("ring_second"):
-        second = around(second, next_y, ring)
+        second = around(second, along_y)
     at = lax.axis_index("sp")
     back = jnp.arange(ring, dtype=jnp.int32)
     places = jnp.concatenate(
@@ -206,7 +230,7 @@
         stream * lax.rsqrt(jnp.mean(stream * stream, axis=1, keepdims=True) + 1e-06) * norm_gain
     ).astype(jnp.bfloat16)
     x = from_everyone(normed).reshape(rows, -1)
-    feed = summed_for_owner(ffn(x, first, second, places, low))
+    feed = summed_for_owner(ffn(x, first, second, places, ring, low))
     return (stream + feed).astype(jnp.bfloat16)
 
 

time: 184 us -> 220 us (1.20); the launches traced: 183 us -> 217 us
  starting transfers between devices: 83.3 us -> 132 us
  blocking collectives: 42.3 us -> 15 us
  local copies, waits for them, and re-layouts: 2.76 us -> 10.1 us
  other arithmetic: 1.14 us -> 3.9 us
  waiting for transfers between devices: 40.6 us -> 42.9 us
    ppermute x14 -> x24, starting transfers between devices: 38.2 us -> 81.1 us  [the longest x6 24.8 us: around(): got[8 - k] = lax.ppermute(got[9 - k], 'sp', down)]
    ppermute x14 -> x24, waiting for transfers between devices: 6.23 us -> 42.9 us  [the longest x2 13.8 us: neighbours(): lax.ppermute(jnp.concatenate([before, shard, after]), 'sp', turned(groups...]
    all_to_all x1 -> x0, blocking collectives: 28.2 us -> none  [spread(): lax.all_to_all(copies, 'sp', 0, 0, tiled=True, axis_index_groups=groups)]
    ppermute x7, starting transfers between devices: 18.6 us -> 38.5 us  [shifted(): lax.ppermute(block, 'sp', [(i, (i + by) % spans) for i in range(spans)])]
    all_to_all x1 -> x0, waiting for transfers between devices: 13.2 us -> none  [spread(): lax.all_to_all(copies, 'sp', 0, 0, tiled=True, axis_index_groups=groups)]
    ppermute x7, waiting for transfers between devices: 11.9 us -> 0.02 us  [shifted(): lax.ppermute(block, 'sp', [(i, (i + by) % spans) for i in range(spans)])]
    all_to_all x1, waiting for transfers between devices: 9.27 us -> 0.01 us  [from_everyone(): return lax.all_to_all(copies, 'tp', split_axis=0, concat_axis=0, tiled=True)]
    all_to_all x1, starting transfers between devices: 13.7 us -> 6.63 us  [summed_for_owner(): tiles = lax.all_to_all(tiles, 'tp', 0, 0, tiled=True)]
  transfers between devices with their start and end apart: 24 -> 33, of which waited for: 7 -> 11; matrix products, arithmetic and copies ran while one was open for 1% -> 4% of each run, Pallas kernels for 3% -> 2%
where the time goes in v4:
time: 220 us; the launch traced here: 217 us
  starting transfers between devices  132 us (60%)
  waiting for transfers between devices  42.9 us (20%)
  blocking collectives  15 us (7%)
  Pallas kernels  10.8 us (5%)
  local copies, waits for them, and re-layouts  10.1 us (5%)
  other arithmetic  3.9 us (2%)
    ppermute x7, starting transfers between devices, shifted(): lax.ppermute(block, 'sp', [(i, (i + by) % spans) for i in range(spans)])  38.5 us
    ppermute x6, starting transfers between devices, around(): got[8 - k] = lax.ppermute(got[9 - k], 'sp', down)  24.8 us
    all_to_all x1, blocking collectives, summed_for_owner(): tiles = lax.all_to_all(tiles, 'tp', 0, 0, tiled=True)  15 us
    ppermute x2, waiting for transfers between devices, neighbours(): lax.ppermute(jnp.concatenate([before, shard, after]), 'sp', turned(groups...  13.8 us
    ppermute x6, starting transfers between devices, around(): got[k] = lax.ppermute(got[k - 1], 'sp', up)  13 us
    ppermute x2, starting transfers between devices, neighbours(): after = lax.ppermute(shard, 'sp', turned(groups, -1))  10.4 us
    ppermute x2, starting transfers between devices, neighbours(): lax.ppermute(jnp.concatenate([before, shard, after]), 'sp', turned(groups...  9.67 us
    ppermute x2, starting transfers between devices, around(): lax.ppermute(got[5][half:], 'sp', down)  9.4 us
  transfers between devices with their start and end apart: 33, of which 11 were waited for; matrix products, arithmetic and copies ran while one was open for 4% of the time, Pallas kernels for 2%

profile of v4, /device:TPU:1, one launch (start us, length us, event | category | flops | bytes accessed | tf_op | source)
XLA Modules:
  0.0 216.5 jit_solution(2694478916178822841)
XLA Ops:
  1.7 6.0 %collective-permute-start.6 = (bf16[144,512]{1,0:T(8,128)(2,1)S(1)}, bf16[144,512]{1,0:T(8,128)(2,1)S(1)}, u32[]{:S(2)}, u32[]{:S(2)}) collective-permute-start(bf16[144,512]{1,0:T(8,128)(2,1)S(1)} %fusion.1.refs_2_), channel_id=1, source_target_pairs={{0,56},{8,64},{16,72},{24,80},{32,88},{40,96},{48,104},{56,112},{6... | collective-permute-start | bytes 442376 | tf_op jit(solution)/shard_map/kv_near/ppermute | solution.py:13
  7.7 5.6 %collective-permute-start.4 = (bf16[144,512]{1,0:T(8,128)(2,1)S(1)}, bf16[144,512]{1,0:T(8,128)(2,1)S(1)}, u32[]{:S(2)}, u32[]{:S(2)}) collective-permute-start(bf16[144,512]{1,0:T(8,128)(2,1)S(1)} %fusion.1.refs_2_), channel_id=1, source_target_pairs={{0,48},{8,56},{16,64},{24,72},{32,80},{40,88},{48,96},{56,104},{64... | collective-permute-start | bytes 442376 | tf_op jit(solution)/shard_map/kv_near/ppermute | solution.py:13
  15.8 7.3 %collective-permute-start.19 = (bf16[32,1152]{1,0:T(8,128)(2,1)S(1)}, bf16[32,1152]{1,0:T(8,128)(2,1)S(1)}, u32[]{:S(2)}, u32[]{:S(2)}) collective-permute-start(bf16[32,1152]{1,0:T(8,128)(2,1)S(1)} %get-tuple-element.5), channel_id=1, source_target_pairs={{0,448},{64,0},{128,64},{192,128},{256,192},{320,256},{384,320},{4... | collective-permute-start | bytes 221192 | tf_op jit(solution)/shard_map/spread_second/ppermute | solution.py:93
  37.1 4.0 %collective-permute-done.8 = bf16[32,1152]{1,0:T(8,128)(2,1)S(1)} collective-permute-done((bf16[32,1152]{1,0:T(8,128)(2,1)S(1)}, bf16[32,1152]{1,0:T(8,128)(2,1)S(1)}, u32[]{:S(2)}, u32[]{:S(2)}) %collective-permute-start.8) | collective-permute-done | bytes 73760 | tf_op jit(solution)/shard_map/spread_first/ppermute | solution.py:94
  41.2 6.0 %collective-permute-start.21 = (bf16[96,1152]{1,0:T(8,128)(2,1)S(1)}, bf16[96,1152]{1,0:T(8,128)(2,1)S(1)}, u32[]{:S(2)}, u32[]{:S(2)}) collective-permute-start(bf16[96,1152]{1,0:T(8,128)(2,1)S(1)} %pad_maximum_fusion.1), channel_id=1, source_target_pairs={{0,320},{64,384},{128,448},{192,0},{256,64},{320,128},{384,192},{4... | collective-permute-start | bytes 663560 | tf_op jit(solution)/shard_map/spread_second/ppermute | solution.py:95
  47.2 8.4 %collective-permute-done.21 = bf16[96,1152]{1,0:T(8,128)(2,1)S(1)} collective-permute-done((bf16[96,1152]{1,0:T(8,128)(2,1)S(1)}, bf16[96,1152]{1,0:T(8,128)(2,1)S(1)}, u32[]{:S(2)}, u32[]{:S(2)}) %collective-permute-start.21) | collective-permute-done | bytes 221216 | tf_op jit(solution)/shard_map/spread_second/ppermute | solution.py:95
  58.1 8.8 %collective-permute-done.22 = bf16[64,1152]{1,0:T(8,128)(2,1)S(1)} collective-permute-done((bf16[64,1152]{1,0:T(8,128)(2,1)S(1)}, bf16[64,1152]{1,0:T(8,128)(2,1)S(1)}, u32[]{:S(2)}, u32[]{:S(2)}) %collective-permute-start.22) | collective-permute-done | bytes 147488 | tf_op jit(solution)/shard_map/spread_second/ppermute | solution.py:96
  67.0 3.7 %collective-permute-start.9 = (bf16[96,1152]{1,0:T(8,128)(2,1)S(1)}, bf16[96,1152]{1,0:T(8,128)(2,1)S(1)}, u32[]{:S(2)}, u32[]{:S(2)}) collective-permute-start(bf16[96,1152]{1,0:T(8,128)(2,1)S(1)} %pad_maximum_fusion), channel_id=1, source_target_pairs={{0,40},{8,48},{16,56},{24,0},{32,8},{40,16},{48,24},{56,32},{64,10... | collective-permute-start | bytes 663560 | tf_op jit(solution)/shard_map/spread_first/ppermute | solution.py:95
  74.1 5.4 %collective-permute-done.9 = bf16[96,1152]{1,0:T(8,128)(2,1)S(1)} collective-permute-done((bf16[96,1152]{1,0:T(8,128)(2,1)S(1)}, bf16[96,1152]{1,0:T(8,128)(2,1)S(1)}, u32[]{:S(2)}, u32[]{:S(2)}) %collective-permute-start.9) | collective-permute-done | bytes 221216 | tf_op jit(solution)/shard_map/spread_first/ppermute | solution.py:95
  79.5 4.1 %collective-permute-start.3 = (bf16[144,512]{1,0:T(8,128)(2,1)S(1)}, bf16[144,512]{1,0:T(8,128)(2,1)S(1)}, u32[]{:S(2)}, u32[]{:S(2)}) collective-permute-start(bf16[144,512]{1,0:T(8,128)(2,1)S(1)} %collective-permute-done.1.refs_4_), channel_id=1, source_target_pairs={{0,16},{8,24},{16,32},{24,40},{32,48},{40,56},{48,64},{56,72},{64,... | collective-permute-start | bytes 442376 | tf_op jit(solution)/shard_map/kv_far/ppermute | solution.py:13
  85.6 16.1 %collective-permute-start.5 = (bf16[144,512]{1,0:T(8,128)(2,1)S(1)}, bf16[144,512]{1,0:T(8,128)(2,1)S(1)}, u32[]{:S(2)}, u32[]{:S(2)}) collective-permute-start(bf16[144,512]{1,0:T(8,128)(2,1)S(1)} %collective-permute-done.4.refs_8_), channel_id=1, source_target_pairs={{0,504},{8,0},{16,8},{24,16},{32,24},{40,32},{48,40},{56,48},{64,5... | collective-permute-start | bytes 442376 | tf_op jit(solution)/shard_map/kv_far/ppermute | solution.py:13
  107.1 3.7 %collective-permute-start.15 = (bf16[256,1152]{1,0:T(8,128)(2,1)S(1)}, bf16[256,1152]{1,0:T(8,128)(2,1)}, u32[]{:S(2)}, u32[]{:S(2)}) collective-permute-start(bf16[256,1152]{1,0:T(8,128)(2,1)S(1)} %constant_dynamic-update-slice_fusion.refs_2_), channel_id=1, source_target_pairs={{0,448},{64,0},{128,64},{192,128},{256,192},{320,256},{384,320},{4... | collective-permute-start | bytes 1769480 | tf_op jit(solution)/shard_map/ring_first/ppermute | solution.py:106
  112.8 5.3 %attention.1 = bf16[128,256]{1,0:T(8,128)(2,1)S(1)} custom-call(f32[4]{0:T(128)S(1)} %copy-done.10, bf16[128,256]{1,0:T(8,128)(2,1)S(1)} %copy-done.9, bf16[144,512]{1,0:T(8,128)(2,1)S(1)} %fusion.1.refs_2_, bf16[144,512]{1,0:T(8,128)(2,1)S(1)} %collective-permute-done.refs_3_, bf16[144,512]{1,0:T(8,128)(2,1)S(1)} %collective-permute-done.1.refs_4_, ...), custom_call_target="tpu_custom_call" | custom-call | tf_op jit(solution)/shard_map/attention/pallas_call | solution.py:78
  119.3 6.6 %all-to-all-start = ((bf16[8,16,2048]{2,1,0:T(8,128)(2,1)}), bf16[8,16,2048]{2,1,0:T(8,128)(2,1)}, u32[]{:S(2)}, u32[]{:S(2)}) async-start(bf16[8,16,2048]{2,1,0:T(8,128)(2,1)} %bitcast.10), calls=%async_computation | async-start | bytes 1048576 | tf_op jit(solution)/shard_map/all_to_all | solution.py:19
  125.9 4.0 %collective-permute-start.28 = (bf16[256,1152]{1,0:T(8,128)(2,1)S(1)}, bf16[256,1152]{1,0:T(8,128)(2,1)}, u32[]{:S(2)}, u32[]{:S(2)}) collective-permute-start(bf16[256,1152]{1,0:T(8,128)(2,1)S(1)} %collective-permute-done.27.refs_19_), channel_id=1, source_target_pairs={{0,56},{8,0},{16,8},{24,16},{32,24},{40,32},{48,40},{56,48},{64,12... | collective-permute-start | bytes 1769480 | tf_op jit(solution)/shard_map/ring_second/ppermute | solution.py:106
  132.7 4.8 %collective-permute-start.16 = (bf16[256,1152]{1,0:T(8,128)(2,1)}, bf16[256,1152]{1,0:T(8,128)(2,1)}, u32[]{:S(2)}, u32[]{:S(2)}) collective-permute-start(bf16[256,1152]{1,0:T(8,128)(2,1)} %collective-permute-done.15.refs_10_), channel_id=1, source_target_pairs={{0,448},{64,0},{128,64},{192,128},{256,192},{320,256},{384,320},{4... | collective-permute-start | bytes 1769480 | tf_op jit(solution)/shard_map/ring_first/ppermute | solution.py:106
  143.0 5.1 %collective-permute-start.29 = (bf16[256,1152]{1,0:T(8,128)(2,1)}, bf16[256,1152]{1,0:T(8,128)(2,1)S(1)}, u32[]{:S(2)}, u32[]{:S(2)}) collective-permute-start(bf16[256,1152]{1,0:T(8,128)(2,1)} %collective-permute-done.28.refs_18_), channel_id=1, source_target_pairs={{0,56},{8,0},{16,8},{24,16},{32,24},{40,32},{48,40},{56,48},{64,12... | collective-permute-start | bytes 1769480 | tf_op jit(solution)/shard_map/ring_second/ppermute | solution.py:106
  150.4 5.3 %collective-permute-start.17 = (bf16[256,1152]{1,0:T(8,128)(2,1)}, bf16[256,1152]{1,0:T(8,128)(2,1)S(1)}, u32[]{:S(2)}, u32[]{:S(2)}) collective-permute-start(bf16[256,1152]{1,0:T(8,128)(2,1)} %collective-permute-done.16.refs_9_), channel_id=1, source_target_pairs={{0,448},{64,0},{128,64},{192,128},{256,192},{320,256},{384,320},{4... | collective-permute-start | bytes 1769480 | tf_op jit(solution)/shard_map/ring_first/ppermute | solution.py:106
  158.6 5.7 %all-to-all-start.1 = ((bf16[8,16,2048]{2,1,0:T(8,128)(2,1)}), bf16[8,16,2048]{2,1,0:T(8,128)(2,1)S(1)}, u32[]{:S(2)}, u32[]{:S(2)}) async-start(bf16[8,16,2048]{2,1,0:T(8,128)(2,1)} %broadcast_in_dim.9), calls=%async_computation.1 | async-start | bytes 1048576 | tf_op jit(solution)/shard_map/all_to_all | solution.py:25
  165.0 4.6 %collective-permute-start.30 = (bf16[128,1152]{1,0:T(8,128)(2,1)}, bf16[128,1152]{1,0:T(8,128)(2,1)}, u32[]{:S(2)}, u32[]{:S(2)}) collective-permute-start(bf16[128,1152]{1,0:T(8,128)(2,1)} %slice.27), channel_id=1, source_target_pairs={{0,56},{8,0},{16,8},{24,16},{32,24},{40,32},{48,40},{56,48},{64,12... | collective-permute-start | bytes 884744 | tf_op jit(solution)/shard_map/ring_second/ppermute | solution.py:107
  173.0 4.8 %collective-permute-start.18 = (bf16[128,1152]{1,0:T(8,128)(2,1)}, bf16[128,1152]{1,0:T(8,128)(2,1)}, u32[]{:S(2)}, u32[]{:S(2)}) collective-permute-start(bf16[128,1152]{1,0:T(8,128)(2,1)} %slice.25), channel_id=1, source_target_pairs={{0,448},{64,0},{128,64},{192,128},{256,192},{320,256},{384,320},{4... | collective-permute-start | bytes 884744 | tf_op jit(solution)/shard_map/ring_first/ppermute | solution.py:107
  184.3 6.8 %collective-permute-done.14.refs_6_ = bf16[128,1152]{1,0:T(8,128)(2,1)} collective-permute-done((bf16[128,1152]{1,0:T(8,128)(2,1)}, bf16[128,1152]{1,0:T(8,128)(2,1)}, u32[]{:S(2)}, u32[]{:S(2)}) %collective-permute-start.14) | collective-permute-done | bytes 294944 | tf_op jit(solution)/shard_map/ring_first/ppermute | solution.py:107
  195.3 5.5 %ffn.1 = bf16[128,2048]{1,0:T(8,128)(2,1)S(1)} custom-call(s32[16]{0:T(128)S(1)} %pad_add_fusion.refs_0_, bf16[128,2048]{1,0:T(8,128)(2,1)S(1)} %bitcast.8, bf16[256,1152]{1,0:T(8,128)(2,1)S(1)} %copy-done.2, bf16[256,1152]{1,0:T(8,128)(2,1)} %collective-permute-done.11.refs_3_, bf16[256,1152]{1,0:T(8,128)(2,1)} %collective-permute-done.12.refs_4_, ...), custom_call_target="tpu_custom_call" | custom-call | tf_op jit(solution)/shard_map/ffn/pallas_call | solution.py:168
  200.8 15.0 %all_to_all.15 = bf16[8,16,2048]{2,1,0:T(8,128)(2,1)S(1)} all-to-all(bf16[8,16,2048]{2,1,0:T(8,128)(2,1)S(1)} %bitcast.9), channel_id=1, replica_groups=mesh['sp'=64,'tp'=8] {'tp'}, dimensions={0} | all-to-all | bytes 1048576 | tf_op jit(solution)/shard_map/all_to_all | solution.py:19
  (108 shorter events, 63.2 us)
Async XLA Ops:
  1.7 100.2 %collective-permute-start.6 = (bf16[144,512]{1,0:T(8,128)(2,1)S(1)}, bf16[144,512]{1,0:T(8,128)(2,1)S(1)}, u32[]{:S(2)}, u32[]{:S(2)}) collective-permute-start(bf16[144,512]{1,0:T(8,128)(2,1)S(1)} %fusion.1.refs_2_), channel_id=1, source_target_pairs={{0,56},{8,64},{16,72},{24,80},{32,88},{40,96},{48,104},{56,112},{6... | collective-permute-start | bytes 442376 | tf_op jit(solution)/shard_map/kv_near/ppermute | solution.py:13
  7.7 75.9 %collective-permute-start.4 = (bf16[144,512]{1,0:T(8,128)(2,1)S(1)}, bf16[144,512]{1,0:T(8,128)(2,1)S(1)}, u32[]{:S(2)}, u32[]{:S(2)}) collective-permute-start(bf16[144,512]{1,0:T(8,128)(2,1)S(1)} %fusion.1.refs_2_), channel_id=1, source_target_pairs={{0,48},{8,56},{16,64},{24,72},{32,80},{40,88},{48,96},{56,104},{64... | collective-permute-start | bytes 442376 | tf_op jit(solution)/shard_map/kv_near/ppermute | solution.py:13
  13.3 57.4 %collective-permute-start.1 = (bf16[144,512]{1,0:T(8,128)(2,1)S(1)}, bf16[144,512]{1,0:T(8,128)(2,1)S(1)}, u32[]{:S(2)}, u32[]{:S(2)}) collective-permute-start(bf16[144,512]{1,0:T(8,128)(2,1)S(1)} %fusion.1.refs_2_), channel_id=1, source_target_pairs={{0,16},{8,24},{16,32},{24,40},{32,48},{40,56},{48,64},{56,72},{64,... | collective-permute-start | bytes 442376 | tf_op jit(solution)/shard_map/kv_near/ppermute | solution.py:13
  25.1 78.7 %collective-permute-start = (bf16[144,512]{1,0:T(8,128)(2,1)S(1)}, bf16[144,512]{1,0:T(8,128)(2,1)S(1)}, u32[]{:S(2)}, u32[]{:S(2)}) collective-permute-start(bf16[144,512]{1,0:T(8,128)(2,1)S(1)} %fusion.1.refs_2_), channel_id=1, source_target_pairs={{0,8},{8,16},{16,24},{24,32},{32,40},{40,48},{48,56},{56,64},{64,7... | collective-permute-start | bytes 442376 | tf_op jit(solution)/shard_map/kv_near/ppermute | solution.py:13
  41.2 14.4 %collective-permute-start.21 = (bf16[96,1152]{1,0:T(8,128)(2,1)S(1)}, bf16[96,1152]{1,0:T(8,128)(2,1)S(1)}, u32[]{:S(2)}, u32[]{:S(2)}) collective-permute-start(bf16[96,1152]{1,0:T(8,128)(2,1)S(1)} %pad_maximum_fusion.1), channel_id=1, source_target_pairs={{0,320},{64,384},{128,448},{192,0},{256,64},{320,128},{384,192},{4... | collective-permute-start | bytes 663560 | tf_op jit(solution)/shard_map/spread_second/ppermute | solution.py:95
  70.7 14.9 %collective-permute-start.10 = (bf16[64,1152]{1,0:T(8,128)(2,1)S(1)}, bf16[64,1152]{1,0:T(8,128)(2,1)S(1)}, u32[]{:S(2)}, u32[]{:S(2)}) collective-permute-start(bf16[64,1152]{1,0:T(8,128)(2,1)S(1)} %pad_maximum_fusion.2), channel_id=1, source_target_pairs={{0,24},{8,32},{16,40},{24,48},{32,56},{40,0},{48,8},{56,16},{64,88... | collective-permute-start | bytes 442376 | tf_op jit(solution)/shard_map/spread_first/ppermute | solution.py:96
  79.5 31.4 %collective-permute-start.3 = (bf16[144,512]{1,0:T(8,128)(2,1)S(1)}, bf16[144,512]{1,0:T(8,128)(2,1)S(1)}, u32[]{:S(2)}, u32[]{:S(2)}) collective-permute-start(bf16[144,512]{1,0:T(8,128)(2,1)S(1)} %collective-permute-done.1.refs_4_), channel_id=1, source_target_pairs={{0,16},{8,24},{16,32},{24,40},{32,48},{40,56},{48,64},{56,72},{64,... | collective-permute-start | bytes 442376 | tf_op jit(solution)/shard_map/kv_far/ppermute | solution.py:13
  83.7 29.1 %collective-permute-start.2 = (bf16[144,512]{1,0:T(8,128)(2,1)S(1)}, bf16[144,512]{1,0:T(8,128)(2,1)S(1)}, u32[]{:S(2)}, u32[]{:S(2)}) collective-permute-start(bf16[144,512]{1,0:T(8,128)(2,1)S(1)} %collective-permute-done.1.refs_4_), channel_id=1, source_target_pairs={{0,8},{8,16},{16,24},{24,32},{32,40},{40,48},{48,56},{56,64},{64,7... | collective-permute-start | bytes 442376 | tf_op jit(solution)/shard_map/kv_far/ppermute | solution.py:13
  85.6 21.5 %collective-permute-start.5 = (bf16[144,512]{1,0:T(8,128)(2,1)S(1)}, bf16[144,512]{1,0:T(8,128)(2,1)S(1)}, u32[]{:S(2)}, u32[]{:S(2)}) collective-permute-start(bf16[144,512]{1,0:T(8,128)(2,1)S(1)} %collective-permute-done.4.refs_8_), channel_id=1, source_target_pairs={{0,504},{8,0},{16,8},{24,16},{32,24},{40,32},{48,40},{56,48},{64,5... | collective-permute-start | bytes 442376 | tf_op jit(solution)/shard_map/kv_far/ppermute | solution.py:13
  101.8 24.1 %collective-permute-start.27 = (bf16[256,1152]{1,0:T(8,128)(2,1)S(1)}, bf16[256,1152]{1,0:T(8,128)(2,1)S(1)}, u32[]{:S(2)}, u32[]{:S(2)}) collective-permute-start(bf16[256,1152]{1,0:T(8,128)(2,1)S(1)} %constant_dynamic-update-slice_fusion.5.refs_11_), channel_id=1, source_target_pairs={{0,56},{8,0},{16,8},{24,16},{32,24},{40,32},{48,40},{56,48},{64,12... | collective-permute-start | bytes 1769480 | tf_op jit(solution)/shard_map/ring_second/ppermute | solution.py:106
  103.8 26.2 %collective-permute-start.23 = (bf16[256,1152]{1,0:T(8,128)(2,1)S(1)}, bf16[256,1152]{1,0:T(8,128)(2,1)S(1)}, u32[]{:S(2)}, u32[]{:S(2)}) collective-permute-start(bf16[256,1152]{1,0:T(8,128)(2,1)S(1)} %constant_dynamic-update-slice_fusion.5.refs_11_), channel_id=1, source_target_pairs={{0,8},{8,16},{16,24},{24,32},{32,40},{40,48},{48,56},{56,0},{64,72... | collective-permute-start | bytes 1769480 | tf_op jit(solution)/shard_map/ring_second/ppermute | solution.py:105
  107.1 25.6 %collective-permute-start.15 = (bf16[256,1152]{1,0:T(8,128)(2,1)S(1)}, bf16[256,1152]{1,0:T(8,128)(2,1)}, u32[]{:S(2)}, u32[]{:S(2)}) collective-permute-start(bf16[256,1152]{1,0:T(8,128)(2,1)S(1)} %constant_dynamic-update-slice_fusion.refs_2_), channel_id=1, source_target_pairs={{0,448},{64,0},{128,64},{192,128},{256,192},{320,256},{384,320},{4... | collective-permute-start | bytes 1769480 | tf_op jit(solution)/shard_map/ring_first/ppermute | solution.py:106
  110.8 26.7 %collective-permute-start.11 = (bf16[256,1152]{1,0:T(8,128)(2,1)S(1)}, bf16[256,1152]{1,0:T(8,128)(2,1)}, u32[]{:S(2)}, u32[]{:S(2)}) collective-permute-start(bf16[256,1152]{1,0:T(8,128)(2,1)S(1)} %constant_dynamic-update-slice_fusion.refs_2_), channel_id=1, source_target_pairs={{0,64},{64,128},{128,192},{192,256},{256,320},{320,384},{384,448},... | collective-permute-start | bytes 1769480 | tf_op jit(solution)/shard_map/ring_first/ppermute | solution.py:105
  119.3 20.2 %all-to-all-start = ((bf16[8,16,2048]{2,1,0:T(8,128)(2,1)}), bf16[8,16,2048]{2,1,0:T(8,128)(2,1)}, u32[]{:S(2)}, u32[]{:S(2)}) async-start(bf16[8,16,2048]{2,1,0:T(8,128)(2,1)} %bitcast.10), calls=%async_computation | async-start | bytes 1048576 | tf_op jit(solution)/shard_map/all_to_all | solution.py:19
  125.9 17.1 %collective-permute-start.28 = (bf16[256,1152]{1,0:T(8,128)(2,1)S(1)}, bf16[256,1152]{1,0:T(8,128)(2,1)}, u32[]{:S(2)}, u32[]{:S(2)}) collective-permute-start(bf16[256,1152]{1,0:T(8,128)(2,1)S(1)} %collective-permute-done.27.refs_19_), channel_id=1, source_target_pairs={{0,56},{8,0},{16,8},{24,16},{32,24},{40,32},{48,40},{56,48},{64,12... | collective-permute-start | bytes 1769480 | tf_op jit(solution)/shard_map/ring_second/ppermute | solution.py:106
  129.9 18.2 %collective-permute-start.24 = (bf16[256,1152]{1,0:T(8,128)(2,1)S(1)}, bf16[256,1152]{1,0:T(8,128)(2,1)}, u32[]{:S(2)}, u32[]{:S(2)}) collective-permute-start(bf16[256,1152]{1,0:T(8,128)(2,1)S(1)} %collective-permute-done.23.refs_12_), channel_id=1, source_target_pairs={{0,8},{8,16},{16,24},{24,32},{32,40},{40,48},{48,56},{56,0},{64,72... | collective-permute-start | bytes 1769480 | tf_op jit(solution)/shard_map/ring_second/ppermute | solution.py:105
  132.7 17.7 %collective-permute-start.16 = (bf16[256,1152]{1,0:T(8,128)(2,1)}, bf16[256,1152]{1,0:T(8,128)(2,1)}, u32[]{:S(2)}, u32[]{:S(2)}) collective-permute-start(bf16[256,1152]{1,0:T(8,128)(2,1)} %collective-permute-done.15.refs_10_), channel_id=1, source_target_pairs={{0,448},{64,0},{128,64},{192,128},{256,192},{320,256},{384,320},{4... | collective-permute-start | bytes 1769480 | tf_op jit(solution)/shard_map/ring_first/ppermute | solution.py:106
  137.6 18.1 %collective-permute-start.12 = (bf16[256,1152]{1,0:T(8,128)(2,1)}, bf16[256,1152]{1,0:T(8,128)(2,1)}, u32[]{:S(2)}, u32[]{:S(2)}) collective-permute-start(bf16[256,1152]{1,0:T(8,128)(2,1)} %collective-permute-done.11.refs_3_), channel_id=1, source_target_pairs={{0,64},{64,128},{128,192},{192,256},{256,320},{320,384},{384,448},... | collective-permute-start | bytes 1769480 | tf_op jit(solution)/shard_map/ring_first/ppermute | solution.py:105
  143.0 21.2 %collective-permute-start.29 = (bf16[256,1152]{1,0:T(8,128)(2,1)}, bf16[256,1152]{1,0:T(8,128)(2,1)S(1)}, u32[]{:S(2)}, u32[]{:S(2)}) collective-permute-start(bf16[256,1152]{1,0:T(8,128)(2,1)} %collective-permute-done.28.refs_18_), channel_id=1, source_target_pairs={{0,56},{8,0},{16,8},{24,16},{32,24},{40,32},{48,40},{56,48},{64,12... | collective-permute-start | bytes 1769480 | tf_op jit(solution)/shard_map/ring_second/ppermute | solution.py:106
  148.1 21.5 %collective-permute-start.25 = (bf16[256,1152]{1,0:T(8,128)(2,1)}, bf16[256,1152]{1,0:T(8,128)(2,1)S(1)}, u32[]{:S(2)}, u32[]{:S(2)}) collective-permute-start(bf16[256,1152]{1,0:T(8,128)(2,1)} %collective-permute-done.24.refs_13_), channel_id=1, source_target_pairs={{0,8},{8,16},{16,24},{24,32},{32,40},{40,48},{48,56},{56,0},{64,72... | collective-permute-start | bytes 1769480 | tf_op jit(solution)/shard_map/ring_second/ppermute | solution.py:105
  150.4 21.9 %collective-permute-start.17 = (bf16[256,1152]{1,0:T(8,128)(2,1)}, bf16[256,1152]{1,0:T(8,128)(2,1)S(1)}, u32[]{:S(2)}, u32[]{:S(2)}) collective-permute-start(bf16[256,1152]{1,0:T(8,128)(2,1)} %collective-permute-done.16.refs_9_), channel_id=1, source_target_pairs={{0,448},{64,0},{128,64},{192,128},{256,192},{320,256},{384,320},{4... | collective-permute-start | bytes 1769480 | tf_op jit(solution)/shard_map/ring_first/ppermute | solution.py:106
  155.7 22.2 %collective-permute-start.13 = (bf16[256,1152]{1,0:T(8,128)(2,1)}, bf16[256,1152]{1,0:T(8,128)(2,1)}, u32[]{:S(2)}, u32[]{:S(2)}) collective-permute-start(bf16[256,1152]{1,0:T(8,128)(2,1)} %collective-permute-done.12.refs_4_), channel_id=1, source_target_pairs={{0,64},{64,128},{128,192},{192,256},{256,320},{320,384},{384,448},... | collective-permute-start | bytes 1769480 | tf_op jit(solution)/shard_map/ring_first/ppermute | solution.py:105
  158.6 23.1 %all-to-all-start.1 = ((bf16[8,16,2048]{2,1,0:T(8,128)(2,1)}), bf16[8,16,2048]{2,1,0:T(8,128)(2,1)S(1)}, u32[]{:S(2)}, u32[]{:S(2)}) async-start(bf16[8,16,2048]{2,1,0:T(8,128)(2,1)} %broadcast_in_dim.9), calls=%async_computation.1 | async-start | bytes 1048576 | tf_op jit(solution)/shard_map/all_to_all | solution.py:25
  165.0 16.6 %collective-permute-start.30 = (bf16[128,1152]{1,0:T(8,128)(2,1)}, bf16[128,1152]{1,0:T(8,128)(2,1)}, u32[]{:S(2)}, u32[]{:S(2)}) collective-permute-start(bf16[128,1152]{1,0:T(8,128)(2,1)} %slice.27), channel_id=1, source_target_pairs={{0,56},{8,0},{16,8},{24,16},{32,24},{40,32},{48,40},{56,48},{64,12... | collective-permute-start | bytes 884744 | tf_op jit(solution)/shard_map/ring_second/ppermute | solution.py:107
  (25 other events, 373.9 us)

commit v5 on v1

--- a/solution.py
+++ b/solution.py
@@ -78,8 +78,58 @@
         out_shape=jax.ShapeDtypeStruct((rows, width), jnp.bfloat16),
         in_specs=[pl.BlockSpec(memory_space=pltpu.SMEM)] + [vmem] * (1 + len(blocks)),
         out_specs=vmem,
+        compiler_params=pltpu.CompilerParams(vmem_limit_bytes=12 << 20),
         name="attention",
     )(offsets, queries, *blocks)
+
+
+def ffn_kernel(cuts, x, weights, out, gate_up, down, sems):
+    units = down.shape[1]
+    copies = [
+        pltpu.make_async_copy(
+            weights.at[pl.ds(a, b - a), pl.ds(0, 2 * units)], gate_up.at[pl.ds(a, b - a)], sems.at[i]
+        )
+        for i, (a, b) in enumerate(cuts)
+    ]
+    copies.append(
+        pltpu.make_async_copy(weights.at[:, pl.ds(2 * units, units)], down, sems.at[len(cuts)])
+    )
+    copies[0].start()
+    acc = None
+    for i, (a, b) in enumerate(cuts):
+        copies[i].wait()
+        copies[i + 1].start()
+        term = jnp.dot(x[:, a:b], gate_up[a:b, :], preferred_element_type=jnp.float32)
+        acc = term if acc is None else acc + term
+    gate, upper = acc[:, :units], acc[:, units:]
+    hidden = (gate / (1.0 + jnp.exp(-gate)) * upper).astype(jnp.bfloat16)
+    copies[-1].wait()
+    out[...] = lax.dot_general(
+        hidden, down[...], (((1,), (1,)), ((), ())), preferred_element_type=jnp.float32
+    ).astype(jnp.bfloat16)
+
+
+def ffn(x, weights, units):
+    width = weights.shape[0]
+    cuts = ((0, 3 * width // 8), (3 * width // 8, width))
+    vmem = pl.BlockSpec(memory_space=pltpu.VMEM)
+
+    def body(*refs):
+        ffn_kernel(cuts, *refs)
+
+    return pl.pallas_call(
+        body,
+        out_shape=jax.ShapeDtypeStruct(x.shape, jnp.bfloat16),
+        in_specs=[vmem, pl.BlockSpec(memory_space=pltpu.HBM)],
+        out_specs=vmem,
+        scratch_shapes=[
+            pltpu.VMEM((width, 2 * units), jnp.bfloat16),
+            pltpu.VMEM((width, units), jnp.bfloat16),
+            pltpu.SemaphoreType.DMA((len(cuts) + 1,)),
+        ],
+        compiler_params=pltpu.CompilerParams(vmem_limit_bytes=48 << 20),
+        name="ffn",
+    )(x, weights)
 
 
 def on_device(
@@ -102,12 +152,9 @@
 
     docs = jnp.pad(doc_ids.astype(jnp.bfloat16)[None], ((0, 15), (0, 2 * keys.shape[1] - rows)))
     own = jnp.concatenate([jnp.concatenate([keys, values], axis=1), docs], axis=0)
-    blocks = {0: own}
-    blocks[7] = shifted(own, 7)
-    for back in range(1, 5):
-        blocks[back] = shifted(blocks[back - 1], 1)
-        if back < 3:
-            blocks[7 - back] = shifted(blocks[8 - back], -1)
+    near = {k: shifted(own, k) for k in (2, 6, 1, 7)}
+    far = {4: shifted(near[2], 2), 3: shifted(near[2], 1), 5: shifted(near[6], -1)}
+    blocks = {0: own, **near, **far}
     attended = attention(queries, [blocks[b] for b in range(8)], score_offset)
 
     mixed_attn = summed_for_owner(
@@ -118,16 +165,7 @@
         stream * lax.rsqrt(jnp.mean(stream * stream, axis=1, keepdims=True) + 1e-06) * norm_gain
     ).astype(jnp.bfloat16)
     span_rows = from_everyone(normed).reshape(rows, -1)
-    gate = jnp.dot(span_rows, weights[:, :units], preferred_element_type=jnp.float32)
-    upper = jnp.dot(span_rows, weights[:, units : 2 * units], preferred_element_type=jnp.float32)
-    hidden = (jax.nn.silu(gate) * upper).astype(jnp.bfloat16)
-    partial_out = lax.dot_general(
-        hidden,
-        weights[:, 2 * units :],
-        (((1,), (1,)), ((), ())),
-        preferred_element_type=jnp.float32,
-    )
-    feed = summed_for_owner(partial_out.astype(jnp.bfloat16))
+    feed = summed_for_owner(ffn(span_rows, weights, units))
     return (stream + feed).astype(jnp.bfloat16)
 
 

time: 150 us -> 153 us (1.020)
  matrix products: 8.13 us -> 0.31 us
  Pallas kernels: 6.72 us -> 12.1 us
  waiting for transfers between devices: 39 us -> 44 us
  starting transfers between devices: 28.3 us -> 30.4 us
  blocking collectives: 46.5 us -> 44.5 us
    all_gather x1, waiting for transfers between devices: 20 us -> 38.5 us  [on_device(): weights = lax.all_gather(packed, 'sp', axis=0, tiled=True)]
    ppermute x7, waiting for transfers between devices: 19 us -> 5.53 us  [shifted(): lax.ppermute(block, 'sp', [(i, (i + by) % spans) for i in range(spans)])]
    dot_general x2 -> x0, matrix products: 6.98 us -> none  [the longest x1 4.52 us: on_device(): lax.dot_general(hidden, weights[:, 2 * units:], (((1,), (1,)), ((), ())),...]
    pallas_call x0 -> x1, Pallas kernels: none -> 6.83 us  [ffn(): pl.pallas_call(body, out_shape=jax.ShapeDtypeStruct(x.shape, jnp.bfloat16...]
    ppermute x7, starting transfers between devices: 28.3 us -> 30.4 us  [shifted(): lax.ppermute(block, 'sp', [(i, (i + by) % spans) for i in range(spans)])]
    all_to_all x2, blocking collectives: 33.7 us -> 31.7 us  [summed_for_owner(): tiles = lax.all_to_all(tiles, 'tp', 0, 0, tiled=True)]
  transfers between devices with their start and end apart: 8 -> 8, of which waited for: 5 -> 5; matrix products, arithmetic and copies ran while one was open for 3% -> 3% of each run, Pallas kernels for 5% -> 3%
where the time goes in v5:
time: 153 us; the launch traced here: 152 us
  blocking collectives  44.5 us (29%)
  waiting for transfers between devices  44 us (29%)
  starting transfers between devices  30.4 us (20%)
  between operations  13.5 us (9%)
  Pallas kernels  12.1 us (8%)
  other arithmetic  5.9 us (4%)
  local copies, waits for them, and re-layouts  1.55 us (1%)
    all_gather x1, waiting for transfers between devices, on_device(): weights = lax.all_gather(packed, 'sp', axis=0, tiled=True)  38.5 us
    all_to_all x2, blocking collectives, summed_for_owner(): tiles = lax.all_to_all(tiles, 'tp', 0, 0, tiled=True)  31.7 us
    ppermute x7, starting transfers between devices, shifted(): lax.ppermute(block, 'sp', [(i, (i + by) % spans) for i in range(spans)])  30.4 us
    all_to_all x1, blocking collectives, from_everyone(): return lax.all_to_all(copies, 'tp', split_axis=0, concat_axis=0, tiled=True)  12.8 us
    pallas_call x1, Pallas kernels, ffn(): pl.pallas_call(body, out_shape=jax.ShapeDtypeStruct(x.shape, jnp.bfloat16...  6.83 us
    ppermute x7, waiting for transfers between devices, shifted(): lax.ppermute(block, 'sp', [(i, (i + by) % spans) for i in range(spans)])  5.53 us
    pallas_call x1, Pallas kernels, attention(): pl.pallas_call(body, out_shape=jax.ShapeDtypeStruct((rows, width), jnp.bf...  5.3 us
  transfers between devices with their start and end apart: 8, of which 5 were waited for; matrix products, arithmetic and copies ran while one was open for 3% of the time, Pallas kernels for 3%

profile of v5, /device:TPU:1, one launch (start us, length us, event | category | flops | bytes accessed | tf_op | source)
XLA Modules:
  0.0 152.4 jit_solution(4365245696827606805)
XLA Ops:
  6.5 1.6 %pad_maximum_fusion = bf16[32,2304]{1,0:T(8,128)(2,1)} fusion(bf16[32,768]{1,0:T(8,128)(2,1)} %bitcast.11, bf16[32,768]{1,0:T(8,128)(2,1)} %param.20, bf16[32,768]{1,0:T(8,128)(2,1)} %param.19), kind=kLoop, calls=%fused_computation.6 | loop fusion | flops 442368 | bytes 294912 | tf_op jit(solution)/shard_map/concatenate | solution.py:150
  8.2 0.7 convert_bitcast_fusion
  8.8 0.9 fusion.1.refs_2_
  9.7 5.0 %collective-permute-start.1 = (bf16[144,512]{1,0:T(8,128)(2,1)S(1)}, bf16[144,512]{1,0:T(8,128)(2,1)S(1)}, u32[]{:S(2)}, u32[]{:S(2)}) collective-permute-start(bf16[144,512]{1,0:T(8,128)(2,1)S(1)} %fusion.1.refs_2_), channel_id=1, source_target_pairs={{0,16},{8,24},{16,32},{24,40},{32,48},{40,56},{48,64},{56,72},{64,... | collective-permute-start | bytes 442376 | tf_op jit(solution)/shard_map/ppermute | solution.py:11
  14.8 5.0 %collective-permute-start.4 = (bf16[144,512]{1,0:T(8,128)(2,1)S(1)}, bf16[144,512]{1,0:T(8,128)(2,1)S(1)}, u32[]{:S(2)}, u32[]{:S(2)}) collective-permute-start(bf16[144,512]{1,0:T(8,128)(2,1)S(1)} %fusion.1.refs_2_), channel_id=1, source_target_pairs={{0,48},{8,56},{16,64},{24,72},{32,80},{40,88},{48,96},{56,104},{64... | collective-permute-start | bytes 442376 | tf_op jit(solution)/shard_map/ppermute | solution.py:11
  19.8 3.2 %collective-permute-start = (bf16[144,512]{1,0:T(8,128)(2,1)S(1)}, bf16[144,512]{1,0:T(8,128)(2,1)S(1)}, u32[]{:S(2)}, u32[]{:S(2)}) collective-permute-start(bf16[144,512]{1,0:T(8,128)(2,1)S(1)} %fusion.1.refs_2_), channel_id=1, source_target_pairs={{0,8},{8,16},{16,24},{24,32},{32,40},{40,48},{48,56},{56,64},{64,7... | collective-permute-start | bytes 442376 | tf_op jit(solution)/shard_map/ppermute | solution.py:11
  23.0 5.1 %collective-permute-start.6 = (bf16[144,512]{1,0:T(8,128)(2,1)S(1)}, bf16[144,512]{1,0:T(8,128)(2,1)S(1)}, u32[]{:S(2)}, u32[]{:S(2)}) collective-permute-start(bf16[144,512]{1,0:T(8,128)(2,1)S(1)} %fusion.1.refs_2_), channel_id=1, source_target_pairs={{0,56},{8,64},{16,72},{24,80},{32,88},{40,96},{48,104},{56,112},{6... | collective-permute-start | bytes 442376 | tf_op jit(solution)/shard_map/ppermute | solution.py:11
  28.1 1.3 collective-permute-done.1.refs_4_
  29.4 4.8 %collective-permute-start.2 = (bf16[144,512]{1,0:T(8,128)(2,1)S(1)}, bf16[144,512]{1,0:T(8,128)(2,1)S(1)}, u32[]{:S(2)}, u32[]{:S(2)}) collective-permute-start(bf16[144,512]{1,0:T(8,128)(2,1)S(1)} %collective-permute-done.1.refs_4_), channel_id=1, source_target_pairs={{0,8},{8,16},{16,24},{24,32},{32,40},{40,48},{48,56},{56,64},{64,7... | collective-permute-start | bytes 442376 | tf_op jit(solution)/shard_map/ppermute | solution.py:11
  34.2 1.9 %collective-permute-start.3 = (bf16[144,512]{1,0:T(8,128)(2,1)S(1)}, bf16[144,512]{1,0:T(8,128)(2,1)S(1)}, u32[]{:S(2)}, u32[]{:S(2)}) collective-permute-start(bf16[144,512]{1,0:T(8,128)(2,1)S(1)} %collective-permute-done.1.refs_4_), channel_id=1, source_target_pairs={{0,16},{8,24},{16,32},{24,40},{32,48},{40,56},{48,64},{56,72},{64,... | collective-permute-start | bytes 442376 | tf_op jit(solution)/shard_map/ppermute | solution.py:11
  36.2 1.1 collective-permute-done.4.refs_8_
  37.2 5.4 %collective-permute-start.5 = (bf16[144,512]{1,0:T(8,128)(2,1)S(1)}, bf16[144,512]{1,0:T(8,128)(2,1)S(1)}, u32[]{:S(2)}, u32[]{:S(2)}) collective-permute-start(bf16[144,512]{1,0:T(8,128)(2,1)S(1)} %collective-permute-done.4.refs_8_), channel_id=1, source_target_pairs={{0,504},{8,0},{16,8},{24,16},{32,24},{40,32},{48,40},{56,48},{64,5... | collective-permute-start | bytes 442376 | tf_op jit(solution)/shard_map/ppermute | solution.py:11
  42.6 0.9 collective-permute-done.6.refs_9_
  43.5 2.2 %collective-permute-done.3.refs_6_ = bf16[144,512]{1,0:T(8,128)(2,1)S(1)} collective-permute-done((bf16[144,512]{1,0:T(8,128)(2,1)S(1)}, bf16[144,512]{1,0:T(8,128)(2,1)S(1)}, u32[]{:S(2)}, u32[]{:S(2)}) %collective-permute-start.3) | collective-permute-done | bytes 147488 | tf_op jit(solution)/shard_map/ppermute | solution.py:11
  45.8 0.8 copy-done.1
  47.3 5.3 %attention.1 = bf16[128,256]{1,0:T(8,128)(2,1)S(1)} custom-call(f32[4]{0:T(128)S(1)} %copy-done.2, bf16[128,256]{1,0:T(8,128)(2,1)S(1)} %copy-done.1, bf16[144,512]{1,0:T(8,128)(2,1)S(1)} %fusion.1.refs_2_, bf16[144,512]{1,0:T(8,128)(2,1)S(1)} %collective-permute-done.refs_3_, bf16[144,512]{1,0:T(8,128)(2,1)S(1)} %collective-permute-done.1.refs_4_, ...), custom_call_target="tpu_custom_call" | custom-call | tf_op jit(solution)/shard_map/attention/pallas_call | solution.py:76
  52.9 17.5 %all_to_all.15 = bf16[8,16,2048]{2,1,0:T(8,128)(2,1)S(1)} all-to-all(bf16[8,16,2048]{2,1,0:T(8,128)(2,1)S(1)} %bitcast.10), channel_id=1, replica_groups=mesh['sp'=64,'tp'=8] {'tp'}, dimensions={0} | all-to-all | bytes 1048576 | tf_op jit(solution)/shard_map/all_to_all | solution.py:17
  70.5 1.0 multiply_reduce_fusion
  71.5 0.9 multiply_convert_fusion
  72.5 12.8 %all_to_all.16 = bf16[8,16,2048]{2,1,0:T(8,128)(2,1)S(1)} all-to-all(bf16[8,16,2048]{2,1,0:T(8,128)(2,1)S(1)} %broadcast_in_dim.9), channel_id=1, replica_groups=mesh['sp'=64,'tp'=8] {'tp'}, dimensions={0} | all-to-all | bytes 1048576 | tf_op jit(solution)/shard_map/all_to_all | solution.py:23
  85.3 38.5 %all-gather.2.cloned.1.call-done.refs_1_ = bf16[2048,2304]{1,0:T(8,128)(2,1)} async-done(((bf16[32,2304]{1,0:T(8,128)(2,1)}), bf16[2048,2304]{1,0:T(8,128)(2,1)}) %all-gather.2.cloned.1.call-update) | async-done | bytes 9437200 | tf_op jit(solution)/shard_map/all_gather | solution.py:151
  123.8 6.8 %ffn.1 = bf16[128,2048]{1,0:T(8,128)(2,1)S(1)} custom-call(bf16[128,2048]{1,0:T(8,128)(2,1)S(1)} %bitcast.8, bf16[2048,2304]{1,0:T(8,128)(2,1)} %all-gather.2.cloned.1.call-done.refs_1_), custom_call_target="tpu_custom_call" | custom-call | tf_op jit(solution)/shard_map/ffn/pallas_call | solution.py:120
  130.6 14.2 %all_to_all.17 = bf16[8,16,2048]{2,1,0:T(8,128)(2,1)S(1)} all-to-all(bf16[8,16,2048]{2,1,0:T(8,128)(2,1)S(1)} %bitcast.9), channel_id=1, replica_groups=mesh['sp'=64,'tp'=8] {'tp'}, dimensions={0} | all-to-all | bytes 1048576 | tf_op jit(solution)/shard_map/all_to_all | solution.py:17
  144.9 0.7 add_convert_fusion
  (17 shorter events, 1.2 us)
Async XLA Ops:
  6.5 46.1 %copy-start = (bf16[256,2048]{1,0:T(8,128)(2,1)S(1)}, bf16[256,2048]{1,0:T(8,128)(2,1)}, u32[]{:S(2)}) copy-start(bf16[256,2048]{1,0:T(8,128)(2,1)} %param.17) | copy-start | bytes 3145732
  6.5 117.2 %all-gather.2.cloned.1.call-start = ((), (), s32[]{:S(2)}) async-start(), calls=%async_computation.3 | async-start | bytes 9584640 | tf_op jit(solution)/shard_map/all_gather | solution.py:151
  8.8 136.1 %copy-start.3 = (bf16[16,2048]{1,0:T(8,128)(2,1)S(1)}, bf16[16,2048]{1,0:T(8,128)(2,1)}, u32[]{:S(2)}) copy-start(bf16[16,2048]{1,0:T(8,128)(2,1)} %param.11) | copy-start | bytes 196612
  9.7 19.7 %collective-permute-start.1 = (bf16[144,512]{1,0:T(8,128)(2,1)S(1)}, bf16[144,512]{1,0:T(8,128)(2,1)S(1)}, u32[]{:S(2)}, u32[]{:S(2)}) collective-permute-start(bf16[144,512]{1,0:T(8,128)(2,1)S(1)} %fusion.1.refs_2_), channel_id=1, source_target_pairs={{0,16},{8,24},{16,32},{24,40},{32,48},{40,56},{48,64},{56,72},{64,... | collective-permute-start | bytes 442376 | tf_op jit(solution)/shard_map/ppermute | solution.py:11
  14.8 22.5 %collective-permute-start.4 = (bf16[144,512]{1,0:T(8,128)(2,1)S(1)}, bf16[144,512]{1,0:T(8,128)(2,1)S(1)}, u32[]{:S(2)}, u32[]{:S(2)}) collective-permute-start(bf16[144,512]{1,0:T(8,128)(2,1)S(1)} %fusion.1.refs_2_), channel_id=1, source_target_pairs={{0,48},{8,56},{16,64},{24,72},{32,80},{40,88},{48,96},{56,104},{64... | collective-permute-start | bytes 442376 | tf_op jit(solution)/shard_map/ppermute | solution.py:11
  19.8 22.8 %collective-permute-start = (bf16[144,512]{1,0:T(8,128)(2,1)S(1)}, bf16[144,512]{1,0:T(8,128)(2,1)S(1)}, u32[]{:S(2)}, u32[]{:S(2)}) collective-permute-start(bf16[144,512]{1,0:T(8,128)(2,1)S(1)} %fusion.1.refs_2_), channel_id=1, source_target_pairs={{0,8},{8,16},{16,24},{24,32},{32,40},{40,48},{48,56},{56,64},{64,7... | collective-permute-start | bytes 442376 | tf_op jit(solution)/shard_map/ppermute | solution.py:11
  23.0 20.5 %collective-permute-start.6 = (bf16[144,512]{1,0:T(8,128)(2,1)S(1)}, bf16[144,512]{1,0:T(8,128)(2,1)S(1)}, u32[]{:S(2)}, u32[]{:S(2)}) collective-permute-start(bf16[144,512]{1,0:T(8,128)(2,1)S(1)} %fusion.1.refs_2_), channel_id=1, source_target_pairs={{0,56},{8,64},{16,72},{24,80},{32,88},{40,96},{48,104},{56,112},{6... | collective-permute-start | bytes 442376 | tf_op jit(solution)/shard_map/ppermute | solution.py:11
  29.4 14.1 %collective-permute-start.2 = (bf16[144,512]{1,0:T(8,128)(2,1)S(1)}, bf16[144,512]{1,0:T(8,128)(2,1)S(1)}, u32[]{:S(2)}, u32[]{:S(2)}) collective-permute-start(bf16[144,512]{1,0:T(8,128)(2,1)S(1)} %collective-permute-done.1.refs_4_), channel_id=1, source_target_pairs={{0,8},{8,16},{16,24},{24,32},{32,40},{40,48},{48,56},{56,64},{64,7... | collective-permute-start | bytes 442376 | tf_op jit(solution)/shard_map/ppermute | solution.py:11
  34.2 11.5 %collective-permute-start.3 = (bf16[144,512]{1,0:T(8,128)(2,1)S(1)}, bf16[144,512]{1,0:T(8,128)(2,1)S(1)}, u32[]{:S(2)}, u32[]{:S(2)}) collective-permute-start(bf16[144,512]{1,0:T(8,128)(2,1)S(1)} %collective-permute-done.1.refs_4_), channel_id=1, source_target_pairs={{0,16},{8,24},{16,32},{24,40},{32,48},{40,56},{48,64},{56,72},{64,... | collective-permute-start | bytes 442376 | tf_op jit(solution)/shard_map/ppermute | solution.py:11
  37.2 8.5 %collective-permute-start.5 = (bf16[144,512]{1,0:T(8,128)(2,1)S(1)}, bf16[144,512]{1,0:T(8,128)(2,1)S(1)}, u32[]{:S(2)}, u32[]{:S(2)}) collective-permute-start(bf16[144,512]{1,0:T(8,128)(2,1)S(1)} %collective-permute-done.4.refs_8_), channel_id=1, source_target_pairs={{0,504},{8,0},{16,8},{24,16},{32,24},{40,32},{48,40},{56,48},{64,5... | collective-permute-start | bytes 442376 | tf_op jit(solution)/shard_map/ppermute | solution.py:11
  45.8 0.8 copy-start.1
  46.6 0.7 copy-start.2
Sparse Core Ops, SparseCore 0:
  10.3 113.3 all-gather.1

commit v6 on v5

--- a/solution.py
+++ b/solution.py
@@ -83,39 +83,66 @@
     )(offsets, queries, *blocks)
 
 
-def ffn_kernel(cuts, x, weights, out, gate_up, down, sems):
+def ffn_kernel(cuts, ahead, x, weights, out, gate_up, down, sems):
     units = down.shape[1]
-    copies = [
-        pltpu.make_async_copy(
-            weights.at[pl.ds(a, b - a), pl.ds(0, 2 * units)], gate_up.at[pl.ds(a, b - a)], sems.at[i]
+    half = down.shape[0] // 2
+
+    def copy(source, target, sem):
+        return pltpu.make_async_copy(source, target, sem)
+
+    stages = []
+    for i, (a, b) in enumerate(cuts):
+        n = (b - a) // 2
+        stages.append(
+            [
+                copy(
+                    weights.at[pl.ds(at, n), pl.ds(0, 2 * units)],
+                    gate_up.at[pl.ds(at, n)],
+                    sems.at[2 * i + j],
+                )
+                for j, at in enumerate((a, a + n))
+            ]
         )
-        for i, (a, b) in enumerate(cuts)
-    ]
-    copies.append(
-        pltpu.make_async_copy(weights.at[:, pl.ds(2 * units, units)], down, sems.at[len(cuts)])
-    )
-    copies[0].start()
+    for j in range(2):
+        rows = pl.ds(j * half, half)
+        stages.append(
+            [copy(weights.at[rows, pl.ds(2 * units, units)], down.at[rows], sems.at[2 * len(cuts) + j])]
+        )
+
+    def start(i):
+        for one in stages[i] if i < len(stages) else ():
+            one.start()
+
+    def wait(i):
+        for one in stages[i]:
+            one.wait()
+        start(i + ahead)
+
+    for i in range(ahead):
+        start(i)
     acc = None
     for i, (a, b) in enumerate(cuts):
-        copies[i].wait()
-        copies[i + 1].start()
+        wait(i)
         term = jnp.dot(x[:, a:b], gate_up[a:b, :], preferred_element_type=jnp.float32)
         acc = term if acc is None else acc + term
     gate, upper = acc[:, :units], acc[:, units:]
     hidden = (gate / (1.0 + jnp.exp(-gate)) * upper).astype(jnp.bfloat16)
-    copies[-1].wait()
-    out[...] = lax.dot_general(
-        hidden, down[...], (((1,), (1,)), ((), ())), preferred_element_type=jnp.float32
-    ).astype(jnp.bfloat16)
+    for j in range(2):
+        wait(len(cuts) + j)
+        rows = slice(j * half, (j + 1) * half)
+        out[:, rows] = lax.dot_general(
+            hidden, down[rows, :], (((1,), (1,)), ((), ())), preferred_element_type=jnp.float32
+        ).astype(jnp.bfloat16)
 
 
 def ffn(x, weights, units):
     width = weights.shape[0]
-    cuts = ((0, 3 * width // 8), (3 * width // 8, width))
+    marks = (0, 3 * width // 8, 11 * width // 16, width)
+    cuts = tuple(zip(marks[:-1], marks[1:]))
     vmem = pl.BlockSpec(memory_space=pltpu.VMEM)
 
     def body(*refs):
-        ffn_kernel(cuts, *refs)
+        ffn_kernel(cuts, 3, *refs)
 
     return pl.pallas_call(
         body,
@@ -125,7 +152,7 @@
         scratch_shapes=[
             pltpu.VMEM((width, 2 * units), jnp.bfloat16),
             pltpu.VMEM((width, units), jnp.bfloat16),
-            pltpu.SemaphoreType.DMA((len(cuts) + 1,)),
+            pltpu.SemaphoreType.DMA((2 * len(cuts) + 2,)),
         ],
         compiler_params=pltpu.CompilerParams(vmem_limit_bytes=48 << 20),
         name="ffn",
@@ -152,9 +179,12 @@
 
     docs = jnp.pad(doc_ids.astype(jnp.bfloat16)[None], ((0, 15), (0, 2 * keys.shape[1] - rows)))
     own = jnp.concatenate([jnp.concatenate([keys, values], axis=1), docs], axis=0)
-    near = {k: shifted(own, k) for k in (2, 6, 1, 7)}
-    far = {4: shifted(near[2], 2), 3: shifted(near[2], 1), 5: shifted(near[6], -1)}
-    blocks = {0: own, **near, **far}
+    blocks = {0: own}
+    blocks[7] = shifted(own, 7)
+    for back in range(1, 5):
+        blocks[back] = shifted(blocks[back - 1], 1)
+        if back < 3:
+            blocks[7 - back] = shifted(blocks[8 - back], -1)
     attended = attention(queries, [blocks[b] for b in range(8)], score_offset)
 
     mixed_attn = summed_for_owner(

time: 153 us -> 147 us (0.961)
  waiting for transfers between devices: 44 us -> 40.5 us
  starting transfers between devices: 30.4 us -> 28.2 us
  blocking collectives: 44.5 us -> 46.5 us
  Pallas kernels: 12.1 us -> 10.2 us
    all_gather x1, waiting for transfers between devices: 38.5 us -> 21.4 us  [on_device(): weights = lax.all_gather(packed, 'sp', axis=0, tiled=True)]
    ppermute x7, waiting for transfers between devices: 5.53 us -> 19.1 us  [shifted(): lax.ppermute(block, 'sp', [(i, (i + by) % spans) for i in range(spans)])]
    ppermute x7, starting transfers between devices: 30.4 us -> 28.2 us  [shifted(): lax.ppermute(block, 'sp', [(i, (i + by) % spans) for i in range(spans)])]
    all_to_all x2, blocking collectives: 31.7 us -> 33.7 us  [summed_for_owner(): tiles = lax.all_to_all(tiles, 'tp', 0, 0, tiled=True)]
    pallas_call x1, Pallas kernels: 6.83 us -> 4.87 us  [ffn(): pl.pallas_call(body, out_shape=jax.ShapeDtypeStruct(x.shape, jnp.bfloat16...]
  transfers between devices with their start and end apart: 8 -> 8, of which waited for: 5 -> 5; matrix products, arithmetic and copies ran while one was open for 3% -> 3% of each run, Pallas kernels for 3% -> 4%
where the time goes in v6:
time: 147 us
  blocking collectives  46.5 us (32%)
  waiting for transfers between devices  40.5 us (28%)
  starting transfers between devices  28.2 us (19%)
  between operations  13.5 us (9%)
  Pallas kernels  10.2 us (7%)
  other arithmetic  5.91 us (4%)
  local copies, waits for them, and re-layouts  1.55 us (1%)
    all_to_all x2, blocking collectives, summed_for_owner(): tiles = lax.all_to_all(tiles, 'tp', 0, 0, tiled=True)  33.7 us
    ppermute x7, starting transfers between devices, shifted(): lax.ppermute(block, 'sp', [(i, (i + by) % spans) for i in range(spans)])  28.2 us
    all_gather x1, waiting for transfers between devices, on_device(): weights = lax.all_gather(packed, 'sp', axis=0, tiled=True)  21.4 us
    ppermute x7, waiting for transfers between devices, shifted(): lax.ppermute(block, 'sp', [(i, (i + by) % spans) for i in range(spans)])  19.1 us
    all_to_all x1, blocking collectives, from_everyone(): return lax.all_to_all(copies, 'tp', split_axis=0, concat_axis=0, tiled=True)  12.8 us
    pallas_call x1, Pallas kernels, attention(): pl.pallas_call(body, out_shape=jax.ShapeDtypeStruct((rows, width), jnp.bf...  5.3 us
    pallas_call x1, Pallas kernels, ffn(): pl.pallas_call(body, out_shape=jax.ShapeDtypeStruct(x.shape, jnp.bfloat16...  4.87 us
  transfers between devices with their start and end apart: 8, of which 5 were waited for; matrix products, arithmetic and copies ran while one was open for 3% of the time, Pallas kernels for 4%

profile of v6, /device:TPU:1, one launch (start us, length us, event | category | flops | bytes accessed | tf_op | source)
XLA Modules:
  0.0 146.7 jit_solution(17354776138253654723)
XLA Ops:
  6.5 1.6 %pad_maximum_fusion = bf16[32,2304]{1,0:T(8,128)(2,1)} fusion(bf16[32,768]{1,0:T(8,128)(2,1)} %bitcast.11, bf16[32,768]{1,0:T(8,128)(2,1)} %param.20, bf16[32,768]{1,0:T(8,128)(2,1)} %param.19), kind=kLoop, calls=%fused_computation.6 | loop fusion | flops 442368 | bytes 294912 | tf_op jit(solution)/shard_map/concatenate | solution.py:177
  8.2 0.7 convert_bitcast_fusion
  8.8 0.9 fusion.1.refs_2_
  9.7 4.0 %collective-permute-start = (bf16[144,512]{1,0:T(8,128)(2,1)S(1)}, bf16[144,512]{1,0:T(8,128)(2,1)S(1)}, u32[]{:S(2)}, u32[]{:S(2)}) collective-permute-start(bf16[144,512]{1,0:T(8,128)(2,1)S(1)} %fusion.1.refs_2_), channel_id=1, source_target_pairs={{0,8},{8,16},{16,24},{24,32},{32,40},{40,48},{48,56},{56,64},{64,7... | collective-permute-start | bytes 442376 | tf_op jit(solution)/shard_map/ppermute | solution.py:11
  13.8 5.1 %collective-permute-start.4 = (bf16[144,512]{1,0:T(8,128)(2,1)S(1)}, bf16[144,512]{1,0:T(8,128)(2,1)S(1)}, u32[]{:S(2)}, u32[]{:S(2)}) collective-permute-start(bf16[144,512]{1,0:T(8,128)(2,1)S(1)} %fusion.1.refs_2_), channel_id=1, source_target_pairs={{0,56},{8,64},{16,72},{24,80},{32,88},{40,96},{48,104},{56,112},{6... | collective-permute-start | bytes 442376 | tf_op jit(solution)/shard_map/ppermute | solution.py:11
  18.9 9.5 %collective-permute-done.refs_3_ = bf16[144,512]{1,0:T(8,128)(2,1)S(1)} collective-permute-done((bf16[144,512]{1,0:T(8,128)(2,1)S(1)}, bf16[144,512]{1,0:T(8,128)(2,1)S(1)}, u32[]{:S(2)}, u32[]{:S(2)}) %collective-permute-start) | collective-permute-done | bytes 147488 | tf_op jit(solution)/shard_map/ppermute | solution.py:11
  28.4 1.9 %collective-permute-start.1 = (bf16[144,512]{1,0:T(8,128)(2,1)S(1)}, bf16[144,512]{1,0:T(8,128)(2,1)S(1)}, u32[]{:S(2)}, u32[]{:S(2)}) collective-permute-start(bf16[144,512]{1,0:T(8,128)(2,1)S(1)} %collective-permute-done.refs_3_), channel_id=1, source_target_pairs={{0,8},{8,16},{16,24},{24,32},{32,40},{40,48},{48,56},{56,64},{64,7... | collective-permute-start | bytes 442376 | tf_op jit(solution)/shard_map/ppermute | solution.py:11
  30.3 6.7 %collective-permute-start.5 = (bf16[144,512]{1,0:T(8,128)(2,1)S(1)}, bf16[144,512]{1,0:T(8,128)(2,1)S(1)}, u32[]{:S(2)}, u32[]{:S(2)}) collective-permute-start(bf16[144,512]{1,0:T(8,128)(2,1)S(1)} %collective-permute-done.4.refs_9_), channel_id=1, source_target_pairs={{0,504},{8,0},{16,8},{24,16},{32,24},{40,32},{48,40},{56,48},{64,5... | collective-permute-start | bytes 442376 | tf_op jit(solution)/shard_map/ppermute | solution.py:11
  37.0 0.7 collective-permute-done.1.refs_4_
  37.7 1.9 %collective-permute-start.2 = (bf16[144,512]{1,0:T(8,128)(2,1)S(1)}, bf16[144,512]{1,0:T(8,128)(2,1)S(1)}, u32[]{:S(2)}, u32[]{:S(2)}) collective-permute-start(bf16[144,512]{1,0:T(8,128)(2,1)S(1)} %collective-permute-done.1.refs_4_), channel_id=1, source_target_pairs={{0,8},{8,16},{16,24},{24,32},{32,40},{40,48},{48,56},{56,64},{64,7... | collective-permute-start | bytes 442376 | tf_op jit(solution)/shard_map/ppermute | solution.py:11
  39.6 6.7 %collective-permute-start.6 = (bf16[144,512]{1,0:T(8,128)(2,1)S(1)}, bf16[144,512]{1,0:T(8,128)(2,1)S(1)}, u32[]{:S(2)}, u32[]{:S(2)}) collective-permute-start(bf16[144,512]{1,0:T(8,128)(2,1)S(1)} %collective-permute-done.5.refs_8_), channel_id=1, source_target_pairs={{0,504},{8,0},{16,8},{24,16},{32,24},{40,32},{48,40},{56,48},{64,5... | collective-permute-start | bytes 442376 | tf_op jit(solution)/shard_map/ppermute | solution.py:11
  46.3 1.2 collective-permute-done.2.refs_5_
  47.6 1.9 %collective-permute-start.3 = (bf16[144,512]{1,0:T(8,128)(2,1)S(1)}, bf16[144,512]{1,0:T(8,128)(2,1)S(1)}, u32[]{:S(2)}, u32[]{:S(2)}) collective-permute-start(bf16[144,512]{1,0:T(8,128)(2,1)S(1)} %collective-permute-done.2.refs_5_), channel_id=1, source_target_pairs={{0,8},{8,16},{16,24},{24,32},{32,40},{40,48},{48,56},{56,64},{64,7... | collective-permute-start | bytes 442376 | tf_op jit(solution)/shard_map/ppermute | solution.py:11
  49.5 7.7 %collective-permute-done.3.refs_6_ = bf16[144,512]{1,0:T(8,128)(2,1)S(1)} collective-permute-done((bf16[144,512]{1,0:T(8,128)(2,1)S(1)}, bf16[144,512]{1,0:T(8,128)(2,1)S(1)}, u32[]{:S(2)}, u32[]{:S(2)}) %collective-permute-start.3) | collective-permute-done | bytes 147488 | tf_op jit(solution)/shard_map/ppermute | solution.py:11
  57.1 0.8 copy-done.1
  58.6 5.3 %attention.1 = bf16[128,256]{1,0:T(8,128)(2,1)S(1)} custom-call(f32[4]{0:T(128)S(1)} %copy-done.2, bf16[128,256]{1,0:T(8,128)(2,1)S(1)} %copy-done.1, bf16[144,512]{1,0:T(8,128)(2,1)S(1)} %fusion.1.refs_2_, bf16[144,512]{1,0:T(8,128)(2,1)S(1)} %collective-permute-done.refs_3_, bf16[144,512]{1,0:T(8,128)(2,1)S(1)} %collective-permute-done.1.refs_4_, ...), custom_call_target="tpu_custom_call" | custom-call | tf_op jit(solution)/shard_map/attention/pallas_call | solution.py:76
  64.3 19.5 %all_to_all.15 = bf16[8,16,2048]{2,1,0:T(8,128)(2,1)S(1)} all-to-all(bf16[8,16,2048]{2,1,0:T(8,128)(2,1)S(1)} %bitcast.10), channel_id=1, replica_groups=mesh['sp'=64,'tp'=8] {'tp'}, dimensions={0} | all-to-all | bytes 1048576 | tf_op jit(solution)/shard_map/all_to_all | solution.py:17
  83.9 1.0 multiply_reduce_fusion
  84.9 0.9 multiply_convert_fusion
  85.9 12.8 %all_to_all.16 = bf16[8,16,2048]{2,1,0:T(8,128)(2,1)S(1)} all-to-all(bf16[8,16,2048]{2,1,0:T(8,128)(2,1)S(1)} %broadcast_in_dim.9), channel_id=1, replica_groups=mesh['sp'=64,'tp'=8] {'tp'}, dimensions={0} | all-to-all | bytes 1048576 | tf_op jit(solution)/shard_map/all_to_all | solution.py:23
  98.6 21.4 %all-gather.2.cloned.1.call-done.refs_1_ = bf16[2048,2304]{1,0:T(8,128)(2,1)} async-done(((bf16[32,2304]{1,0:T(8,128)(2,1)}), bf16[2048,2304]{1,0:T(8,128)(2,1)}) %all-gather.2.cloned.1.call-update) | async-done | bytes 9437200 | tf_op jit(solution)/shard_map/all_gather | solution.py:178
  120.0 4.9 %ffn.1 = bf16[128,2048]{1,0:T(8,128)(2,1)S(1)} custom-call(bf16[128,2048]{1,0:T(8,128)(2,1)S(1)} %bitcast.8, bf16[2048,2304]{1,0:T(8,128)(2,1)} %all-gather.2.cloned.1.call-done.refs_1_), custom_call_target="tpu_custom_call" | custom-call | tf_op jit(solution)/shard_map/ffn/pallas_call | solution.py:147
  124.9 14.2 %all_to_all.17 = bf16[8,16,2048]{2,1,0:T(8,128)(2,1)S(1)} all-to-all(bf16[8,16,2048]{2,1,0:T(8,128)(2,1)S(1)} %bitcast.9), channel_id=1, replica_groups=mesh['sp'=64,'tp'=8] {'tp'}, dimensions={0} | all-to-all | bytes 1048576 | tf_op jit(solution)/shard_map/all_to_all | solution.py:17
  139.2 0.7 add_convert_fusion
  (17 shorter events, 1.2 us)
Async XLA Ops:
  6.5 57.4 %copy-start = (bf16[256,2048]{1,0:T(8,128)(2,1)S(1)}, bf16[256,2048]{1,0:T(8,128)(2,1)}, u32[]{:S(2)}) copy-start(bf16[256,2048]{1,0:T(8,128)(2,1)} %param.17) | copy-start | bytes 3145732
  6.5 113.5 %all-gather.2.cloned.1.call-start = ((), (), s32[]{:S(2)}) async-start(), calls=%async_computation.3 | async-start | bytes 9584640 | tf_op jit(solution)/shard_map/all_gather | solution.py:178
  8.8 130.4 %copy-start.3 = (bf16[16,2048]{1,0:T(8,128)(2,1)S(1)}, bf16[16,2048]{1,0:T(8,128)(2,1)}, u32[]{:S(2)}) copy-start(bf16[16,2048]{1,0:T(8,128)(2,1)} %param.11) | copy-start | bytes 196612
  9.7 18.6 %collective-permute-start = (bf16[144,512]{1,0:T(8,128)(2,1)S(1)}, bf16[144,512]{1,0:T(8,128)(2,1)S(1)}, u32[]{:S(2)}, u32[]{:S(2)}) collective-permute-start(bf16[144,512]{1,0:T(8,128)(2,1)S(1)} %fusion.1.refs_2_), channel_id=1, source_target_pairs={{0,8},{8,16},{16,24},{24,32},{32,40},{40,48},{48,56},{56,64},{64,7... | collective-permute-start | bytes 442376 | tf_op jit(solution)/shard_map/ppermute | solution.py:11
  13.8 16.6 %collective-permute-start.4 = (bf16[144,512]{1,0:T(8,128)(2,1)S(1)}, bf16[144,512]{1,0:T(8,128)(2,1)S(1)}, u32[]{:S(2)}, u32[]{:S(2)}) collective-permute-start(bf16[144,512]{1,0:T(8,128)(2,1)S(1)} %fusion.1.refs_2_), channel_id=1, source_target_pairs={{0,56},{8,64},{16,72},{24,80},{32,88},{40,96},{48,104},{56,112},{6... | collective-permute-start | bytes 442376 | tf_op jit(solution)/shard_map/ppermute | solution.py:11
  28.4 9.3 %collective-permute-start.1 = (bf16[144,512]{1,0:T(8,128)(2,1)S(1)}, bf16[144,512]{1,0:T(8,128)(2,1)S(1)}, u32[]{:S(2)}, u32[]{:S(2)}) collective-permute-start(bf16[144,512]{1,0:T(8,128)(2,1)S(1)} %collective-permute-done.refs_3_), channel_id=1, source_target_pairs={{0,8},{8,16},{16,24},{24,32},{32,40},{40,48},{48,56},{56,64},{64,7... | collective-permute-start | bytes 442376 | tf_op jit(solution)/shard_map/ppermute | solution.py:11
  30.3 9.3 %collective-permute-start.5 = (bf16[144,512]{1,0:T(8,128)(2,1)S(1)}, bf16[144,512]{1,0:T(8,128)(2,1)S(1)}, u32[]{:S(2)}, u32[]{:S(2)}) collective-permute-start(bf16[144,512]{1,0:T(8,128)(2,1)S(1)} %collective-permute-done.4.refs_9_), channel_id=1, source_target_pairs={{0,504},{8,0},{16,8},{24,16},{32,24},{40,32},{48,40},{56,48},{64,5... | collective-permute-start | bytes 442376 | tf_op jit(solution)/shard_map/ppermute | solution.py:11
  37.7 9.9 %collective-permute-start.2 = (bf16[144,512]{1,0:T(8,128)(2,1)S(1)}, bf16[144,512]{1,0:T(8,128)(2,1)S(1)}, u32[]{:S(2)}, u32[]{:S(2)}) collective-permute-start(bf16[144,512]{1,0:T(8,128)(2,1)S(1)} %collective-permute-done.1.refs_4_), channel_id=1, source_target_pairs={{0,8},{8,16},{16,24},{24,32},{32,40},{40,48},{48,56},{56,64},{64,7... | collective-permute-start | bytes 442376 | tf_op jit(solution)/shard_map/ppermute | solution.py:11
  39.6 9.9 %collective-permute-start.6 = (bf16[144,512]{1,0:T(8,128)(2,1)S(1)}, bf16[144,512]{1,0:T(8,128)(2,1)S(1)}, u32[]{:S(2)}, u32[]{:S(2)}) collective-permute-start(bf16[144,512]{1,0:T(8,128)(2,1)S(1)} %collective-permute-done.5.refs_8_), channel_id=1, source_target_pairs={{0,504},{8,0},{16,8},{24,16},{32,24},{40,32},{48,40},{56,48},{64,5... | collective-permute-start | bytes 442376 | tf_op jit(solution)/shard_map/ppermute | solution.py:11
  47.6 9.6 %collective-permute-start.3 = (bf16[144,512]{1,0:T(8,128)(2,1)S(1)}, bf16[144,512]{1,0:T(8,128)(2,1)S(1)}, u32[]{:S(2)}, u32[]{:S(2)}) collective-permute-start(bf16[144,512]{1,0:T(8,128)(2,1)S(1)} %collective-permute-done.2.refs_5_), channel_id=1, source_target_pairs={{0,8},{8,16},{16,24},{24,32},{32,40},{40,48},{48,56},{56,64},{64,7... | collective-permute-start | bytes 442376 | tf_op jit(solution)/shard_map/ppermute | solution.py:11
  57.1 0.8 copy-start.1
  58.0 0.7 copy-start.2
Sparse Core Ops, SparseCore 0:
  10.3 109.6 all-gather.1

commit v7 on v6

--- a/solution.py
+++ b/solution.py
@@ -83,9 +83,10 @@
     )(offsets, queries, *blocks)
 
 
-def ffn_kernel(cuts, ahead, x, weights, out, gate_up, down, sems):
+def ffn_kernel(cuts, ahead, x, gate_low, weights, out, gate_up, down, sems):
     units = down.shape[1]
     half = down.shape[0] // 2
+    wide = gate_up.shape[1]
 
     def copy(source, target, sem):
         return pltpu.make_async_copy(source, target, sem)
@@ -96,7 +97,7 @@
         stages.append(
             [
                 copy(
-                    weights.at[pl.ds(at, n), pl.ds(0, 2 * units)],
+                    weights.at[pl.ds(at, n), pl.ds(0, wide)],
                     gate_up.at[pl.ds(at, n)],
                     sems.at[2 * i + j],
                 )
@@ -106,7 +107,7 @@
     for j in range(2):
         rows = pl.ds(j * half, half)
         stages.append(
-            [copy(weights.at[rows, pl.ds(2 * units, units)], down.at[rows], sems.at[2 * len(cuts) + j])]
+            [copy(weights.at[rows, pl.ds(wide, units)], down.at[rows], sems.at[2 * len(cuts) + j])]
         )
 
     def start(i):
@@ -125,7 +126,8 @@
         wait(i)
         term = jnp.dot(x[:, a:b], gate_up[a:b, :], preferred_element_type=jnp.float32)
         acc = term if acc is None else acc + term
-    gate, upper = acc[:, :units], acc[:, units:]
+    gate = jnp.concatenate([gate_low[...], acc[:, : wide - units]], axis=1)
+    upper = acc[:, wide - units :]
     hidden = (gate / (1.0 + jnp.exp(-gate)) * upper).astype(jnp.bfloat16)
     for j in range(2):
         wait(len(cuts) + j)
@@ -135,8 +137,9 @@
         ).astype(jnp.bfloat16)
 
 
-def ffn(x, weights, units):
+def ffn(x, gate_low, weights, units):
     width = weights.shape[0]
+    wide = weights.shape[1] - units
     marks = (0, 3 * width // 8, 11 * width // 16, width)
     cuts = tuple(zip(marks[:-1], marks[1:]))
     vmem = pl.BlockSpec(memory_space=pltpu.VMEM)
@@ -147,16 +150,45 @@
     return pl.pallas_call(
         body,
         out_shape=jax.ShapeDtypeStruct(x.shape, jnp.bfloat16),
-        in_specs=[vmem, pl.BlockSpec(memory_space=pltpu.HBM)],
+        in_specs=[vmem, vmem, pl.BlockSpec(memory_space=pltpu.HBM)],
         out_specs=vmem,
         scratch_shapes=[
-            pltpu.VMEM((width, 2 * units), jnp.bfloat16),
+            pltpu.VMEM((width, wide), jnp.bfloat16),
             pltpu.VMEM((width, units), jnp.bfloat16),
             pltpu.SemaphoreType.DMA((2 * len(cuts) + 2,)),
         ],
         compiler_params=pltpu.CompilerParams(vmem_limit_bytes=48 << 20),
         name="ffn",
-    )(x, weights)
+    )(x, gate_low, weights)
+
+
+def side_kernel(start, x, *refs):
+    blocks, out = refs[:-1], refs[-1]
+    step = blocks[0].shape[0]
+    width = x.shape[1]
+    turned = pltpu.roll(x[...].astype(jnp.float32), (width - start[0]) & (width - 1), 1)
+    turned = turned.astype(jnp.bfloat16)
+    acc = None
+    for i in range(len(blocks)):
+        term = jnp.dot(
+            turned[:, i * step : (i + 1) * step],
+            blocks[len(blocks) - 1 - i][...],
+            preferred_element_type=jnp.float32,
+        )
+        acc = term if acc is None else acc + term
+    out[...] = acc
+
+
+def side(x, blocks, start):
+    vmem = pl.BlockSpec(memory_space=pltpu.VMEM)
+    return pl.pallas_call(
+        side_kernel,
+        out_shape=jax.ShapeDtypeStruct((x.shape[0], blocks[0].shape[1]), jnp.float32),
+        in_specs=[pl.BlockSpec(memory_space=pltpu.SMEM)] + [vmem] * (1 + len(blocks)),
+        out_specs=vmem,
+        compiler_params=pltpu.CompilerParams(vmem_limit_bytes=12 << 20),
+        name="side",
+    )(start, x, *blocks)
 
 
 def on_device(
@@ -174,17 +206,33 @@
 ):
     rows = queries.shape[0]
     units = gate_weight.shape[1]
-    packed = jnp.concatenate([gate_weight, up_weight, down_weight.T], axis=1)
+    low = units // 2
+    packed = jnp.concatenate([gate_weight[:, low:], up_weight, down_weight.T], axis=1)
     weights = lax.all_gather(packed, "sp", axis=0, tiled=True)
 
     docs = jnp.pad(doc_ids.astype(jnp.bfloat16)[None], ((0, 15), (0, 2 * keys.shape[1] - rows)))
-    own = jnp.concatenate([jnp.concatenate([keys, values], axis=1), docs], axis=0)
-    blocks = {0: own}
+    shard = jnp.pad(gate_weight[:, :low], ((0, 0), (0, 2 * keys.shape[1] - low)))
+    tall = rows + docs.shape[0]
+    own = jnp.concatenate([jnp.concatenate([keys, values], axis=1), docs])
+    both = jnp.concatenate([own, shard])
+    blocks = {0: both}
+    blocks[1] = shifted(both, 1)
     blocks[7] = shifted(own, 7)
-    for back in range(1, 5):
-        blocks[back] = shifted(blocks[back - 1], 1)
-        if back < 3:
-            blocks[7 - back] = shifted(blocks[8 - back], -1)
+    after = shifted(shard, -1)
+    blocks[2] = shifted(blocks[1], 1)
+    blocks[6] = shifted(jnp.concatenate([blocks[7], after]), -1)
+    blocks[3] = shifted(blocks[2], 1)
+    blocks[5] = shifted(blocks[6], -1)
+    blocks[4] = shifted(blocks[3], 1)
+    near = [blocks[k][tall:, :low] for k in (4, 3, 2, 1)]
+    near += [shard[:, :low], after[:, :low]] + [blocks[k][tall:, :low] for k in (6, 5)]
+    ring, rings = len(near), lax.axis_size("sp") // len(near)
+    sides = {0: jnp.concatenate(near)}
+    for k in range(1, rings // 2 + 1):
+        sides[k] = shifted(sides[k - 1], ring)
+        if k < rings // 2:
+            sides[rings - k] = shifted(sides[(rings - k + 1) % rings], -ring)
+    start = ((lax.axis_index("sp") + ring // 2) & (ring * rings - 1)) * near[0].shape[0]
     attended = attention(queries, [blocks[b] for b in range(8)], score_offset)
 
     mixed_attn = summed_for_owner(
@@ -195,7 +243,8 @@
         stream * lax.rsqrt(jnp.mean(stream * stream, axis=1, keepdims=True) + 1e-06) * norm_gain
     ).astype(jnp.bfloat16)
     span_rows = from_everyone(normed).reshape(rows, -1)
-    feed = summed_for_owner(ffn(span_rows, weights, units))
+    gate_low = side(span_rows, [sides[k] for k in range(rings)], start[None])
+    feed = summed_for_owner(ffn(span_rows, gate_low, weights, units))
     return (stream + feed).astype(jnp.bfloat16)
 
 
@@ -214,6 +263,7 @@
         P("tp", "sp"),
     )
     out_specs = P(("sp", "tp"), None)
+
     return jax.shard_map(
         on_device, mesh=mesh, in_specs=in_specs, out_specs=out_specs, check_vma=False
     )

time: 147 us -> 164 us (1.12)
  starting transfers between devices: 28.2 us -> 73.9 us
  blocking collectives: 46.5 us -> 15.6 us
  local copies, waits for them, and re-layouts: 1.55 us -> 5.01 us
  waiting for transfers between devices: 40.5 us -> 38 us
    ppermute x7 -> x15, starting transfers between devices: 28.2 us -> 58.2 us  [shifted(): lax.ppermute(block, 'sp', [(i, (i + by) % spans) for i in range(spans)])]
    all_gather x1, waiting for transfers between devices: 21.4 us -> 0.02 us  [on_device(): weights = lax.all_gather(packed, 'sp', axis=0, tiled=True)]
    ppermute x7 -> x15, waiting for transfers between devices: 19.1 us -> 38 us  [shifted(): lax.ppermute(block, 'sp', [(i, (i + by) % spans) for i in range(spans)])]
    all_to_all x2 -> x1, blocking collectives: 33.7 us -> 15.6 us  [summed_for_owner(): tiles = lax.all_to_all(tiles, 'tp', 0, 0, tiled=True)]
    all_to_all x0 -> x2, starting transfers between devices: none -> 15.7 us  [the longest x1 10.3 us: summed_for_owner(): tiles = lax.all_to_all(tiles, 'tp', 0, 0, tiled=True)]
    all_to_all x1 -> x0, blocking collectives: 12.8 us -> none  [from_everyone(): return lax.all_to_all(copies, 'tp', split_axis=0, concat_axis=0, tiled=True)]
  transfers between devices with their start and end apart: 8 -> 18, of which waited for: 5 -> 9; matrix products, arithmetic and copies ran while one was open for 3% -> 4% of each run, Pallas kernels for 4% -> 4%
where the time goes in v7:
time: 164 us; the launch traced here: 163 us
  starting transfers between devices  73.9 us (45%)
  waiting for transfers between devices  38 us (23%)
  blocking collectives  15.6 us (10%)
  between operations  13.7 us (8%)
  Pallas kernels  10.3 us (6%)
  other arithmetic  5.67 us (3%)
  local copies, waits for them, and re-layouts  5.01 us (3%)
    ppermute x15, starting transfers between devices, shifted(): lax.ppermute(block, 'sp', [(i, (i + by) % spans) for i in range(spans)])  58.2 us
    ppermute x15, waiting for transfers between devices, shifted(): lax.ppermute(block, 'sp', [(i, (i + by) % spans) for i in range(spans)])  38 us
    all_to_all x1, blocking collectives, summed_for_owner(): tiles = lax.all_to_all(tiles, 'tp', 0, 0, tiled=True)  15.6 us
    all_to_all x1, starting transfers between devices, summed_for_owner(): tiles = lax.all_to_all(tiles, 'tp', 0, 0, tiled=True)  10.3 us
    all_to_all x1, starting transfers between devices, from_everyone(): return lax.all_to_all(copies, 'tp', split_axis=0, concat_axis=0, tiled=True)  5.35 us
    pallas_call x1, Pallas kernels, attention(): pl.pallas_call(body, out_shape=jax.ShapeDtypeStruct((rows, width), jnp.bf...  5.27 us
    pallas_call x1, Pallas kernels, ffn(): pl.pallas_call(body, out_shape=jax.ShapeDtypeStruct(x.shape, jnp.bfloat16...  4.44 us
  transfers between devices with their start and end apart: 18, of which 9 were waited for; matrix products, arithmetic and copies ran while one was open for 4% of the time, Pallas kernels for 4%

profile of v7, /device:TPU:1, one launch (start us, length us, event | category | flops | bytes accessed | tf_op | source)
XLA Modules:
  0.0 163.3 jit_solution(12110291927030892655)
XLA Ops:
  12.0 4.0 %collective-permute-start = (bf16[176,512]{1,0:T(8,128)(2,1)S(1)}, bf16[176,512]{1,0:T(8,128)(2,1)S(1)}, u32[]{:S(2)}, u32[]{:S(2)}) collective-permute-start(bf16[176,512]{1,0:T(8,128)(2,1)S(1)} %pad_maximum_fusion.refs_2_), channel_id=1, source_target_pairs={{0,8},{8,16},{16,24},{24,32},{32,40},{40,48},{48,56},{56,64},{64,7... | collective-permute-start | bytes 540680 | tf_op jit(solution)/shard_map/ppermute | solution.py:11
  16.1 5.1 %collective-permute-start.4 = (bf16[144,512]{1,0:T(8,128)(2,1)S(1)}, bf16[144,512]{1,0:T(8,128)(2,1)S(1)}, u32[]{:S(2)}, u32[]{:S(2)}) collective-permute-start(bf16[144,512]{1,0:T(8,128)(2,1)S(1)} %pad_maximum_fusion.2), channel_id=1, source_target_pairs={{0,56},{8,64},{16,72},{24,80},{32,88},{40,96},{48,104},{56,112},{6... | collective-permute-start | bytes 442376 | tf_op jit(solution)/shard_map/ppermute | solution.py:11
  21.2 10.5 %collective-permute-done.refs_3_ = bf16[176,512]{1,0:T(8,128)(2,1)S(1)} collective-permute-done((bf16[176,512]{1,0:T(8,128)(2,1)S(1)}, bf16[176,512]{1,0:T(8,128)(2,1)S(1)}, u32[]{:S(2)}, u32[]{:S(2)}) %collective-permute-start) | collective-permute-done | bytes 180256 | tf_op jit(solution)/shard_map/ppermute | solution.py:11
  33.6 6.7 %collective-permute-start.5 = (bf16[32,512]{1,0:T(8,128)(2,1)S(1)}, bf16[32,512]{1,0:T(8,128)(2,1)S(1)}, u32[]{:S(2)}, u32[]{:S(2)}) collective-permute-start(bf16[32,512]{1,0:T(8,128)(2,1)S(1)} %slice_select_fusion), channel_id=1, source_target_pairs={{0,504},{8,0},{16,8},{24,16},{32,24},{40,32},{48,40},{56,48},{64,5... | collective-permute-start | bytes 98312 | tf_op jit(solution)/shard_map/ppermute | solution.py:11
  41.3 7.1 %collective-permute-start.6 = (bf16[176,512]{1,0:T(8,128)(2,1)S(1)}, bf16[176,512]{1,0:T(8,128)(2,1)S(1)}, u32[]{:S(2)}, u32[]{:S(2)}) collective-permute-start(bf16[176,512]{1,0:T(8,128)(2,1)S(1)} %pad_maximum_fusion.1), channel_id=1, source_target_pairs={{0,504},{8,0},{16,8},{24,16},{32,24},{40,32},{48,40},{56,48},{64,5... | collective-permute-start | bytes 540680 | tf_op jit(solution)/shard_map/ppermute | solution.py:11
  48.4 1.9 %collective-permute-start.2 = (bf16[176,512]{1,0:T(8,128)(2,1)S(1)}, bf16[176,512]{1,0:T(8,128)(2,1)S(1)}, u32[]{:S(2)}, u32[]{:S(2)}) collective-permute-start(bf16[176,512]{1,0:T(8,128)(2,1)S(1)} %collective-permute-done.1.refs_4_), channel_id=1, source_target_pairs={{0,8},{8,16},{16,24},{24,32},{32,40},{40,48},{48,56},{56,64},{64,7... | collective-permute-start | bytes 540680 | tf_op jit(solution)/shard_map/ppermute | solution.py:11
  51.3 7.2 %collective-permute-start.7 = (bf16[176,512]{1,0:T(8,128)(2,1)S(1)}, bf16[176,512]{1,0:T(8,128)(2,1)S(1)}, u32[]{:S(2)}, u32[]{:S(2)}) collective-permute-start(bf16[176,512]{1,0:T(8,128)(2,1)S(1)} %collective-permute-done.6.refs_8_), channel_id=1, source_target_pairs={{0,504},{8,0},{16,8},{24,16},{32,24},{40,32},{48,40},{56,48},{64,5... | collective-permute-start | bytes 540680 | tf_op jit(solution)/shard_map/ppermute | solution.py:11
  58.5 1.9 %collective-permute-start.3 = (bf16[176,512]{1,0:T(8,128)(2,1)S(1)}, bf16[176,512]{1,0:T(8,128)(2,1)S(1)}, u32[]{:S(2)}, u32[]{:S(2)}) collective-permute-start(bf16[176,512]{1,0:T(8,128)(2,1)S(1)} %collective-permute-done.2.refs_5_), channel_id=1, source_target_pairs={{0,8},{8,16},{16,24},{24,32},{32,40},{40,48},{48,56},{56,64},{64,7... | collective-permute-start | bytes 540680 | tf_op jit(solution)/shard_map/ppermute | solution.py:11
  61.1 7.0 %collective-permute-done.3.refs_6_ = bf16[176,512]{1,0:T(8,128)(2,1)S(1)} collective-permute-done((bf16[176,512]{1,0:T(8,128)(2,1)S(1)}, bf16[176,512]{1,0:T(8,128)(2,1)S(1)}, u32[]{:S(2)}, u32[]{:S(2)}) %collective-permute-start.3) | collective-permute-done | bytes 180256 | tf_op jit(solution)/shard_map/ppermute | solution.py:11
  69.6 5.3 %attention.1 = bf16[128,256]{1,0:T(8,128)(2,1)S(1)} custom-call(f32[4]{0:T(128)S(1)} %copy-done.2, bf16[128,256]{1,0:T(8,128)(2,1)S(1)} %copy-done.1, bf16[176,512]{1,0:T(8,128)(2,1)S(1)} %pad_maximum_fusion.refs_2_, bf16[176,512]{1,0:T(8,128)(2,1)S(1)} %collective-permute-done.refs_3_, bf16[176,512]{1,0:T(8,128)(2,1)S(1)} %collective-permute-done.1.refs_4_, ...), custom_call_target="tpu_custom_call" | custom-call | tf_op jit(solution)/shard_map/attention/pallas_call | solution.py:76
  76.0 10.3 %all-to-all-start = ((bf16[8,16,2048]{2,1,0:T(8,128)(2,1)}), bf16[8,16,2048]{2,1,0:T(8,128)(2,1)S(1)}, u32[]{:S(2)}, u32[]{:S(2)}) async-start(bf16[8,16,2048]{2,1,0:T(8,128)(2,1)} %bitcast.1), calls=%async_computation | async-start | bytes 1048576 | tf_op jit(solution)/shard_map/all_to_all | solution.py:17
  86.5 2.1 %collective-permute-start.8 = (bf16[256,384]{1,0:T(8,128)(2,1)S(1)}, bf16[256,384]{1,0:T(8,128)(2,1)S(1)}, u32[]{:S(2)}, u32[]{:S(2)}) collective-permute-start(bf16[256,384]{1,0:T(8,128)(2,1)S(1)} %slice_dynamic-update-slice_fusion.refs_0_), channel_id=1, source_target_pairs={{0,64},{8,72},{16,80},{24,88},{32,96},{40,104},{48,112},{56,120},{... | collective-permute-start | bytes 589832 | tf_op jit(solution)/shard_map/ppermute | solution.py:11
  88.6 4.6 %collective-permute-start.12 = (bf16[256,384]{1,0:T(8,128)(2,1)S(1)}, bf16[256,384]{1,0:T(8,128)(2,1)S(1)}, u32[]{:S(2)}, u32[]{:S(2)}) collective-permute-start(bf16[256,384]{1,0:T(8,128)(2,1)S(1)} %slice_dynamic-update-slice_fusion.refs_0_), channel_id=1, source_target_pairs={{0,448},{8,456},{16,464},{24,472},{32,480},{40,488},{48,496},{56,5... | collective-permute-start | bytes 589832 | tf_op jit(solution)/shard_map/ppermute | solution.py:11
  93.1 7.0 %collective-permute-done.8.refs_1_ = bf16[256,384]{1,0:T(8,128)(2,1)S(1)} collective-permute-done((bf16[256,384]{1,0:T(8,128)(2,1)S(1)}, bf16[256,384]{1,0:T(8,128)(2,1)S(1)}, u32[]{:S(2)}, u32[]{:S(2)}) %collective-permute-start.8) | collective-permute-done | bytes 196640 | tf_op jit(solution)/shard_map/ppermute | solution.py:11
  100.1 1.9 %collective-permute-start.9 = (bf16[256,384]{1,0:T(8,128)(2,1)S(1)}, bf16[256,384]{1,0:T(8,128)(2,1)S(1)}, u32[]{:S(2)}, u32[]{:S(2)}) collective-permute-start(bf16[256,384]{1,0:T(8,128)(2,1)S(1)} %collective-permute-done.8.refs_1_), channel_id=1, source_target_pairs={{0,64},{8,72},{16,80},{24,88},{32,96},{40,104},{48,112},{56,120},{... | collective-permute-start | bytes 589832 | tf_op jit(solution)/shard_map/ppermute | solution.py:11
  104.9 5.4 %all-to-all-start.1 = ((bf16[8,16,2048]{2,1,0:T(8,128)(2,1)}), bf16[8,16,2048]{2,1,0:T(8,128)(2,1)S(1)}, u32[]{:S(2)}, u32[]{:S(2)}) async-start(bf16[8,16,2048]{2,1,0:T(8,128)(2,1)} %broadcast_in_dim.12), calls=%async_computation.1 | async-start | bytes 1048576 | tf_op jit(solution)/shard_map/all_to_all | solution.py:23
  110.3 4.8 %collective-permute-start.13 = (bf16[256,384]{1,0:T(8,128)(2,1)S(1)}, bf16[256,384]{1,0:T(8,128)(2,1)S(1)}, u32[]{:S(2)}, u32[]{:S(2)}) collective-permute-start(bf16[256,384]{1,0:T(8,128)(2,1)S(1)} %collective-permute-done.12.refs_7_), channel_id=1, source_target_pairs={{0,448},{8,456},{16,464},{24,472},{32,480},{40,488},{48,496},{56,5... | collective-permute-start | bytes 589832 | tf_op jit(solution)/shard_map/ppermute | solution.py:11
  115.2 1.9 %collective-permute-start.10 = (bf16[256,384]{1,0:T(8,128)(2,1)S(1)}, bf16[256,384]{1,0:T(8,128)(2,1)S(1)}, u32[]{:S(2)}, u32[]{:S(2)}) collective-permute-start(bf16[256,384]{1,0:T(8,128)(2,1)S(1)} %collective-permute-done.9.refs_2_), channel_id=1, source_target_pairs={{0,64},{8,72},{16,80},{24,88},{32,96},{40,104},{48,112},{56,120},{... | collective-permute-start | bytes 589832 | tf_op jit(solution)/shard_map/ppermute | solution.py:11
  117.1 4.4 %collective-permute-done.13.refs_6_ = bf16[256,384]{1,0:T(8,128)(2,1)S(1)} collective-permute-done((bf16[256,384]{1,0:T(8,128)(2,1)S(1)}, bf16[256,384]{1,0:T(8,128)(2,1)S(1)}, u32[]{:S(2)}, u32[]{:S(2)}) %collective-permute-start.13) | collective-permute-done | bytes 196640 | tf_op jit(solution)/shard_map/ppermute | solution.py:11
  121.5 5.2 %collective-permute-start.14 = (bf16[256,384]{1,0:T(8,128)(2,1)S(1)}, bf16[256,384]{1,0:T(8,128)(2,1)S(1)}, u32[]{:S(2)}, u32[]{:S(2)}) collective-permute-start(bf16[256,384]{1,0:T(8,128)(2,1)S(1)} %collective-permute-done.13.refs_6_), channel_id=1, source_target_pairs={{0,448},{8,456},{16,464},{24,472},{32,480},{40,488},{48,496},{56,5... | collective-permute-start | bytes 589832 | tf_op jit(solution)/shard_map/ppermute | solution.py:11
  126.7 1.9 %collective-permute-start.11 = (bf16[256,384]{1,0:T(8,128)(2,1)S(1)}, bf16[256,384]{1,0:T(8,128)(2,1)S(1)}, u32[]{:S(2)}, u32[]{:S(2)}) collective-permute-start(bf16[256,384]{1,0:T(8,128)(2,1)S(1)} %collective-permute-done.10.refs_3_), channel_id=1, source_target_pairs={{0,64},{8,72},{16,80},{24,88},{32,96},{40,104},{48,112},{56,120},{... | collective-permute-start | bytes 589832 | tf_op jit(solution)/shard_map/ppermute | solution.py:11
  130.0 5.1 %collective-permute-done.11.refs_4_ = bf16[256,384]{1,0:T(8,128)(2,1)S(1)} collective-permute-done((bf16[256,384]{1,0:T(8,128)(2,1)S(1)}, bf16[256,384]{1,0:T(8,128)(2,1)S(1)}, u32[]{:S(2)}, u32[]{:S(2)}) %collective-permute-start.11) | collective-permute-done | bytes 196640 | tf_op jit(solution)/shard_map/ppermute | solution.py:11
  135.7 4.4 %ffn.1 = bf16[128,2048]{1,0:T(8,128)(2,1)S(1)} custom-call(bf16[128,2048]{1,0:T(8,128)(2,1)S(1)} %bitcast.10, f32[128,384]{1,0:T(8,128)S(1)} %side.1.refs_1_, bf16[2048,1920]{1,0:T(8,128)(2,1)} %all-gather.2.cloned.1.call-done.refs_2_), custom_call_target="tpu_custom_call" | custom-call | tf_op jit(solution)/shard_map/ffn/pallas_call | solution.py:150
  140.2 15.6 %all_to_all.15 = bf16[8,16,2048]{2,1,0:T(8,128)(2,1)S(1)} all-to-all(bf16[8,16,2048]{2,1,0:T(8,128)(2,1)S(1)} %bitcast.11), channel_id=1, replica_groups=mesh['sp'=64,'tp'=8] {'tp'}, dimensions={0} | all-to-all | bytes 1048576 | tf_op jit(solution)/shard_map/all_to_all | solution.py:17
  (51 shorter events, 18.5 us)
Async XLA Ops:
  6.5 68.3 %copy-start = (bf16[256,2048]{1,0:T(8,128)(2,1)S(1)}, bf16[256,2048]{1,0:T(8,128)(2,1)}, u32[]{:S(2)}) copy-start(bf16[256,2048]{1,0:T(8,128)(2,1)} %param.17) | copy-start | bytes 3145732
  6.5 129.2 %all-gather.2.cloned.1.call-start = ((), (), s32[]{:S(2)}) async-start(), calls=%async_computation.3 | async-start | bytes 7987200 | tf_op jit(solution)/shard_map/all_gather | solution.py:211
  12.0 19.7 %collective-permute-start = (bf16[176,512]{1,0:T(8,128)(2,1)S(1)}, bf16[176,512]{1,0:T(8,128)(2,1)S(1)}, u32[]{:S(2)}, u32[]{:S(2)}) collective-permute-start(bf16[176,512]{1,0:T(8,128)(2,1)S(1)} %pad_maximum_fusion.refs_2_), channel_id=1, source_target_pairs={{0,8},{8,16},{16,24},{24,32},{32,40},{40,48},{48,56},{56,64},{64,7... | collective-permute-start | bytes 540680 | tf_op jit(solution)/shard_map/ppermute | solution.py:11
  16.1 25.2 %collective-permute-start.4 = (bf16[144,512]{1,0:T(8,128)(2,1)S(1)}, bf16[144,512]{1,0:T(8,128)(2,1)S(1)}, u32[]{:S(2)}, u32[]{:S(2)}) collective-permute-start(bf16[144,512]{1,0:T(8,128)(2,1)S(1)} %pad_maximum_fusion.2), channel_id=1, source_target_pairs={{0,56},{8,64},{16,72},{24,80},{32,88},{40,96},{48,104},{56,112},{6... | collective-permute-start | bytes 442376 | tf_op jit(solution)/shard_map/ppermute | solution.py:11
  31.7 16.7 %collective-permute-start.1 = (bf16[176,512]{1,0:T(8,128)(2,1)S(1)}, bf16[176,512]{1,0:T(8,128)(2,1)S(1)}, u32[]{:S(2)}, u32[]{:S(2)}) collective-permute-start(bf16[176,512]{1,0:T(8,128)(2,1)S(1)} %collective-permute-done.refs_3_), channel_id=1, source_target_pairs={{0,8},{8,16},{16,24},{24,32},{32,40},{40,48},{48,56},{56,64},{64,7... | collective-permute-start | bytes 540680 | tf_op jit(solution)/shard_map/ppermute | solution.py:11
  33.6 7.7 %collective-permute-start.5 = (bf16[32,512]{1,0:T(8,128)(2,1)S(1)}, bf16[32,512]{1,0:T(8,128)(2,1)S(1)}, u32[]{:S(2)}, u32[]{:S(2)}) collective-permute-start(bf16[32,512]{1,0:T(8,128)(2,1)S(1)} %slice_select_fusion), channel_id=1, source_target_pairs={{0,504},{8,0},{16,8},{24,16},{32,24},{40,32},{48,40},{56,48},{64,5... | collective-permute-start | bytes 98312 | tf_op jit(solution)/shard_map/ppermute | solution.py:11
  41.3 10.0 %collective-permute-start.6 = (bf16[176,512]{1,0:T(8,128)(2,1)S(1)}, bf16[176,512]{1,0:T(8,128)(2,1)S(1)}, u32[]{:S(2)}, u32[]{:S(2)}) collective-permute-start(bf16[176,512]{1,0:T(8,128)(2,1)S(1)} %pad_maximum_fusion.1), channel_id=1, source_target_pairs={{0,504},{8,0},{16,8},{24,16},{32,24},{40,32},{48,40},{56,48},{64,5... | collective-permute-start | bytes 540680 | tf_op jit(solution)/shard_map/ppermute | solution.py:11
  48.4 10.1 %collective-permute-start.2 = (bf16[176,512]{1,0:T(8,128)(2,1)S(1)}, bf16[176,512]{1,0:T(8,128)(2,1)S(1)}, u32[]{:S(2)}, u32[]{:S(2)}) collective-permute-start(bf16[176,512]{1,0:T(8,128)(2,1)S(1)} %collective-permute-done.1.refs_4_), channel_id=1, source_target_pairs={{0,8},{8,16},{16,24},{24,32},{32,40},{40,48},{48,56},{56,64},{64,7... | collective-permute-start | bytes 540680 | tf_op jit(solution)/shard_map/ppermute | solution.py:11
  51.3 9.8 %collective-permute-start.7 = (bf16[176,512]{1,0:T(8,128)(2,1)S(1)}, bf16[176,512]{1,0:T(8,128)(2,1)S(1)}, u32[]{:S(2)}, u32[]{:S(2)}) collective-permute-start(bf16[176,512]{1,0:T(8,128)(2,1)S(1)} %collective-permute-done.6.refs_8_), channel_id=1, source_target_pairs={{0,504},{8,0},{16,8},{24,16},{32,24},{40,32},{48,40},{56,48},{64,5... | collective-permute-start | bytes 540680 | tf_op jit(solution)/shard_map/ppermute | solution.py:11
  58.5 9.6 %collective-permute-start.3 = (bf16[176,512]{1,0:T(8,128)(2,1)S(1)}, bf16[176,512]{1,0:T(8,128)(2,1)S(1)}, u32[]{:S(2)}, u32[]{:S(2)}) collective-permute-start(bf16[176,512]{1,0:T(8,128)(2,1)S(1)} %collective-permute-done.2.refs_5_), channel_id=1, source_target_pairs={{0,8},{8,16},{16,24},{24,32},{32,40},{40,48},{48,56},{56,64},{64,7... | collective-permute-start | bytes 540680 | tf_op jit(solution)/shard_map/ppermute | solution.py:11
  68.1 0.8 copy-start.1
  68.9 0.7 copy-start.2
  76.0 26.0 %all-to-all-start = ((bf16[8,16,2048]{2,1,0:T(8,128)(2,1)}), bf16[8,16,2048]{2,1,0:T(8,128)(2,1)S(1)}, u32[]{:S(2)}, u32[]{:S(2)}) async-start(bf16[8,16,2048]{2,1,0:T(8,128)(2,1)} %bitcast.1), calls=%async_computation | async-start | bytes 1048576 | tf_op jit(solution)/shard_map/all_to_all | solution.py:17
  86.5 69.3 %copy-start.3 = (bf16[16,2048]{1,0:T(8,128)(2,1)S(1)}, bf16[16,2048]{1,0:T(8,128)(2,1)}, u32[]{:S(2)}) copy-start(bf16[16,2048]{1,0:T(8,128)(2,1)} %param.11) | copy-start | bytes 196612
  86.5 13.6 %collective-permute-start.8 = (bf16[256,384]{1,0:T(8,128)(2,1)S(1)}, bf16[256,384]{1,0:T(8,128)(2,1)S(1)}, u32[]{:S(2)}, u32[]{:S(2)}) collective-permute-start(bf16[256,384]{1,0:T(8,128)(2,1)S(1)} %slice_dynamic-update-slice_fusion.refs_0_), channel_id=1, source_target_pairs={{0,64},{8,72},{16,80},{24,88},{32,96},{40,104},{48,112},{56,120},{... | collective-permute-start | bytes 589832 | tf_op jit(solution)/shard_map/ppermute | solution.py:11
  88.6 21.7 %collective-permute-start.12 = (bf16[256,384]{1,0:T(8,128)(2,1)S(1)}, bf16[256,384]{1,0:T(8,128)(2,1)S(1)}, u32[]{:S(2)}, u32[]{:S(2)}) collective-permute-start(bf16[256,384]{1,0:T(8,128)(2,1)S(1)} %slice_dynamic-update-slice_fusion.refs_0_), channel_id=1, source_target_pairs={{0,448},{8,456},{16,464},{24,472},{32,480},{40,488},{48,496},{56,5... | collective-permute-start | bytes 589832 | tf_op jit(solution)/shard_map/ppermute | solution.py:11
  100.1 15.0 %collective-permute-start.9 = (bf16[256,384]{1,0:T(8,128)(2,1)S(1)}, bf16[256,384]{1,0:T(8,128)(2,1)S(1)}, u32[]{:S(2)}, u32[]{:S(2)}) collective-permute-start(bf16[256,384]{1,0:T(8,128)(2,1)S(1)} %collective-permute-done.8.refs_1_), channel_id=1, source_target_pairs={{0,64},{8,72},{16,80},{24,88},{32,96},{40,104},{48,112},{56,120},{... | collective-permute-start | bytes 589832 | tf_op jit(solution)/shard_map/ppermute | solution.py:11
  104.9 30.1 %all-to-all-start.1 = ((bf16[8,16,2048]{2,1,0:T(8,128)(2,1)}), bf16[8,16,2048]{2,1,0:T(8,128)(2,1)S(1)}, u32[]{:S(2)}, u32[]{:S(2)}) async-start(bf16[8,16,2048]{2,1,0:T(8,128)(2,1)} %broadcast_in_dim.12), calls=%async_computation.1 | async-start | bytes 1048576 | tf_op jit(solution)/shard_map/all_to_all | solution.py:23
  110.3 11.2 %collective-permute-start.13 = (bf16[256,384]{1,0:T(8,128)(2,1)S(1)}, bf16[256,384]{1,0:T(8,128)(2,1)S(1)}, u32[]{:S(2)}, u32[]{:S(2)}) collective-permute-start(bf16[256,384]{1,0:T(8,128)(2,1)S(1)} %collective-permute-done.12.refs_7_), channel_id=1, source_target_pairs={{0,448},{8,456},{16,464},{24,472},{32,480},{40,488},{48,496},{56,5... | collective-permute-start | bytes 589832 | tf_op jit(solution)/shard_map/ppermute | solution.py:11
  115.2 11.5 %collective-permute-start.10 = (bf16[256,384]{1,0:T(8,128)(2,1)S(1)}, bf16[256,384]{1,0:T(8,128)(2,1)S(1)}, u32[]{:S(2)}, u32[]{:S(2)}) collective-permute-start(bf16[256,384]{1,0:T(8,128)(2,1)S(1)} %collective-permute-done.9.refs_2_), channel_id=1, source_target_pairs={{0,64},{8,72},{16,80},{24,88},{32,96},{40,104},{48,112},{56,120},{... | collective-permute-start | bytes 589832 | tf_op jit(solution)/shard_map/ppermute | solution.py:11
  121.5 8.5 %collective-permute-start.14 = (bf16[256,384]{1,0:T(8,128)(2,1)S(1)}, bf16[256,384]{1,0:T(8,128)(2,1)S(1)}, u32[]{:S(2)}, u32[]{:S(2)}) collective-permute-start(bf16[256,384]{1,0:T(8,128)(2,1)S(1)} %collective-permute-done.13.refs_6_), channel_id=1, source_target_pairs={{0,448},{8,456},{16,464},{24,472},{32,480},{40,488},{48,496},{56,5... | collective-permute-start | bytes 589832 | tf_op jit(solution)/shard_map/ppermute | solution.py:11
  126.7 8.4 %collective-permute-start.11 = (bf16[256,384]{1,0:T(8,128)(2,1)S(1)}, bf16[256,384]{1,0:T(8,128)(2,1)S(1)}, u32[]{:S(2)}, u32[]{:S(2)}) collective-permute-start(bf16[256,384]{1,0:T(8,128)(2,1)S(1)} %collective-permute-done.10.refs_3_), channel_id=1, source_target_pairs={{0,64},{8,72},{16,80},{24,88},{32,96},{40,104},{48,112},{56,120},{... | collective-permute-start | bytes 589832 | tf_op jit(solution)/shard_map/ppermute | solution.py:11
Sparse Core Ops, SparseCore 0:
  10.3 111.0 all-gather.1

commit v8 on v7

--- a/solution.py
+++ b/solution.py
@@ -162,24 +162,18 @@
     )(x, gate_low, weights)
 
 
-def side_kernel(start, x, *refs):
+def side_kernel(places, x, *refs):
     blocks, out = refs[:-1], refs[-1]
     step = blocks[0].shape[0]
-    width = x.shape[1]
-    turned = pltpu.roll(x[...].astype(jnp.float32), (width - start[0]) & (width - 1), 1)
-    turned = turned.astype(jnp.bfloat16)
     acc = None
-    for i in range(len(blocks)):
-        term = jnp.dot(
-            turned[:, i * step : (i + 1) * step],
-            blocks[len(blocks) - 1 - i][...],
-            preferred_element_type=jnp.float32,
-        )
+    for k in range(len(blocks)):
+        part = x[:, pl.ds(pl.multiple_of(places[k] * step, step), step)]
+        term = jnp.dot(part, blocks[k][...], preferred_element_type=jnp.float32)
         acc = term if acc is None else acc + term
     out[...] = acc
 
 
-def side(x, blocks, start):
+def side(x, blocks, places):
     vmem = pl.BlockSpec(memory_space=pltpu.VMEM)
     return pl.pallas_call(
         side_kernel,
@@ -188,7 +182,7 @@
         out_specs=vmem,
         compiler_params=pltpu.CompilerParams(vmem_limit_bytes=12 << 20),
         name="side",
-    )(start, x, *blocks)
+    )(places, x, *blocks)
 
 
 def on_device(
@@ -211,28 +205,26 @@
     weights = lax.all_gather(packed, "sp", axis=0, tiled=True)
 
     docs = jnp.pad(doc_ids.astype(jnp.bfloat16)[None], ((0, 15), (0, 2 * keys.shape[1] - rows)))
-    shard = jnp.pad(gate_weight[:, :low], ((0, 0), (0, 2 * keys.shape[1] - low)))
-    tall = rows + docs.shape[0]
     own = jnp.concatenate([jnp.concatenate([keys, values], axis=1), docs])
-    both = jnp.concatenate([own, shard])
-    blocks = {0: both}
-    blocks[1] = shifted(both, 1)
-    blocks[7] = shifted(own, 7)
-    after = shifted(shard, -1)
-    blocks[2] = shifted(blocks[1], 1)
-    blocks[6] = shifted(jnp.concatenate([blocks[7], after]), -1)
-    blocks[3] = shifted(blocks[2], 1)
-    blocks[5] = shifted(blocks[6], -1)
-    blocks[4] = shifted(blocks[3], 1)
-    near = [blocks[k][tall:, :low] for k in (4, 3, 2, 1)]
-    near += [shard[:, :low], after[:, :low]] + [blocks[k][tall:, :low] for k in (6, 5)]
-    ring, rings = len(near), lax.axis_size("sp") // len(near)
-    sides = {0: jnp.concatenate(near)}
+    ring = 8
+    rings = lax.axis_size("sp") // ring
+    blocks, sides = {0: own}, {}
+    blocks[1], blocks[7] = shifted(own, 1), shifted(own, 7)
+    shard = gate_weight[:, :low]
+    copies = jnp.broadcast_to(shard, (ring, *shard.shape))
+    groups = [list(range(i * ring, (i + 1) * ring)) for i in range(rings)]
+    tiles = lax.all_to_all(copies, "sp", 0, 0, tiled=True, axis_index_groups=groups)
+    sides[0] = tiles.reshape(ring * shard.shape[0], low)
     for k in range(1, rings // 2 + 1):
         sides[k] = shifted(sides[k - 1], ring)
         if k < rings // 2:
             sides[rings - k] = shifted(sides[(rings - k + 1) % rings], -ring)
-    start = ((lax.axis_index("sp") + ring // 2) & (ring * rings - 1)) * near[0].shape[0]
+    for k in range(2, 5):
+        blocks[k] = shifted(blocks[k - 1], 1)
+        if k < 4:
+            blocks[8 - k] = shifted(blocks[9 - k], -1)
+    back = jnp.arange(rings, dtype=jnp.int32)
+    places = (lax.axis_index("sp") // ring + rings - back) & (rings - 1)
     attended = attention(queries, [blocks[b] for b in range(8)], score_offset)
 
     mixed_attn = summed_for_owner(
@@ -243,7 +235,7 @@
         stream * lax.rsqrt(jnp.mean(stream * stream, axis=1, keepdims=True) + 1e-06) * norm_gain
     ).astype(jnp.bfloat16)
     span_rows = from_everyone(normed).reshape(rows, -1)
-    gate_low = side(span_rows, [sides[k] for k in range(rings)], start[None])
+    gate_low = side(span_rows, [sides[k] for k in range(rings)], places)
     feed = summed_for_owner(ffn(span_rows, gate_low, weights, units))
     return (stream + feed).astype(jnp.bfloat16)
 

time: 164 us -> 159 us (0.970)
  starting transfers between devices: 73.9 us -> 70.8 us
    ppermute x15 -> x14, starting transfers between devices: 58.2 us -> 50.9 us  [shifted(): lax.ppermute(block, 'sp', [(i, (i + by) % spans) for i in range(spans)])]
    all_to_all x0 -> x1, starting transfers between devices: none -> 3.39 us  [on_device(): lax.all_to_all(copies, 'sp', 0, 0, tiled=True, axis_index_groups=groups)]
    ppermute x15 -> x14, waiting for transfers between devices: 38 us -> 36.4 us  [shifted(): lax.ppermute(block, 'sp', [(i, (i + by) % spans) for i in range(spans)])]
where the time goes in v8:
time: 159 us; the launch traced here: 158 us
  starting transfers between devices  70.8 us (45%)
  waiting for transfers between devices  36.4 us (23%)
  blocking collectives  15.3 us (10%)
  between operations  13.6 us (9%)
  Pallas kernels  10.7 us (7%)
  other arithmetic  5.77 us (4%)
  local copies, waits for them, and re-layouts  3.93 us (2%)
    ppermute x14, starting transfers between devices, shifted(): lax.ppermute(block, 'sp', [(i, (i + by) % spans) for i in range(spans)])  50.9 us
    ppermute x14, waiting for transfers between devices, shifted(): lax.ppermute(block, 'sp', [(i, (i + by) % spans) for i in range(spans)])  36.4 us
    all_to_all x1, blocking collectives, summed_for_owner(): tiles = lax.all_to_all(tiles, 'tp', 0, 0, tiled=True)  15.3 us
    all_to_all x1, starting transfers between devices, summed_for_owner(): tiles = lax.all_to_all(tiles, 'tp', 0, 0, tiled=True)  11.2 us
    all_to_all x1, starting transfers between devices, from_everyone(): return lax.all_to_all(copies, 'tp', split_axis=0, concat_axis=0, tiled=True)  5.3 us
    pallas_call x1, Pallas kernels, attention(): pl.pallas_call(body, out_shape=jax.ShapeDtypeStruct((rows, width), jnp.bf...  5.26 us
    pallas_call x1, Pallas kernels, ffn(): pl.pallas_call(body, out_shape=jax.ShapeDtypeStruct(x.shape, jnp.bfloat16...  4.42 us
    all_to_all x1, starting transfers between devices, on_device(): lax.all_to_all(copies, 'sp', 0, 0, tiled=True, axis_index_groups=groups)  3.39 us
  transfers between devices with their start and end apart: 18, of which 9 were waited for; matrix products, arithmetic and copies ran while one was open for 4% of the time, Pallas kernels for 4%

profile of v8, /device:TPU:1, one launch (start us, length us, event | category | flops | bytes accessed | tf_op | source)
XLA Modules:
  0.0 157.6 jit_solution(18190332094356548204)
XLA Ops:
  10.4 4.0 %collective-permute-start = (bf16[144,512]{1,0:T(8,128)(2,1)S(1)}, bf16[144,512]{1,0:T(8,128)(2,1)S(1)}, u32[]{:S(2)}, u32[]{:S(2)}) collective-permute-start(bf16[144,512]{1,0:T(8,128)(2,1)S(1)} %fusion.1.refs_2_), channel_id=1, source_target_pairs={{0,8},{8,16},{16,24},{24,32},{32,40},{40,48},{48,56},{56,64},{64,7... | collective-permute-start | bytes 442376 | tf_op jit(solution)/shard_map/ppermute | solution.py:11
  14.5 5.1 %collective-permute-start.4 = (bf16[144,512]{1,0:T(8,128)(2,1)S(1)}, bf16[144,512]{1,0:T(8,128)(2,1)S(1)}, u32[]{:S(2)}, u32[]{:S(2)}) collective-permute-start(bf16[144,512]{1,0:T(8,128)(2,1)S(1)} %fusion.1.refs_2_), channel_id=1, source_target_pairs={{0,56},{8,64},{16,72},{24,80},{32,88},{40,96},{48,104},{56,112},{6... | collective-permute-start | bytes 442376 | tf_op jit(solution)/shard_map/ppermute | solution.py:11
  19.6 9.5 %collective-permute-done.refs_3_ = bf16[144,512]{1,0:T(8,128)(2,1)S(1)} collective-permute-done((bf16[144,512]{1,0:T(8,128)(2,1)S(1)}, bf16[144,512]{1,0:T(8,128)(2,1)S(1)}, u32[]{:S(2)}, u32[]{:S(2)}) %collective-permute-start) | collective-permute-done | bytes 147488 | tf_op jit(solution)/shard_map/ppermute | solution.py:11
  29.1 1.9 %collective-permute-start.1 = (bf16[144,512]{1,0:T(8,128)(2,1)S(1)}, bf16[144,512]{1,0:T(8,128)(2,1)S(1)}, u32[]{:S(2)}, u32[]{:S(2)}) collective-permute-start(bf16[144,512]{1,0:T(8,128)(2,1)S(1)} %collective-permute-done.refs_3_), channel_id=1, source_target_pairs={{0,8},{8,16},{16,24},{24,32},{32,40},{40,48},{48,56},{56,64},{64,7... | collective-permute-start | bytes 442376 | tf_op jit(solution)/shard_map/ppermute | solution.py:11
  31.0 6.7 %collective-permute-start.5 = (bf16[144,512]{1,0:T(8,128)(2,1)S(1)}, bf16[144,512]{1,0:T(8,128)(2,1)S(1)}, u32[]{:S(2)}, u32[]{:S(2)}) collective-permute-start(bf16[144,512]{1,0:T(8,128)(2,1)S(1)} %collective-permute-done.4.refs_9_), channel_id=1, source_target_pairs={{0,504},{8,0},{16,8},{24,16},{32,24},{40,32},{48,40},{56,48},{64,5... | collective-permute-start | bytes 442376 | tf_op jit(solution)/shard_map/ppermute | solution.py:11
  38.4 1.9 %collective-permute-start.2 = (bf16[144,512]{1,0:T(8,128)(2,1)S(1)}, bf16[144,512]{1,0:T(8,128)(2,1)S(1)}, u32[]{:S(2)}, u32[]{:S(2)}) collective-permute-start(bf16[144,512]{1,0:T(8,128)(2,1)S(1)} %collective-permute-done.1.refs_4_), channel_id=1, source_target_pairs={{0,8},{8,16},{16,24},{24,32},{32,40},{40,48},{48,56},{56,64},{64,7... | collective-permute-start | bytes 442376 | tf_op jit(solution)/shard_map/ppermute | solution.py:11
  40.3 6.8 %collective-permute-start.6 = (bf16[144,512]{1,0:T(8,128)(2,1)S(1)}, bf16[144,512]{1,0:T(8,128)(2,1)S(1)}, u32[]{:S(2)}, u32[]{:S(2)}) collective-permute-start(bf16[144,512]{1,0:T(8,128)(2,1)S(1)} %collective-permute-done.5.refs_8_), channel_id=1, source_target_pairs={{0,504},{8,0},{16,8},{24,16},{32,24},{40,32},{48,40},{56,48},{64,5... | collective-permute-start | bytes 442376 | tf_op jit(solution)/shard_map/ppermute | solution.py:11
  48.1 1.9 %collective-permute-start.3 = (bf16[144,512]{1,0:T(8,128)(2,1)S(1)}, bf16[144,512]{1,0:T(8,128)(2,1)S(1)}, u32[]{:S(2)}, u32[]{:S(2)}) collective-permute-start(bf16[144,512]{1,0:T(8,128)(2,1)S(1)} %collective-permute-done.2.refs_5_), channel_id=1, source_target_pairs={{0,8},{8,16},{16,24},{24,32},{32,40},{40,48},{48,56},{56,64},{64,7... | collective-permute-start | bytes 442376 | tf_op jit(solution)/shard_map/ppermute | solution.py:11
  50.7 3.4 %all-to-all-start.2 = ((bf16[8,32,384]{2,1,0:T(8,128)(2,1)}), bf16[8,32,384]{2,1,0:T(8,128)(2,1)S(1)}, u32[]{:S(2)}, u32[]{:S(2)}) async-start(bf16[8,32,384]{2,1,0:T(8,128)(2,1)} %broadcast_in_dim.13), calls=%async_computation.2 | async-start | bytes 393216 | tf_op jit(solution)/shard_map/all_to_all | solution.py:216
  54.2 3.8 %collective-permute-done.3.refs_6_ = bf16[144,512]{1,0:T(8,128)(2,1)S(1)} collective-permute-done((bf16[144,512]{1,0:T(8,128)(2,1)S(1)}, bf16[144,512]{1,0:T(8,128)(2,1)S(1)}, u32[]{:S(2)}, u32[]{:S(2)}) %collective-permute-start.3) | collective-permute-done | bytes 147488 | tf_op jit(solution)/shard_map/ppermute | solution.py:11
  59.4 5.3 %attention.1 = bf16[128,256]{1,0:T(8,128)(2,1)S(1)} custom-call(f32[4]{0:T(128)S(1)} %copy-done.2, bf16[128,256]{1,0:T(8,128)(2,1)S(1)} %copy-done.1, bf16[144,512]{1,0:T(8,128)(2,1)S(1)} %fusion.1.refs_2_, bf16[144,512]{1,0:T(8,128)(2,1)S(1)} %collective-permute-done.refs_3_, bf16[144,512]{1,0:T(8,128)(2,1)S(1)} %collective-permute-done.1.refs_4_, ...), custom_call_target="tpu_custom_call" | custom-call | tf_op jit(solution)/shard_map/attention/pallas_call | solution.py:76
  65.8 11.2 %all-to-all-start = ((bf16[8,16,2048]{2,1,0:T(8,128)(2,1)}), bf16[8,16,2048]{2,1,0:T(8,128)(2,1)S(1)}, u32[]{:S(2)}, u32[]{:S(2)}) async-start(bf16[8,16,2048]{2,1,0:T(8,128)(2,1)} %bitcast.1), calls=%async_computation | async-start | bytes 1048576 | tf_op jit(solution)/shard_map/all_to_all | solution.py:17
  77.0 2.0 %collective-permute-start.7 = (bf16[256,384]{1,0:T(8,128)(2,1)S(1)}, bf16[256,384]{1,0:T(8,128)(2,1)S(1)}, u32[]{:S(2)}, u32[]{:S(2)}) collective-permute-start(bf16[256,384]{1,0:T(8,128)(2,1)S(1)} %bitcast.12), channel_id=1, source_target_pairs={{0,64},{8,72},{16,80},{24,88},{32,96},{40,104},{48,112},{56,120},{... | collective-permute-start | bytes 589832 | tf_op jit(solution)/shard_map/ppermute | solution.py:11
  79.1 4.6 %collective-permute-start.11 = (bf16[256,384]{1,0:T(8,128)(2,1)S(1)}, bf16[256,384]{1,0:T(8,128)(2,1)S(1)}, u32[]{:S(2)}, u32[]{:S(2)}) collective-permute-start(bf16[256,384]{1,0:T(8,128)(2,1)S(1)} %bitcast.13), channel_id=1, source_target_pairs={{0,448},{8,456},{16,464},{24,472},{32,480},{40,488},{48,496},{56,5... | collective-permute-start | bytes 589832 | tf_op jit(solution)/shard_map/ppermute | solution.py:11
  83.7 7.8 %collective-permute-done.7.refs_1_ = bf16[256,384]{1,0:T(8,128)(2,1)S(1)} collective-permute-done((bf16[256,384]{1,0:T(8,128)(2,1)S(1)}, bf16[256,384]{1,0:T(8,128)(2,1)S(1)}, u32[]{:S(2)}, u32[]{:S(2)}) %collective-permute-start.7) | collective-permute-done | bytes 196640 | tf_op jit(solution)/shard_map/ppermute | solution.py:11
  96.4 5.3 %all-to-all-start.1 = ((bf16[8,16,2048]{2,1,0:T(8,128)(2,1)}), bf16[8,16,2048]{2,1,0:T(8,128)(2,1)S(1)}, u32[]{:S(2)}, u32[]{:S(2)}) async-start(bf16[8,16,2048]{2,1,0:T(8,128)(2,1)} %broadcast_in_dim.12), calls=%async_computation.1 | async-start | bytes 1048576 | tf_op jit(solution)/shard_map/all_to_all | solution.py:23
  101.7 4.8 %collective-permute-start.12 = (bf16[256,384]{1,0:T(8,128)(2,1)S(1)}, bf16[256,384]{1,0:T(8,128)(2,1)S(1)}, u32[]{:S(2)}, u32[]{:S(2)}) collective-permute-start(bf16[256,384]{1,0:T(8,128)(2,1)S(1)} %collective-permute-done.11.refs_7_), channel_id=1, source_target_pairs={{0,448},{8,456},{16,464},{24,472},{32,480},{40,488},{48,496},{56,5... | collective-permute-start | bytes 589832 | tf_op jit(solution)/shard_map/ppermute | solution.py:11
  106.5 1.9 %collective-permute-start.9 = (bf16[256,384]{1,0:T(8,128)(2,1)S(1)}, bf16[256,384]{1,0:T(8,128)(2,1)S(1)}, u32[]{:S(2)}, u32[]{:S(2)}) collective-permute-start(bf16[256,384]{1,0:T(8,128)(2,1)S(1)} %collective-permute-done.8.refs_2_), channel_id=1, source_target_pairs={{0,64},{8,72},{16,80},{24,88},{32,96},{40,104},{48,112},{56,120},{... | collective-permute-start | bytes 589832 | tf_op jit(solution)/shard_map/ppermute | solution.py:11
  108.4 6.1 %collective-permute-done.12.refs_6_ = bf16[256,384]{1,0:T(8,128)(2,1)S(1)} collective-permute-done((bf16[256,384]{1,0:T(8,128)(2,1)S(1)}, bf16[256,384]{1,0:T(8,128)(2,1)S(1)}, u32[]{:S(2)}, u32[]{:S(2)}) %collective-permute-start.12) | collective-permute-done | bytes 196640 | tf_op jit(solution)/shard_map/ppermute | solution.py:11
  114.5 5.4 %collective-permute-start.13 = (bf16[256,384]{1,0:T(8,128)(2,1)S(1)}, bf16[256,384]{1,0:T(8,128)(2,1)S(1)}, u32[]{:S(2)}, u32[]{:S(2)}) collective-permute-start(bf16[256,384]{1,0:T(8,128)(2,1)S(1)} %collective-permute-done.12.refs_6_), channel_id=1, source_target_pairs={{0,448},{8,456},{16,464},{24,472},{32,480},{40,488},{48,496},{56,5... | collective-permute-start | bytes 589832 | tf_op jit(solution)/shard_map/ppermute | solution.py:11
  122.7 2.8 %collective-permute-done.13.refs_5_ = bf16[256,384]{1,0:T(8,128)(2,1)S(1)} collective-permute-done((bf16[256,384]{1,0:T(8,128)(2,1)S(1)}, bf16[256,384]{1,0:T(8,128)(2,1)S(1)}, u32[]{:S(2)}, u32[]{:S(2)}) %collective-permute-start.13) | collective-permute-done | bytes 196640 | tf_op jit(solution)/shard_map/ppermute | solution.py:11
  125.5 3.8 %collective-permute-done.10.refs_4_ = bf16[256,384]{1,0:T(8,128)(2,1)S(1)} collective-permute-done((bf16[256,384]{1,0:T(8,128)(2,1)S(1)}, bf16[256,384]{1,0:T(8,128)(2,1)S(1)}, u32[]{:S(2)}, u32[]{:S(2)}) %collective-permute-start.10) | collective-permute-done | bytes 196640 | tf_op jit(solution)/shard_map/ppermute | solution.py:11
  130.3 4.4 %ffn.1 = bf16[128,2048]{1,0:T(8,128)(2,1)S(1)} custom-call(bf16[128,2048]{1,0:T(8,128)(2,1)S(1)} %bitcast.10, f32[128,384]{1,0:T(8,128)S(1)} %side.1.refs_1_, bf16[2048,1920]{1,0:T(8,128)(2,1)} %all-gather.2.cloned.1.call-done.refs_2_), custom_call_target="tpu_custom_call" | custom-call | tf_op jit(solution)/shard_map/ffn/pallas_call | solution.py:150
  134.7 15.3 %all_to_all.20 = bf16[8,16,2048]{2,1,0:T(8,128)(2,1)S(1)} all-to-all(bf16[8,16,2048]{2,1,0:T(8,128)(2,1)S(1)} %bitcast.11), channel_id=1, replica_groups=mesh['sp'=64,'tp'=8] {'tp'}, dimensions={0} | all-to-all | bytes 1048576 | tf_op jit(solution)/shard_map/all_to_all | solution.py:17
  (39 shorter events, 18.3 us)
Async XLA Ops:
  6.5 58.1 %copy-start = (bf16[256,2048]{1,0:T(8,128)(2,1)S(1)}, bf16[256,2048]{1,0:T(8,128)(2,1)}, u32[]{:S(2)}) copy-start(bf16[256,2048]{1,0:T(8,128)(2,1)} %param.17) | copy-start | bytes 3145732
  6.5 123.8 %all-gather.2.cloned.1.call-start = ((), (), s32[]{:S(2)}) async-start(), calls=%async_computation.4 | async-start | bytes 7987200 | tf_op jit(solution)/shard_map/all_gather | solution.py:205
  10.4 18.6 %collective-permute-start = (bf16[144,512]{1,0:T(8,128)(2,1)S(1)}, bf16[144,512]{1,0:T(8,128)(2,1)S(1)}, u32[]{:S(2)}, u32[]{:S(2)}) collective-permute-start(bf16[144,512]{1,0:T(8,128)(2,1)S(1)} %fusion.1.refs_2_), channel_id=1, source_target_pairs={{0,8},{8,16},{16,24},{24,32},{32,40},{40,48},{48,56},{56,64},{64,7... | collective-permute-start | bytes 442376 | tf_op jit(solution)/shard_map/ppermute | solution.py:11
  14.5 16.6 %collective-permute-start.4 = (bf16[144,512]{1,0:T(8,128)(2,1)S(1)}, bf16[144,512]{1,0:T(8,128)(2,1)S(1)}, u32[]{:S(2)}, u32[]{:S(2)}) collective-permute-start(bf16[144,512]{1,0:T(8,128)(2,1)S(1)} %fusion.1.refs_2_), channel_id=1, source_target_pairs={{0,56},{8,64},{16,72},{24,80},{32,88},{40,96},{48,104},{56,112},{6... | collective-permute-start | bytes 442376 | tf_op jit(solution)/shard_map/ppermute | solution.py:11
  29.1 9.3 %collective-permute-start.1 = (bf16[144,512]{1,0:T(8,128)(2,1)S(1)}, bf16[144,512]{1,0:T(8,128)(2,1)S(1)}, u32[]{:S(2)}, u32[]{:S(2)}) collective-permute-start(bf16[144,512]{1,0:T(8,128)(2,1)S(1)} %collective-permute-done.refs_3_), channel_id=1, source_target_pairs={{0,8},{8,16},{16,24},{24,32},{32,40},{40,48},{48,56},{56,64},{64,7... | collective-permute-start | bytes 442376 | tf_op jit(solution)/shard_map/ppermute | solution.py:11
  31.0 9.3 %collective-permute-start.5 = (bf16[144,512]{1,0:T(8,128)(2,1)S(1)}, bf16[144,512]{1,0:T(8,128)(2,1)S(1)}, u32[]{:S(2)}, u32[]{:S(2)}) collective-permute-start(bf16[144,512]{1,0:T(8,128)(2,1)S(1)} %collective-permute-done.4.refs_9_), channel_id=1, source_target_pairs={{0,504},{8,0},{16,8},{24,16},{32,24},{40,32},{48,40},{56,48},{64,5... | collective-permute-start | bytes 442376 | tf_op jit(solution)/shard_map/ppermute | solution.py:11
  38.4 9.8 %collective-permute-start.2 = (bf16[144,512]{1,0:T(8,128)(2,1)S(1)}, bf16[144,512]{1,0:T(8,128)(2,1)S(1)}, u32[]{:S(2)}, u32[]{:S(2)}) collective-permute-start(bf16[144,512]{1,0:T(8,128)(2,1)S(1)} %collective-permute-done.1.refs_4_), channel_id=1, source_target_pairs={{0,8},{8,16},{16,24},{24,32},{32,40},{40,48},{48,56},{56,64},{64,7... | collective-permute-start | bytes 442376 | tf_op jit(solution)/shard_map/ppermute | solution.py:11
  40.3 13.9 %collective-permute-start.6 = (bf16[144,512]{1,0:T(8,128)(2,1)S(1)}, bf16[144,512]{1,0:T(8,128)(2,1)S(1)}, u32[]{:S(2)}, u32[]{:S(2)}) collective-permute-start(bf16[144,512]{1,0:T(8,128)(2,1)S(1)} %collective-permute-done.5.refs_8_), channel_id=1, source_target_pairs={{0,504},{8,0},{16,8},{24,16},{32,24},{40,32},{48,40},{56,48},{64,5... | collective-permute-start | bytes 442376 | tf_op jit(solution)/shard_map/ppermute | solution.py:11
  48.1 9.8 %collective-permute-start.3 = (bf16[144,512]{1,0:T(8,128)(2,1)S(1)}, bf16[144,512]{1,0:T(8,128)(2,1)S(1)}, u32[]{:S(2)}, u32[]{:S(2)}) collective-permute-start(bf16[144,512]{1,0:T(8,128)(2,1)S(1)} %collective-permute-done.2.refs_5_), channel_id=1, source_target_pairs={{0,8},{8,16},{16,24},{24,32},{32,40},{40,48},{48,56},{56,64},{64,7... | collective-permute-start | bytes 442376 | tf_op jit(solution)/shard_map/ppermute | solution.py:11
  50.7 15.1 %all-to-all-start.2 = ((bf16[8,32,384]{2,1,0:T(8,128)(2,1)}), bf16[8,32,384]{2,1,0:T(8,128)(2,1)S(1)}, u32[]{:S(2)}, u32[]{:S(2)}) async-start(bf16[8,32,384]{2,1,0:T(8,128)(2,1)} %broadcast_in_dim.13), calls=%async_computation.2 | async-start | bytes 393216 | tf_op jit(solution)/shard_map/all_to_all | solution.py:216
  57.9 0.8 copy-start.1
  58.8 0.7 copy-start.2
  65.8 27.6 %all-to-all-start = ((bf16[8,16,2048]{2,1,0:T(8,128)(2,1)}), bf16[8,16,2048]{2,1,0:T(8,128)(2,1)S(1)}, u32[]{:S(2)}, u32[]{:S(2)}) async-start(bf16[8,16,2048]{2,1,0:T(8,128)(2,1)} %bitcast.1), calls=%async_computation | async-start | bytes 1048576 | tf_op jit(solution)/shard_map/all_to_all | solution.py:17
  77.0 73.1 %copy-start.3 = (bf16[16,2048]{1,0:T(8,128)(2,1)S(1)}, bf16[16,2048]{1,0:T(8,128)(2,1)}, u32[]{:S(2)}) copy-start(bf16[16,2048]{1,0:T(8,128)(2,1)} %param.11) | copy-start | bytes 196612
  77.0 14.5 %collective-permute-start.7 = (bf16[256,384]{1,0:T(8,128)(2,1)S(1)}, bf16[256,384]{1,0:T(8,128)(2,1)S(1)}, u32[]{:S(2)}, u32[]{:S(2)}) collective-permute-start(bf16[256,384]{1,0:T(8,128)(2,1)S(1)} %bitcast.12), channel_id=1, source_target_pairs={{0,64},{8,72},{16,80},{24,88},{32,96},{40,104},{48,112},{56,120},{... | collective-permute-start | bytes 589832 | tf_op jit(solution)/shard_map/ppermute | solution.py:11
  79.1 22.6 %collective-permute-start.11 = (bf16[256,384]{1,0:T(8,128)(2,1)S(1)}, bf16[256,384]{1,0:T(8,128)(2,1)S(1)}, u32[]{:S(2)}, u32[]{:S(2)}) collective-permute-start(bf16[256,384]{1,0:T(8,128)(2,1)S(1)} %bitcast.13), channel_id=1, source_target_pairs={{0,448},{8,456},{16,464},{24,472},{32,480},{40,488},{48,496},{56,5... | collective-permute-start | bytes 589832 | tf_op jit(solution)/shard_map/ppermute | solution.py:11
  91.5 15.0 %collective-permute-start.8 = (bf16[256,384]{1,0:T(8,128)(2,1)S(1)}, bf16[256,384]{1,0:T(8,128)(2,1)S(1)}, u32[]{:S(2)}, u32[]{:S(2)}) collective-permute-start(bf16[256,384]{1,0:T(8,128)(2,1)S(1)} %collective-permute-done.7.refs_1_), channel_id=1, source_target_pairs={{0,64},{8,72},{16,80},{24,88},{32,96},{40,104},{48,112},{56,120},{... | collective-permute-start | bytes 589832 | tf_op jit(solution)/shard_map/ppermute | solution.py:11
  96.4 32.9 %all-to-all-start.1 = ((bf16[8,16,2048]{2,1,0:T(8,128)(2,1)}), bf16[8,16,2048]{2,1,0:T(8,128)(2,1)S(1)}, u32[]{:S(2)}, u32[]{:S(2)}) async-start(bf16[8,16,2048]{2,1,0:T(8,128)(2,1)} %broadcast_in_dim.12), calls=%async_computation.1 | async-start | bytes 1048576 | tf_op jit(solution)/shard_map/all_to_all | solution.py:23
  101.7 12.9 %collective-permute-start.12 = (bf16[256,384]{1,0:T(8,128)(2,1)S(1)}, bf16[256,384]{1,0:T(8,128)(2,1)S(1)}, u32[]{:S(2)}, u32[]{:S(2)}) collective-permute-start(bf16[256,384]{1,0:T(8,128)(2,1)S(1)} %collective-permute-done.11.refs_7_), channel_id=1, source_target_pairs={{0,448},{8,456},{16,464},{24,472},{32,480},{40,488},{48,496},{56,5... | collective-permute-start | bytes 589832 | tf_op jit(solution)/shard_map/ppermute | solution.py:11
  106.5 14.2 %collective-permute-start.9 = (bf16[256,384]{1,0:T(8,128)(2,1)S(1)}, bf16[256,384]{1,0:T(8,128)(2,1)S(1)}, u32[]{:S(2)}, u32[]{:S(2)}) collective-permute-start(bf16[256,384]{1,0:T(8,128)(2,1)S(1)} %collective-permute-done.8.refs_2_), channel_id=1, source_target_pairs={{0,64},{8,72},{16,80},{24,88},{32,96},{40,104},{48,112},{56,120},{... | collective-permute-start | bytes 589832 | tf_op jit(solution)/shard_map/ppermute | solution.py:11
  114.5 11.0 %collective-permute-start.13 = (bf16[256,384]{1,0:T(8,128)(2,1)S(1)}, bf16[256,384]{1,0:T(8,128)(2,1)S(1)}, u32[]{:S(2)}, u32[]{:S(2)}) collective-permute-start(bf16[256,384]{1,0:T(8,128)(2,1)S(1)} %collective-permute-done.12.refs_6_), channel_id=1, source_target_pairs={{0,448},{8,456},{16,464},{24,472},{32,480},{40,488},{48,496},{56,5... | collective-permute-start | bytes 589832 | tf_op jit(solution)/shard_map/ppermute | solution.py:11
  120.7 8.5 %collective-permute-start.10 = (bf16[256,384]{1,0:T(8,128)(2,1)S(1)}, bf16[256,384]{1,0:T(8,128)(2,1)S(1)}, u32[]{:S(2)}, u32[]{:S(2)}) collective-permute-start(bf16[256,384]{1,0:T(8,128)(2,1)S(1)} %collective-permute-done.9.refs_3_), channel_id=1, source_target_pairs={{0,64},{8,72},{16,80},{24,88},{32,96},{40,104},{48,112},{56,120},{... | collective-permute-start | bytes 589832 | tf_op jit(solution)/shard_map/ppermute | solution.py:11
Sparse Core Ops, SparseCore 0:
  10.3 115.2 all-gather.1

commit v9 on v6

--- a/solution.py
+++ b/solution.py
@@ -142,7 +142,7 @@
     vmem = pl.BlockSpec(memory_space=pltpu.VMEM)
 
     def body(*refs):
-        ffn_kernel(cuts, 3, *refs)
+        ffn_kernel(cuts, 4, *refs)
 
     return pl.pallas_call(
         body,
@@ -177,7 +177,7 @@
     packed = jnp.concatenate([gate_weight, up_weight, down_weight.T], axis=1)
     weights = lax.all_gather(packed, "sp", axis=0, tiled=True)
 
-    docs = jnp.pad(doc_ids.astype(jnp.bfloat16)[None], ((0, 15), (0, 2 * keys.shape[1] - rows)))
+    docs = jnp.pad(doc_ids.astype(jnp.bfloat16)[None], ((0, 7), (0, 2 * keys.shape[1] - rows)))
     own = jnp.concatenate([jnp.concatenate([keys, values], axis=1), docs], axis=0)
     blocks = {0: own}
     blocks[7] = shifted(own, 7)

time: 147 us -> 147 us (level)
  no operation moved by 1% of the time
where the time goes in v9:
time: 147 us
  blocking collectives  46.7 us (32%)
  waiting for transfers between devices  40.1 us (27%)
  starting transfers between devices  28.4 us (19%)
  between operations  13.5 us (9%)
  Pallas kernels  10 us (7%)
  other arithmetic  5.9 us (4%)
  local copies, waits for them, and re-layouts  1.55 us (1%)
    all_to_all x2, blocking collectives, summed_for_owner(): tiles = lax.all_to_all(tiles, 'tp', 0, 0, tiled=True)  33.9 us
    ppermute x7, starting transfers between devices, shifted(): lax.ppermute(block, 'sp', [(i, (i + by) % spans) for i in range(spans)])  28.4 us
    all_gather x1, waiting for transfers between devices, on_device(): weights = lax.all_gather(packed, 'sp', axis=0, tiled=True)  22.1 us
    ppermute x7, waiting for transfers between devices, shifted(): lax.ppermute(block, 'sp', [(i, (i + by) % spans) for i in range(spans)])  17.9 us
    all_to_all x1, blocking collectives, from_everyone(): return lax.all_to_all(copies, 'tp', split_axis=0, concat_axis=0, tiled=True)  12.8 us
    pallas_call x1, Pallas kernels, attention(): pl.pallas_call(body, out_shape=jax.ShapeDtypeStruct((rows, width), jnp.bf...  5.3 us
    pallas_call x1, Pallas kernels, ffn(): pl.pallas_call(body, out_shape=jax.ShapeDtypeStruct(x.shape, jnp.bfloat16...  4.71 us
  transfers between devices with their start and end apart: 8, of which 5 were waited for; matrix products, arithmetic and copies ran while one was open for 3% of the time, Pallas kernels for 4%

profile of v9, /device:TPU:1, one launch (start us, length us, event | category | flops | bytes accessed | tf_op | source)
XLA Modules:
  0.0 146.5 jit_solution(4111221918250704395)
XLA Ops:
  6.5 1.6 %pad_maximum_fusion = bf16[32,2304]{1,0:T(8,128)(2,1)} fusion(bf16[32,768]{1,0:T(8,128)(2,1)} %bitcast.11, bf16[32,768]{1,0:T(8,128)(2,1)} %param.20, bf16[32,768]{1,0:T(8,128)(2,1)} %param.19), kind=kLoop, calls=%fused_computation.5 | loop fusion | flops 442368 | bytes 294912 | tf_op jit(solution)/shard_map/concatenate | solution.py:177
  8.2 0.7 convert_bitcast_fusion
  8.8 0.9 fusion.1.refs_2_
  9.7 4.0 %collective-permute-start = (bf16[136,512]{1,0:T(8,128)(2,1)S(1)}, bf16[136,512]{1,0:T(8,128)(2,1)S(1)}, u32[]{:S(2)}, u32[]{:S(2)}) collective-permute-start(bf16[136,512]{1,0:T(8,128)(2,1)S(1)} %fusion.1.refs_2_), channel_id=1, source_target_pairs={{0,8},{8,16},{16,24},{24,32},{32,40},{40,48},{48,56},{56,64},{64,7... | collective-permute-start | bytes 417800 | tf_op jit(solution)/shard_map/ppermute | solution.py:11
  13.8 5.1 %collective-permute-start.4 = (bf16[136,512]{1,0:T(8,128)(2,1)S(1)}, bf16[136,512]{1,0:T(8,128)(2,1)S(1)}, u32[]{:S(2)}, u32[]{:S(2)}) collective-permute-start(bf16[136,512]{1,0:T(8,128)(2,1)S(1)} %fusion.1.refs_2_), channel_id=1, source_target_pairs={{0,56},{8,64},{16,72},{24,80},{32,88},{40,96},{48,104},{56,112},{6... | collective-permute-start | bytes 417800 | tf_op jit(solution)/shard_map/ppermute | solution.py:11
  18.9 9.1 %collective-permute-done.refs_3_ = bf16[136,512]{1,0:T(8,128)(2,1)S(1)} collective-permute-done((bf16[136,512]{1,0:T(8,128)(2,1)S(1)}, bf16[136,512]{1,0:T(8,128)(2,1)S(1)}, u32[]{:S(2)}, u32[]{:S(2)}) %collective-permute-start) | collective-permute-done | bytes 139296 | tf_op jit(solution)/shard_map/ppermute | solution.py:11
  28.0 1.9 %collective-permute-start.1 = (bf16[136,512]{1,0:T(8,128)(2,1)S(1)}, bf16[136,512]{1,0:T(8,128)(2,1)S(1)}, u32[]{:S(2)}, u32[]{:S(2)}) collective-permute-start(bf16[136,512]{1,0:T(8,128)(2,1)S(1)} %collective-permute-done.refs_3_), channel_id=1, source_target_pairs={{0,8},{8,16},{16,24},{24,32},{32,40},{40,48},{48,56},{56,64},{64,7... | collective-permute-start | bytes 417800 | tf_op jit(solution)/shard_map/ppermute | solution.py:11
  30.0 6.7 %collective-permute-start.5 = (bf16[136,512]{1,0:T(8,128)(2,1)S(1)}, bf16[136,512]{1,0:T(8,128)(2,1)S(1)}, u32[]{:S(2)}, u32[]{:S(2)}) collective-permute-start(bf16[136,512]{1,0:T(8,128)(2,1)S(1)} %collective-permute-done.4.refs_9_), channel_id=1, source_target_pairs={{0,504},{8,0},{16,8},{24,16},{32,24},{40,32},{48,40},{56,48},{64,5... | collective-permute-start | bytes 417800 | tf_op jit(solution)/shard_map/ppermute | solution.py:11
  37.2 1.9 %collective-permute-start.2 = (bf16[136,512]{1,0:T(8,128)(2,1)S(1)}, bf16[136,512]{1,0:T(8,128)(2,1)S(1)}, u32[]{:S(2)}, u32[]{:S(2)}) collective-permute-start(bf16[136,512]{1,0:T(8,128)(2,1)S(1)} %collective-permute-done.1.refs_4_), channel_id=1, source_target_pairs={{0,8},{8,16},{16,24},{24,32},{32,40},{40,48},{48,56},{56,64},{64,7... | collective-permute-start | bytes 417800 | tf_op jit(solution)/shard_map/ppermute | solution.py:11
  39.2 6.9 %collective-permute-start.6 = (bf16[136,512]{1,0:T(8,128)(2,1)S(1)}, bf16[136,512]{1,0:T(8,128)(2,1)S(1)}, u32[]{:S(2)}, u32[]{:S(2)}) collective-permute-start(bf16[136,512]{1,0:T(8,128)(2,1)S(1)} %collective-permute-done.5.refs_8_), channel_id=1, source_target_pairs={{0,504},{8,0},{16,8},{24,16},{32,24},{40,32},{48,40},{56,48},{64,5... | collective-permute-start | bytes 417800 | tf_op jit(solution)/shard_map/ppermute | solution.py:11
  46.1 0.9 collective-permute-done.2.refs_5_
  47.0 1.9 %collective-permute-start.3 = (bf16[136,512]{1,0:T(8,128)(2,1)S(1)}, bf16[136,512]{1,0:T(8,128)(2,1)S(1)}, u32[]{:S(2)}, u32[]{:S(2)}) collective-permute-start(bf16[136,512]{1,0:T(8,128)(2,1)S(1)} %collective-permute-done.2.refs_5_), channel_id=1, source_target_pairs={{0,8},{8,16},{16,24},{24,32},{32,40},{40,48},{48,56},{56,64},{64,7... | collective-permute-start | bytes 417800 | tf_op jit(solution)/shard_map/ppermute | solution.py:11
  48.9 7.3 %collective-permute-done.3.refs_6_ = bf16[136,512]{1,0:T(8,128)(2,1)S(1)} collective-permute-done((bf16[136,512]{1,0:T(8,128)(2,1)S(1)}, bf16[136,512]{1,0:T(8,128)(2,1)S(1)}, u32[]{:S(2)}, u32[]{:S(2)}) %collective-permute-start.3) | collective-permute-done | bytes 139296 | tf_op jit(solution)/shard_map/ppermute | solution.py:11
  56.2 0.8 copy-done.1
  57.0 0.7 copy-done.2
  57.7 5.3 %attention.1 = bf16[128,256]{1,0:T(8,128)(2,1)S(1)} custom-call(f32[4]{0:T(128)S(1)} %copy-done.2, bf16[128,256]{1,0:T(8,128)(2,1)S(1)} %copy-done.1, bf16[136,512]{1,0:T(8,128)(2,1)S(1)} %fusion.1.refs_2_, bf16[136,512]{1,0:T(8,128)(2,1)S(1)} %collective-permute-done.refs_3_, bf16[136,512]{1,0:T(8,128)(2,1)S(1)} %collective-permute-done.1.refs_4_, ...), custom_call_target="tpu_custom_call" | custom-call | tf_op jit(solution)/shard_map/attention/pallas_call | solution.py:76
  63.3 19.7 %all_to_all.15 = bf16[8,16,2048]{2,1,0:T(8,128)(2,1)S(1)} all-to-all(bf16[8,16,2048]{2,1,0:T(8,128)(2,1)S(1)} %bitcast.10), channel_id=1, replica_groups=mesh['sp'=64,'tp'=8] {'tp'}, dimensions={0} | all-to-all | bytes 1048576 | tf_op jit(solution)/shard_map/all_to_all | solution.py:17
  83.1 1.0 multiply_reduce_fusion
  84.1 0.9 multiply_convert_fusion
  85.1 12.8 %all_to_all.16 = bf16[8,16,2048]{2,1,0:T(8,128)(2,1)S(1)} all-to-all(bf16[8,16,2048]{2,1,0:T(8,128)(2,1)S(1)} %broadcast_in_dim.9), channel_id=1, replica_groups=mesh['sp'=64,'tp'=8] {'tp'}, dimensions={0} | all-to-all | bytes 1048576 | tf_op jit(solution)/shard_map/all_to_all | solution.py:23
  97.9 22.1 %all-gather.2.cloned.1.call-done.refs_1_ = bf16[2048,2304]{1,0:T(8,128)(2,1)} async-done(((bf16[32,2304]{1,0:T(8,128)(2,1)}), bf16[2048,2304]{1,0:T(8,128)(2,1)}) %all-gather.2.cloned.1.call-update) | async-done | bytes 9437200 | tf_op jit(solution)/shard_map/all_gather | solution.py:178
  120.0 4.7 %ffn.1 = bf16[128,2048]{1,0:T(8,128)(2,1)S(1)} custom-call(bf16[128,2048]{1,0:T(8,128)(2,1)S(1)} %bitcast.8, bf16[2048,2304]{1,0:T(8,128)(2,1)} %all-gather.2.cloned.1.call-done.refs_1_), custom_call_target="tpu_custom_call" | custom-call | tf_op jit(solution)/shard_map/ffn/pallas_call | solution.py:147
  124.7 14.2 %all_to_all.17 = bf16[8,16,2048]{2,1,0:T(8,128)(2,1)S(1)} all-to-all(bf16[8,16,2048]{2,1,0:T(8,128)(2,1)S(1)} %bitcast.9), channel_id=1, replica_groups=mesh['sp'=64,'tp'=8] {'tp'}, dimensions={0} | all-to-all | bytes 1048576 | tf_op jit(solution)/shard_map/all_to_all | solution.py:17
  139.0 0.7 add_convert_fusion
  (17 shorter events, 1.2 us)
Async XLA Ops:
  6.5 56.4 %copy-start = (bf16[256,2048]{1,0:T(8,128)(2,1)S(1)}, bf16[256,2048]{1,0:T(8,128)(2,1)}, u32[]{:S(2)}) copy-start(bf16[256,2048]{1,0:T(8,128)(2,1)} %param.17) | copy-start | bytes 3145732
  6.5 113.5 %all-gather.2.cloned.1.call-start = ((), (), s32[]{:S(2)}) async-start(), calls=%async_computation.3 | async-start | bytes 9584640 | tf_op jit(solution)/shard_map/all_gather | solution.py:178
  8.8 130.2 %copy-start.3 = (bf16[16,2048]{1,0:T(8,128)(2,1)S(1)}, bf16[16,2048]{1,0:T(8,128)(2,1)}, u32[]{:S(2)}) copy-start(bf16[16,2048]{1,0:T(8,128)(2,1)} %param.11) | copy-start | bytes 196612
  9.7 18.3 %collective-permute-start = (bf16[136,512]{1,0:T(8,128)(2,1)S(1)}, bf16[136,512]{1,0:T(8,128)(2,1)S(1)}, u32[]{:S(2)}, u32[]{:S(2)}) collective-permute-start(bf16[136,512]{1,0:T(8,128)(2,1)S(1)} %fusion.1.refs_2_), channel_id=1, source_target_pairs={{0,8},{8,16},{16,24},{24,32},{32,40},{40,48},{48,56},{56,64},{64,7... | collective-permute-start | bytes 417800 | tf_op jit(solution)/shard_map/ppermute | solution.py:11
  13.8 16.2 %collective-permute-start.4 = (bf16[136,512]{1,0:T(8,128)(2,1)S(1)}, bf16[136,512]{1,0:T(8,128)(2,1)S(1)}, u32[]{:S(2)}, u32[]{:S(2)}) collective-permute-start(bf16[136,512]{1,0:T(8,128)(2,1)S(1)} %fusion.1.refs_2_), channel_id=1, source_target_pairs={{0,56},{8,64},{16,72},{24,80},{32,88},{40,96},{48,104},{56,112},{6... | collective-permute-start | bytes 417800 | tf_op jit(solution)/shard_map/ppermute | solution.py:11
  28.0 9.2 %collective-permute-start.1 = (bf16[136,512]{1,0:T(8,128)(2,1)S(1)}, bf16[136,512]{1,0:T(8,128)(2,1)S(1)}, u32[]{:S(2)}, u32[]{:S(2)}) collective-permute-start(bf16[136,512]{1,0:T(8,128)(2,1)S(1)} %collective-permute-done.refs_3_), channel_id=1, source_target_pairs={{0,8},{8,16},{16,24},{24,32},{32,40},{40,48},{48,56},{56,64},{64,7... | collective-permute-start | bytes 417800 | tf_op jit(solution)/shard_map/ppermute | solution.py:11
  30.0 9.2 %collective-permute-start.5 = (bf16[136,512]{1,0:T(8,128)(2,1)S(1)}, bf16[136,512]{1,0:T(8,128)(2,1)S(1)}, u32[]{:S(2)}, u32[]{:S(2)}) collective-permute-start(bf16[136,512]{1,0:T(8,128)(2,1)S(1)} %collective-permute-done.4.refs_9_), channel_id=1, source_target_pairs={{0,504},{8,0},{16,8},{24,16},{32,24},{40,32},{48,40},{56,48},{64,5... | collective-permute-start | bytes 417800 | tf_op jit(solution)/shard_map/ppermute | solution.py:11
  37.2 9.7 %collective-permute-start.2 = (bf16[136,512]{1,0:T(8,128)(2,1)S(1)}, bf16[136,512]{1,0:T(8,128)(2,1)S(1)}, u32[]{:S(2)}, u32[]{:S(2)}) collective-permute-start(bf16[136,512]{1,0:T(8,128)(2,1)S(1)} %collective-permute-done.1.refs_4_), channel_id=1, source_target_pairs={{0,8},{8,16},{16,24},{24,32},{32,40},{40,48},{48,56},{56,64},{64,7... | collective-permute-start | bytes 417800 | tf_op jit(solution)/shard_map/ppermute | solution.py:11
  39.2 9.7 %collective-permute-start.6 = (bf16[136,512]{1,0:T(8,128)(2,1)S(1)}, bf16[136,512]{1,0:T(8,128)(2,1)S(1)}, u32[]{:S(2)}, u32[]{:S(2)}) collective-permute-start(bf16[136,512]{1,0:T(8,128)(2,1)S(1)} %collective-permute-done.5.refs_8_), channel_id=1, source_target_pairs={{0,504},{8,0},{16,8},{24,16},{32,24},{40,32},{48,40},{56,48},{64,5... | collective-permute-start | bytes 417800 | tf_op jit(solution)/shard_map/ppermute | solution.py:11
  47.0 9.2 %collective-permute-start.3 = (bf16[136,512]{1,0:T(8,128)(2,1)S(1)}, bf16[136,512]{1,0:T(8,128)(2,1)S(1)}, u32[]{:S(2)}, u32[]{:S(2)}) collective-permute-start(bf16[136,512]{1,0:T(8,128)(2,1)S(1)} %collective-permute-done.2.refs_5_), channel_id=1, source_target_pairs={{0,8},{8,16},{16,24},{24,32},{32,40},{40,48},{48,56},{56,64},{64,7... | collective-permute-start | bytes 417800 | tf_op jit(solution)/shard_map/ppermute | solution.py:11
  56.2 0.8 copy-start.1
  57.0 0.7 copy-start.2
Sparse Core Ops, SparseCore 0:
  10.3 109.6 all-gather.1

commit v10 on v9

--- a/solution.py
+++ b/solution.py
@@ -181,10 +181,14 @@
     own = jnp.concatenate([jnp.concatenate([keys, values], axis=1), docs], axis=0)
     blocks = {0: own}
     blocks[7] = shifted(own, 7)
-    for back in range(1, 5):
+    for back in range(1, 4):
         blocks[back] = shifted(blocks[back - 1], 1)
         if back < 3:
             blocks[7 - back] = shifted(blocks[8 - back], -1)
+    width = keys.shape[1]
+    blocks[4] = jnp.concatenate(
+        [shifted(blocks[3][:, :width], 1), shifted(blocks[5][:, width:], -1)], axis=1
+    )
     attended = attention(queries, [blocks[b] for b in range(8)], score_offset)
 
     mixed_attn = summed_for_owner(

time: 147 us -> 147 us (level)
  starting transfers between devices: 28.4 us -> 35.4 us
  waiting for transfers between devices: 40.1 us -> 33.5 us
    ppermute x7 -> x8, starting transfers between devices: 28.4 us -> 35.4 us  [shifted(): lax.ppermute(block, 'sp', [(i, (i + by) % spans) for i in range(spans)])]
    ppermute x7 -> x8, waiting for transfers between devices: 17.9 us -> 12 us  [shifted(): lax.ppermute(block, 'sp', [(i, (i + by) % spans) for i in range(spans)])]
  transfers between devices with their start and end apart: 8 -> 9, of which waited for: 5 -> 5; matrix products, arithmetic and copies ran while one was open for 3% -> 3% of each run, Pallas kernels for 4% -> 4%
where the time goes in v10:
time: 147 us
  blocking collectives  46.3 us (31%)
  starting transfers between devices  35.4 us (24%)
  waiting for transfers between devices  33.5 us (23%)
  between operations  13.6 us (9%)
  Pallas kernels  10 us (7%)
  other arithmetic  5.88 us (4%)
  local copies, waits for them, and re-layouts  1.55 us (1%)
    ppermute x8, starting transfers between devices, shifted(): lax.ppermute(block, 'sp', [(i, (i + by) % spans) for i in range(spans)])  35.4 us
    all_to_all x2, blocking collectives, summed_for_owner(): tiles = lax.all_to_all(tiles, 'tp', 0, 0, tiled=True)  33.6 us
    all_gather x1, waiting for transfers between devices, on_device(): weights = lax.all_gather(packed, 'sp', axis=0, tiled=True)  21.5 us
    all_to_all x1, blocking collectives, from_everyone(): return lax.all_to_all(copies, 'tp', split_axis=0, concat_axis=0, tiled=True)  12.8 us
    ppermute x8, waiting for transfers between devices, shifted(): lax.ppermute(block, 'sp', [(i, (i + by) % spans) for i in range(spans)])  12 us
    pallas_call x1, Pallas kernels, attention(): pl.pallas_call(body, out_shape=jax.ShapeDtypeStruct((rows, width), jnp.bf...  5.3 us
    pallas_call x1, Pallas kernels, ffn(): pl.pallas_call(body, out_shape=jax.ShapeDtypeStruct(x.shape, jnp.bfloat16...  4.7 us
  transfers between devices with their start and end apart: 9, of which 5 were waited for; matrix products, arithmetic and copies ran while one was open for 3% of the time, Pallas kernels for 4%

profile of v10, /device:TPU:1, one launch (start us, length us, event | category | flops | bytes accessed | tf_op | source)
XLA Modules:
  0.0 146.6 jit_solution(5924831929855934031)
XLA Ops:
  6.5 1.6 %pad_maximum_fusion = bf16[32,2304]{1,0:T(8,128)(2,1)} fusion(bf16[32,768]{1,0:T(8,128)(2,1)} %bitcast.11, bf16[32,768]{1,0:T(8,128)(2,1)} %param.20, bf16[32,768]{1,0:T(8,128)(2,1)} %param.19), kind=kLoop, calls=%fused_computation.5 | loop fusion | flops 442368 | bytes 294912 | tf_op jit(solution)/shard_map/concatenate | solution.py:177
  8.2 0.7 convert_bitcast_fusion
  8.8 0.9 fusion.1.refs_2_
  9.7 4.0 %collective-permute-start = (bf16[136,512]{1,0:T(8,128)(2,1)S(1)}, bf16[136,512]{1,0:T(8,128)(2,1)S(1)}, u32[]{:S(2)}, u32[]{:S(2)}) collective-permute-start(bf16[136,512]{1,0:T(8,128)(2,1)S(1)} %fusion.1.refs_2_), channel_id=1, source_target_pairs={{0,8},{8,16},{16,24},{24,32},{32,40},{40,48},{48,56},{56,64},{64,7... | collective-permute-start | bytes 417800 | tf_op jit(solution)/shard_map/ppermute | solution.py:11
  13.7 5.1 %collective-permute-start.4 = (bf16[136,512]{1,0:T(8,128)(2,1)S(1)}, bf16[136,512]{1,0:T(8,128)(2,1)S(1)}, u32[]{:S(2)}, u32[]{:S(2)}) collective-permute-start(bf16[136,512]{1,0:T(8,128)(2,1)S(1)} %fusion.1.refs_2_), channel_id=1, source_target_pairs={{0,56},{8,64},{16,72},{24,80},{32,88},{40,96},{48,104},{56,112},{6... | collective-permute-start | bytes 417800 | tf_op jit(solution)/shard_map/ppermute | solution.py:11
  18.8 9.1 %collective-permute-done.refs_3_ = bf16[136,512]{1,0:T(8,128)(2,1)S(1)} collective-permute-done((bf16[136,512]{1,0:T(8,128)(2,1)S(1)}, bf16[136,512]{1,0:T(8,128)(2,1)S(1)}, u32[]{:S(2)}, u32[]{:S(2)}) %collective-permute-start) | collective-permute-done | bytes 139296 | tf_op jit(solution)/shard_map/ppermute | solution.py:11
  28.0 1.9 %collective-permute-start.1 = (bf16[136,512]{1,0:T(8,128)(2,1)S(1)}, bf16[136,512]{1,0:T(8,128)(2,1)S(1)}, u32[]{:S(2)}, u32[]{:S(2)}) collective-permute-start(bf16[136,512]{1,0:T(8,128)(2,1)S(1)} %collective-permute-done.refs_3_), channel_id=1, source_target_pairs={{0,8},{8,16},{16,24},{24,32},{32,40},{40,48},{48,56},{56,64},{64,7... | collective-permute-start | bytes 417800 | tf_op jit(solution)/shard_map/ppermute | solution.py:11
  29.9 6.7 %collective-permute-start.5 = (bf16[136,512]{1,0:T(8,128)(2,1)S(1)}, bf16[136,512]{1,0:T(8,128)(2,1)S(1)}, u32[]{:S(2)}, u32[]{:S(2)}) collective-permute-start(bf16[136,512]{1,0:T(8,128)(2,1)S(1)} %collective-permute-done.4.refs_9_), channel_id=1, source_target_pairs={{0,504},{8,0},{16,8},{24,16},{32,24},{40,32},{48,40},{56,48},{64,5... | collective-permute-start | bytes 417800 | tf_op jit(solution)/shard_map/ppermute | solution.py:11
  37.2 1.9 %collective-permute-start.2 = (bf16[136,512]{1,0:T(8,128)(2,1)S(1)}, bf16[136,512]{1,0:T(8,128)(2,1)S(1)}, u32[]{:S(2)}, u32[]{:S(2)}) collective-permute-start(bf16[136,512]{1,0:T(8,128)(2,1)S(1)} %collective-permute-done.1.refs_4_), channel_id=1, source_target_pairs={{0,8},{8,16},{16,24},{24,32},{32,40},{40,48},{48,56},{56,64},{64,7... | collective-permute-start | bytes 417800 | tf_op jit(solution)/shard_map/ppermute | solution.py:11
  39.1 6.9 %collective-permute-start.6 = (bf16[136,512]{1,0:T(8,128)(2,1)S(1)}, bf16[136,512]{1,0:T(8,128)(2,1)S(1)}, u32[]{:S(2)}, u32[]{:S(2)}) collective-permute-start(bf16[136,512]{1,0:T(8,128)(2,1)S(1)} %collective-permute-done.5.refs_8_), channel_id=1, source_target_pairs={{0,504},{8,0},{16,8},{24,16},{32,24},{40,32},{48,40},{56,48},{64,5... | collective-permute-start | bytes 417800 | tf_op jit(solution)/shard_map/ppermute | solution.py:11
  46.1 0.9 collective-permute-done.2.refs_5_
  46.9 1.9 %collective-permute-start.3 = (bf16[136,256]{1,0:T(8,128)(2,1)S(1)}, bf16[136,256]{1,0:T(8,128)(2,1)S(1)}, u32[]{:S(2)}, u32[]{:S(2)}) collective-permute-start(bf16[136,256]{1,0:T(8,128)(2,1)S(1)} %slice.8), channel_id=1, source_target_pairs={{0,8},{8,16},{16,24},{24,32},{32,40},{40,48},{48,56},{56,64},{64,7... | collective-permute-start | bytes 208904 | tf_op jit(solution)/shard_map/ppermute | solution.py:11
  48.9 7.0 %collective-permute-start.7 = (bf16[136,256]{1,0:T(8,128)(2,1)S(1)}, bf16[136,256]{1,0:T(8,128)(2,1)S(1)}, u32[]{:S(2)}, u32[]{:S(2)}) collective-permute-start(bf16[136,256]{1,0:T(8,128)(2,1)S(1)} %slice.9), channel_id=1, source_target_pairs={{0,504},{8,0},{16,8},{24,16},{32,24},{40,32},{48,40},{56,48},{64,5... | collective-permute-start | bytes 208904 | tf_op jit(solution)/shard_map/ppermute | solution.py:11
  55.9 1.3 collective-permute-done.7
  57.2 0.8 copy-done.1
  58.7 5.3 %attention.1 = bf16[128,256]{1,0:T(8,128)(2,1)S(1)} custom-call(f32[4]{0:T(128)S(1)} %copy-done.2, bf16[128,256]{1,0:T(8,128)(2,1)S(1)} %copy-done.1, bf16[136,512]{1,0:T(8,128)(2,1)S(1)} %fusion.1.refs_2_, bf16[136,512]{1,0:T(8,128)(2,1)S(1)} %collective-permute-done.refs_3_, bf16[136,512]{1,0:T(8,128)(2,1)S(1)} %collective-permute-done.1.refs_4_, ...), custom_call_target="tpu_custom_call" | custom-call | tf_op jit(solution)/shard_map/attention/pallas_call | solution.py:76
  64.4 19.3 %all_to_all.15 = bf16[8,16,2048]{2,1,0:T(8,128)(2,1)S(1)} all-to-all(bf16[8,16,2048]{2,1,0:T(8,128)(2,1)S(1)} %bitcast.10), channel_id=1, replica_groups=mesh['sp'=64,'tp'=8] {'tp'}, dimensions={0} | all-to-all | bytes 1048576 | tf_op jit(solution)/shard_map/all_to_all | solution.py:17
  83.8 1.0 multiply_reduce_fusion
  84.8 0.9 multiply_convert_fusion
  85.8 12.8 %all_to_all.16 = bf16[8,16,2048]{2,1,0:T(8,128)(2,1)S(1)} all-to-all(bf16[8,16,2048]{2,1,0:T(8,128)(2,1)S(1)} %broadcast_in_dim.9), channel_id=1, replica_groups=mesh['sp'=64,'tp'=8] {'tp'}, dimensions={0} | all-to-all | bytes 1048576 | tf_op jit(solution)/shard_map/all_to_all | solution.py:23
  98.5 21.5 %all-gather.2.cloned.1.call-done.refs_1_ = bf16[2048,2304]{1,0:T(8,128)(2,1)} async-done(((bf16[32,2304]{1,0:T(8,128)(2,1)}), bf16[2048,2304]{1,0:T(8,128)(2,1)}) %all-gather.2.cloned.1.call-update) | async-done | bytes 9437200 | tf_op jit(solution)/shard_map/all_gather | solution.py:178
  120.1 4.7 %ffn.1 = bf16[128,2048]{1,0:T(8,128)(2,1)S(1)} custom-call(bf16[128,2048]{1,0:T(8,128)(2,1)S(1)} %bitcast.8, bf16[2048,2304]{1,0:T(8,128)(2,1)} %all-gather.2.cloned.1.call-done.refs_1_), custom_call_target="tpu_custom_call" | custom-call | tf_op jit(solution)/shard_map/ffn/pallas_call | solution.py:147
  124.8 14.2 %all_to_all.17 = bf16[8,16,2048]{2,1,0:T(8,128)(2,1)S(1)} all-to-all(bf16[8,16,2048]{2,1,0:T(8,128)(2,1)S(1)} %bitcast.9), channel_id=1, replica_groups=mesh['sp'=64,'tp'=8] {'tp'}, dimensions={0} | all-to-all | bytes 1048576 | tf_op jit(solution)/shard_map/all_to_all | solution.py:17
  139.1 0.7 add_convert_fusion
  (22 shorter events, 1.8 us)
Async XLA Ops:
  6.5 57.5 %copy-start = (bf16[256,2048]{1,0:T(8,128)(2,1)S(1)}, bf16[256,2048]{1,0:T(8,128)(2,1)}, u32[]{:S(2)}) copy-start(bf16[256,2048]{1,0:T(8,128)(2,1)} %param.17) | copy-start | bytes 3145732
  6.5 113.5 %all-gather.2.cloned.1.call-start = ((), (), s32[]{:S(2)}) async-start(), calls=%async_computation.3 | async-start | bytes 9584640 | tf_op jit(solution)/shard_map/all_gather | solution.py:178
  9.7 18.3 %collective-permute-start = (bf16[136,512]{1,0:T(8,128)(2,1)S(1)}, bf16[136,512]{1,0:T(8,128)(2,1)S(1)}, u32[]{:S(2)}, u32[]{:S(2)}) collective-permute-start(bf16[136,512]{1,0:T(8,128)(2,1)S(1)} %fusion.1.refs_2_), channel_id=1, source_target_pairs={{0,8},{8,16},{16,24},{24,32},{32,40},{40,48},{48,56},{56,64},{64,7... | collective-permute-start | bytes 417800 | tf_op jit(solution)/shard_map/ppermute | solution.py:11
  13.7 16.2 %collective-permute-start.4 = (bf16[136,512]{1,0:T(8,128)(2,1)S(1)}, bf16[136,512]{1,0:T(8,128)(2,1)S(1)}, u32[]{:S(2)}, u32[]{:S(2)}) collective-permute-start(bf16[136,512]{1,0:T(8,128)(2,1)S(1)} %fusion.1.refs_2_), channel_id=1, source_target_pairs={{0,56},{8,64},{16,72},{24,80},{32,88},{40,96},{48,104},{56,112},{6... | collective-permute-start | bytes 417800 | tf_op jit(solution)/shard_map/ppermute | solution.py:11
  28.0 9.2 %collective-permute-start.1 = (bf16[136,512]{1,0:T(8,128)(2,1)S(1)}, bf16[136,512]{1,0:T(8,128)(2,1)S(1)}, u32[]{:S(2)}, u32[]{:S(2)}) collective-permute-start(bf16[136,512]{1,0:T(8,128)(2,1)S(1)} %collective-permute-done.refs_3_), channel_id=1, source_target_pairs={{0,8},{8,16},{16,24},{24,32},{32,40},{40,48},{48,56},{56,64},{64,7... | collective-permute-start | bytes 417800 | tf_op jit(solution)/shard_map/ppermute | solution.py:11
  29.9 9.2 %collective-permute-start.5 = (bf16[136,512]{1,0:T(8,128)(2,1)S(1)}, bf16[136,512]{1,0:T(8,128)(2,1)S(1)}, u32[]{:S(2)}, u32[]{:S(2)}) collective-permute-start(bf16[136,512]{1,0:T(8,128)(2,1)S(1)} %collective-permute-done.4.refs_9_), channel_id=1, source_target_pairs={{0,504},{8,0},{16,8},{24,16},{32,24},{40,32},{48,40},{56,48},{64,5... | collective-permute-start | bytes 417800 | tf_op jit(solution)/shard_map/ppermute | solution.py:11
  37.2 9.7 %collective-permute-start.2 = (bf16[136,512]{1,0:T(8,128)(2,1)S(1)}, bf16[136,512]{1,0:T(8,128)(2,1)S(1)}, u32[]{:S(2)}, u32[]{:S(2)}) collective-permute-start(bf16[136,512]{1,0:T(8,128)(2,1)S(1)} %collective-permute-done.1.refs_4_), channel_id=1, source_target_pairs={{0,8},{8,16},{16,24},{24,32},{32,40},{40,48},{48,56},{56,64},{64,7... | collective-permute-start | bytes 417800 | tf_op jit(solution)/shard_map/ppermute | solution.py:11
  39.1 9.7 %collective-permute-start.6 = (bf16[136,512]{1,0:T(8,128)(2,1)S(1)}, bf16[136,512]{1,0:T(8,128)(2,1)S(1)}, u32[]{:S(2)}, u32[]{:S(2)}) collective-permute-start(bf16[136,512]{1,0:T(8,128)(2,1)S(1)} %collective-permute-done.5.refs_8_), channel_id=1, source_target_pairs={{0,504},{8,0},{16,8},{24,16},{32,24},{40,32},{48,40},{56,48},{64,5... | collective-permute-start | bytes 417800 | tf_op jit(solution)/shard_map/ppermute | solution.py:11
  46.9 8.9 %collective-permute-start.3 = (bf16[136,256]{1,0:T(8,128)(2,1)S(1)}, bf16[136,256]{1,0:T(8,128)(2,1)S(1)}, u32[]{:S(2)}, u32[]{:S(2)}) collective-permute-start(bf16[136,256]{1,0:T(8,128)(2,1)S(1)} %slice.8), channel_id=1, source_target_pairs={{0,8},{8,16},{16,24},{24,32},{32,40},{40,48},{48,56},{56,64},{64,7... | collective-permute-start | bytes 208904 | tf_op jit(solution)/shard_map/ppermute | solution.py:11
  48.9 8.3 %collective-permute-start.7 = (bf16[136,256]{1,0:T(8,128)(2,1)S(1)}, bf16[136,256]{1,0:T(8,128)(2,1)S(1)}, u32[]{:S(2)}, u32[]{:S(2)}) collective-permute-start(bf16[136,256]{1,0:T(8,128)(2,1)S(1)} %slice.9), channel_id=1, source_target_pairs={{0,504},{8,0},{16,8},{24,16},{32,24},{40,32},{48,40},{56,48},{64,5... | collective-permute-start | bytes 208904 | tf_op jit(solution)/shard_map/ppermute | solution.py:11
  57.2 0.8 copy-start.1
  58.1 0.7 copy-start.2
  58.7 80.3 %copy-start.3 = (bf16[16,2048]{1,0:T(8,128)(2,1)S(1)}, bf16[16,2048]{1,0:T(8,128)(2,1)}, u32[]{:S(2)}) copy-start(bf16[16,2048]{1,0:T(8,128)(2,1)} %param.11) | copy-start | bytes 196612
Sparse Core Ops, SparseCore 0:
  10.3 109.6 all-gather.1

commit v11 on v9

--- a/solution.py
+++ b/solution.py
@@ -181,9 +181,9 @@
     own = jnp.concatenate([jnp.concatenate([keys, values], axis=1), docs], axis=0)
     blocks = {0: own}
     blocks[7] = shifted(own, 7)
-    for back in range(1, 5):
+    for back in range(1, 4):
         blocks[back] = shifted(blocks[back - 1], 1)
-        if back < 3:
+        if back < 4:
             blocks[7 - back] = shifted(blocks[8 - back], -1)
     attended = attention(queries, [blocks[b] for b in range(8)], score_offset)
 

time: 147 us -> 147 us (level)
  starting transfers between devices: 28.4 us -> 32.2 us
  blocking collectives: 46.7 us -> 44.5 us
    ppermute x7, waiting for transfers between devices: 17.9 us -> 11.3 us  [shifted(): lax.ppermute(block, 'sp', [(i, (i + by) % spans) for i in range(spans)])]
    all_gather x1, waiting for transfers between devices: 22.1 us -> 27.4 us  [on_device(): weights = lax.all_gather(packed, 'sp', axis=0, tiled=True)]
    ppermute x7, starting transfers between devices: 28.4 us -> 32.2 us  [shifted(): lax.ppermute(block, 'sp', [(i, (i + by) % spans) for i in range(spans)])]
    all_to_all x2, blocking collectives: 33.9 us -> 31.8 us  [summed_for_owner(): tiles = lax.all_to_all(tiles, 'tp', 0, 0, tiled=True)]
  transfers between devices with their start and end apart: 8 -> 8, of which waited for: 5 -> 6; matrix products, arithmetic and copies ran while one was open for 3% -> 3% of each run, Pallas kernels for 4% -> 4%
where the time goes in v11:
time: 147 us
  blocking collectives  44.5 us (30%)
  waiting for transfers between devices  38.7 us (26%)
  starting transfers between devices  32.2 us (22%)
  between operations  13.5 us (9%)
  Pallas kernels  10 us (7%)
  other arithmetic  5.91 us (4%)
  local copies, waits for them, and re-layouts  1.55 us (1%)
    ppermute x7, starting transfers between devices, shifted(): lax.ppermute(block, 'sp', [(i, (i + by) % spans) for i in range(spans)])  32.2 us
    all_to_all x2, blocking collectives, summed_for_owner(): tiles = lax.all_to_all(tiles, 'tp', 0, 0, tiled=True)  31.8 us
    all_gather x1, waiting for transfers between devices, on_device(): weights = lax.all_gather(packed, 'sp', axis=0, tiled=True)  27.4 us
    all_to_all x1, blocking collectives, from_everyone(): return lax.all_to_all(copies, 'tp', split_axis=0, concat_axis=0, tiled=True)  12.8 us
    ppermute x7, waiting for transfers between devices, shifted(): lax.ppermute(block, 'sp', [(i, (i + by) % spans) for i in range(spans)])  11.3 us
    pallas_call x1, Pallas kernels, attention(): pl.pallas_call(body, out_shape=jax.ShapeDtypeStruct((rows, width), jnp.bf...  5.3 us
    pallas_call x1, Pallas kernels, ffn(): pl.pallas_call(body, out_shape=jax.ShapeDtypeStruct(x.shape, jnp.bfloat16...  4.7 us
  transfers between devices with their start and end apart: 8, of which 6 were waited for; matrix products, arithmetic and copies ran while one was open for 3% of the time, Pallas kernels for 4%

profile of v11, /device:TPU:1, one launch (start us, length us, event | category | flops | bytes accessed | tf_op | source)
XLA Modules:
  0.0 146.7 jit_solution(681254426963074186)
XLA Ops:
  6.5 1.6 %pad_maximum_fusion = bf16[32,2304]{1,0:T(8,128)(2,1)} fusion(bf16[32,768]{1,0:T(8,128)(2,1)} %bitcast.11, bf16[32,768]{1,0:T(8,128)(2,1)} %param.20, bf16[32,768]{1,0:T(8,128)(2,1)} %param.19), kind=kLoop, calls=%fused_computation.5 | loop fusion | flops 442368 | bytes 294912 | tf_op jit(solution)/shard_map/concatenate | solution.py:177
  8.2 0.7 convert_bitcast_fusion
  8.8 0.9 fusion.1.refs_2_
  9.7 5.9 %collective-permute-start.3 = (bf16[136,512]{1,0:T(8,128)(2,1)S(1)}, bf16[136,512]{1,0:T(8,128)(2,1)S(1)}, u32[]{:S(2)}, u32[]{:S(2)}) collective-permute-start(bf16[136,512]{1,0:T(8,128)(2,1)S(1)} %fusion.1.refs_2_), channel_id=1, source_target_pairs={{0,56},{8,64},{16,72},{24,80},{32,88},{40,96},{48,104},{56,112},{6... | collective-permute-start | bytes 417800 | tf_op jit(solution)/shard_map/ppermute | solution.py:11
  15.7 2.0 %collective-permute-start = (bf16[136,512]{1,0:T(8,128)(2,1)S(1)}, bf16[136,512]{1,0:T(8,128)(2,1)S(1)}, u32[]{:S(2)}, u32[]{:S(2)}) collective-permute-start(bf16[136,512]{1,0:T(8,128)(2,1)S(1)} %fusion.1.refs_2_), channel_id=1, source_target_pairs={{0,8},{8,16},{16,24},{24,32},{32,40},{40,48},{48,56},{56,64},{64,7... | collective-permute-start | bytes 417800 | tf_op jit(solution)/shard_map/ppermute | solution.py:11
  17.7 7.9 %collective-permute-done.3.refs_9_ = bf16[136,512]{1,0:T(8,128)(2,1)S(1)} collective-permute-done((bf16[136,512]{1,0:T(8,128)(2,1)S(1)}, bf16[136,512]{1,0:T(8,128)(2,1)S(1)}, u32[]{:S(2)}, u32[]{:S(2)}) %collective-permute-start.3) | collective-permute-done | bytes 139296 | tf_op jit(solution)/shard_map/ppermute | solution.py:11
  25.6 6.2 %collective-permute-start.4 = (bf16[136,512]{1,0:T(8,128)(2,1)S(1)}, bf16[136,512]{1,0:T(8,128)(2,1)S(1)}, u32[]{:S(2)}, u32[]{:S(2)}) collective-permute-start(bf16[136,512]{1,0:T(8,128)(2,1)S(1)} %collective-permute-done.3.refs_9_), channel_id=1, source_target_pairs={{0,504},{8,0},{16,8},{24,16},{32,24},{40,32},{48,40},{56,48},{64,5... | collective-permute-start | bytes 417800 | tf_op jit(solution)/shard_map/ppermute | solution.py:11
  31.8 1.9 %collective-permute-start.1 = (bf16[136,512]{1,0:T(8,128)(2,1)S(1)}, bf16[136,512]{1,0:T(8,128)(2,1)S(1)}, u32[]{:S(2)}, u32[]{:S(2)}) collective-permute-start(bf16[136,512]{1,0:T(8,128)(2,1)S(1)} %collective-permute-done.refs_3_), channel_id=1, source_target_pairs={{0,8},{8,16},{16,24},{24,32},{32,40},{40,48},{48,56},{56,64},{64,7... | collective-permute-start | bytes 417800 | tf_op jit(solution)/shard_map/ppermute | solution.py:11
  34.1 7.1 %collective-permute-start.5 = (bf16[136,512]{1,0:T(8,128)(2,1)S(1)}, bf16[136,512]{1,0:T(8,128)(2,1)S(1)}, u32[]{:S(2)}, u32[]{:S(2)}) collective-permute-start(bf16[136,512]{1,0:T(8,128)(2,1)S(1)} %collective-permute-done.4.refs_8_), channel_id=1, source_target_pairs={{0,504},{8,0},{16,8},{24,16},{32,24},{40,32},{48,40},{56,48},{64,5... | collective-permute-start | bytes 417800 | tf_op jit(solution)/shard_map/ppermute | solution.py:11
  41.2 1.9 %collective-permute-start.2 = (bf16[136,512]{1,0:T(8,128)(2,1)S(1)}, bf16[136,512]{1,0:T(8,128)(2,1)S(1)}, u32[]{:S(2)}, u32[]{:S(2)}) collective-permute-start(bf16[136,512]{1,0:T(8,128)(2,1)S(1)} %collective-permute-done.1.refs_4_), channel_id=1, source_target_pairs={{0,8},{8,16},{16,24},{24,32},{32,40},{40,48},{48,56},{56,64},{64,7... | collective-permute-start | bytes 417800 | tf_op jit(solution)/shard_map/ppermute | solution.py:11
  43.2 0.7 collective-permute-done.5.refs_7_
  43.8 7.1 %collective-permute-start.6 = (bf16[136,512]{1,0:T(8,128)(2,1)S(1)}, bf16[136,512]{1,0:T(8,128)(2,1)S(1)}, u32[]{:S(2)}, u32[]{:S(2)}) collective-permute-start(bf16[136,512]{1,0:T(8,128)(2,1)S(1)} %collective-permute-done.5.refs_7_), channel_id=1, source_target_pairs={{0,504},{8,0},{16,8},{24,16},{32,24},{40,32},{48,40},{56,48},{64,5... | collective-permute-start | bytes 417800 | tf_op jit(solution)/shard_map/ppermute | solution.py:11
  51.3 1.9 %collective-permute-done.6.refs_6_ = bf16[136,512]{1,0:T(8,128)(2,1)S(1)} collective-permute-done((bf16[136,512]{1,0:T(8,128)(2,1)S(1)}, bf16[136,512]{1,0:T(8,128)(2,1)S(1)}, u32[]{:S(2)}, u32[]{:S(2)}) %collective-permute-start.6) | collective-permute-done | bytes 139296 | tf_op jit(solution)/shard_map/ppermute | solution.py:11
  53.3 0.8 copy-done.1
  54.1 0.7 copy-done.2
  54.8 5.3 %attention.1 = bf16[128,256]{1,0:T(8,128)(2,1)S(1)} custom-call(f32[4]{0:T(128)S(1)} %copy-done.2, bf16[128,256]{1,0:T(8,128)(2,1)S(1)} %copy-done.1, bf16[136,512]{1,0:T(8,128)(2,1)S(1)} %fusion.1.refs_2_, bf16[136,512]{1,0:T(8,128)(2,1)S(1)} %collective-permute-done.refs_3_, bf16[136,512]{1,0:T(8,128)(2,1)S(1)} %collective-permute-done.1.refs_4_, ...), custom_call_target="tpu_custom_call" | custom-call | tf_op jit(solution)/shard_map/attention/pallas_call | solution.py:76
  60.4 17.5 %all_to_all.15 = bf16[8,16,2048]{2,1,0:T(8,128)(2,1)S(1)} all-to-all(bf16[8,16,2048]{2,1,0:T(8,128)(2,1)S(1)} %bitcast.10), channel_id=1, replica_groups=mesh['sp'=64,'tp'=8] {'tp'}, dimensions={0} | all-to-all | bytes 1048576 | tf_op jit(solution)/shard_map/all_to_all | solution.py:17
  78.0 1.0 multiply_reduce_fusion
  79.0 1.0 multiply_convert_fusion
  80.0 12.8 %all_to_all.16 = bf16[8,16,2048]{2,1,0:T(8,128)(2,1)S(1)} all-to-all(bf16[8,16,2048]{2,1,0:T(8,128)(2,1)S(1)} %broadcast_in_dim.9), channel_id=1, replica_groups=mesh['sp'=64,'tp'=8] {'tp'}, dimensions={0} | all-to-all | bytes 1048576 | tf_op jit(solution)/shard_map/all_to_all | solution.py:23
  92.8 27.4 %all-gather.2.cloned.1.call-done.refs_1_ = bf16[2048,2304]{1,0:T(8,128)(2,1)} async-done(((bf16[32,2304]{1,0:T(8,128)(2,1)}), bf16[2048,2304]{1,0:T(8,128)(2,1)}) %all-gather.2.cloned.1.call-update) | async-done | bytes 9437200 | tf_op jit(solution)/shard_map/all_gather | solution.py:178
  120.2 4.7 %ffn.1 = bf16[128,2048]{1,0:T(8,128)(2,1)S(1)} custom-call(bf16[128,2048]{1,0:T(8,128)(2,1)S(1)} %bitcast.8, bf16[2048,2304]{1,0:T(8,128)(2,1)} %all-gather.2.cloned.1.call-done.refs_1_), custom_call_target="tpu_custom_call" | custom-call | tf_op jit(solution)/shard_map/ffn/pallas_call | solution.py:147
  124.9 14.2 %all_to_all.17 = bf16[8,16,2048]{2,1,0:T(8,128)(2,1)S(1)} all-to-all(bf16[8,16,2048]{2,1,0:T(8,128)(2,1)S(1)} %bitcast.9), channel_id=1, replica_groups=mesh['sp'=64,'tp'=8] {'tp'}, dimensions={0} | all-to-all | bytes 1048576 | tf_op jit(solution)/shard_map/all_to_all | solution.py:17
  139.2 0.7 add_convert_fusion
  (17 shorter events, 1.2 us)
Async XLA Ops:
  6.5 53.5 %copy-start = (bf16[256,2048]{1,0:T(8,128)(2,1)S(1)}, bf16[256,2048]{1,0:T(8,128)(2,1)}, u32[]{:S(2)}) copy-start(bf16[256,2048]{1,0:T(8,128)(2,1)} %param.17) | copy-start | bytes 3145732
  6.5 113.6 %all-gather.2.cloned.1.call-start = ((), (), s32[]{:S(2)}) async-start(), calls=%async_computation.3 | async-start | bytes 9584640 | tf_op jit(solution)/shard_map/all_gather | solution.py:178
  8.8 130.4 %copy-start.3 = (bf16[16,2048]{1,0:T(8,128)(2,1)S(1)}, bf16[16,2048]{1,0:T(8,128)(2,1)}, u32[]{:S(2)}) copy-start(bf16[16,2048]{1,0:T(8,128)(2,1)} %param.11) | copy-start | bytes 196612
  9.7 15.9 %collective-permute-start.3 = (bf16[136,512]{1,0:T(8,128)(2,1)S(1)}, bf16[136,512]{1,0:T(8,128)(2,1)S(1)}, u32[]{:S(2)}, u32[]{:S(2)}) collective-permute-start(bf16[136,512]{1,0:T(8,128)(2,1)S(1)} %fusion.1.refs_2_), channel_id=1, source_target_pairs={{0,56},{8,64},{16,72},{24,80},{32,88},{40,96},{48,104},{56,112},{6... | collective-permute-start | bytes 417800 | tf_op jit(solution)/shard_map/ppermute | solution.py:11
  15.7 16.1 %collective-permute-start = (bf16[136,512]{1,0:T(8,128)(2,1)S(1)}, bf16[136,512]{1,0:T(8,128)(2,1)S(1)}, u32[]{:S(2)}, u32[]{:S(2)}) collective-permute-start(bf16[136,512]{1,0:T(8,128)(2,1)S(1)} %fusion.1.refs_2_), channel_id=1, source_target_pairs={{0,8},{8,16},{16,24},{24,32},{32,40},{40,48},{48,56},{56,64},{64,7... | collective-permute-start | bytes 417800 | tf_op jit(solution)/shard_map/ppermute | solution.py:11
  25.6 8.5 %collective-permute-start.4 = (bf16[136,512]{1,0:T(8,128)(2,1)S(1)}, bf16[136,512]{1,0:T(8,128)(2,1)S(1)}, u32[]{:S(2)}, u32[]{:S(2)}) collective-permute-start(bf16[136,512]{1,0:T(8,128)(2,1)S(1)} %collective-permute-done.3.refs_9_), channel_id=1, source_target_pairs={{0,504},{8,0},{16,8},{24,16},{32,24},{40,32},{48,40},{56,48},{64,5... | collective-permute-start | bytes 417800 | tf_op jit(solution)/shard_map/ppermute | solution.py:11
  31.8 9.4 %collective-permute-start.1 = (bf16[136,512]{1,0:T(8,128)(2,1)S(1)}, bf16[136,512]{1,0:T(8,128)(2,1)S(1)}, u32[]{:S(2)}, u32[]{:S(2)}) collective-permute-start(bf16[136,512]{1,0:T(8,128)(2,1)S(1)} %collective-permute-done.refs_3_), channel_id=1, source_target_pairs={{0,8},{8,16},{16,24},{24,32},{32,40},{40,48},{48,56},{56,64},{64,7... | collective-permute-start | bytes 417800 | tf_op jit(solution)/shard_map/ppermute | solution.py:11
  34.1 9.8 %collective-permute-start.5 = (bf16[136,512]{1,0:T(8,128)(2,1)S(1)}, bf16[136,512]{1,0:T(8,128)(2,1)S(1)}, u32[]{:S(2)}, u32[]{:S(2)}) collective-permute-start(bf16[136,512]{1,0:T(8,128)(2,1)S(1)} %collective-permute-done.4.refs_8_), channel_id=1, source_target_pairs={{0,504},{8,0},{16,8},{24,16},{32,24},{40,32},{48,40},{56,48},{64,5... | collective-permute-start | bytes 417800 | tf_op jit(solution)/shard_map/ppermute | solution.py:11
  41.2 10.1 %collective-permute-start.2 = (bf16[136,512]{1,0:T(8,128)(2,1)S(1)}, bf16[136,512]{1,0:T(8,128)(2,1)S(1)}, u32[]{:S(2)}, u32[]{:S(2)}) collective-permute-start(bf16[136,512]{1,0:T(8,128)(2,1)S(1)} %collective-permute-done.1.refs_4_), channel_id=1, source_target_pairs={{0,8},{8,16},{16,24},{24,32},{32,40},{40,48},{48,56},{56,64},{64,7... | collective-permute-start | bytes 417800 | tf_op jit(solution)/shard_map/ppermute | solution.py:11
  43.8 9.4 %collective-permute-start.6 = (bf16[136,512]{1,0:T(8,128)(2,1)S(1)}, bf16[136,512]{1,0:T(8,128)(2,1)S(1)}, u32[]{:S(2)}, u32[]{:S(2)}) collective-permute-start(bf16[136,512]{1,0:T(8,128)(2,1)S(1)} %collective-permute-done.5.refs_7_), channel_id=1, source_target_pairs={{0,504},{8,0},{16,8},{24,16},{32,24},{40,32},{48,40},{56,48},{64,5... | collective-permute-start | bytes 417800 | tf_op jit(solution)/shard_map/ppermute | solution.py:11
  53.3 0.8 copy-start.1
  54.1 0.7 copy-start.2
Sparse Core Ops, SparseCore 0:
  10.3 109.7 all-gather.1
